TPU v7x, 128 devices: a whole 4x4x4 slice. The times are simulated.
128 devices in a mesh: ra: 16 (over z, x), cb: 8 (over y, core).
Axes of the slice: x: 4, y: 4, z: 4, core: 2. Of those that a mesh axis runs over, the one named last changes fastest.
Arguments:
- inputs: bfloat16 [1536, 4096], P(None, 'ra'), may hold values from -12 to 12
- gate_weight: bfloat16 [2, 4096, 11264], P(None, 'ra', 'cb'), may hold values from -0.09375 to 0.09375
- up_weight: bfloat16 [2, 4096, 11264], P(None, 'ra', 'cb'), may hold values from -0.09375 to 0.09375
- down_weight: bfloat16 [2, 11264, 4096], P(None, 'cb', 'ra'), may hold values from -0.0546875 to 0.0546875
- norm_gain: float32 [2, 4096], P(None, 'ra'), may hold values from 0.05 to 8
- norm_shift: float32 [2, 4096], P(None, 'ra'), may hold values from -1.5 to 1.5
Outputs:
- outputs: bfloat16 [1536, 4096], P(None, 'ra')
All inputs are finite; a program needn't handle non-finite values.
Results may differ from a plain program's by a relative error of at most 0.04.
Values may be sent and summed in bfloat16 or wider, within the bound.
A program may use at most 64 MiB of HBM per device.

v0:
```python
import functools

import jax
import jax.numpy as jnp
from jax import lax
from jax.sharding import Mesh
from jax.sharding import PartitionSpec as P

LAYERS = 2
RA = ("ra_0", "ra_1")


RESIDUAL = 0.5
EPSILON = 1e-05


def in_blocks(shard, dim, peers):
    lengths = shard.shape
    parts = shard.reshape(*lengths[:dim], peers, lengths[dim] // peers, *lengths[dim + 1 :])
    return jnp.moveaxis(parts, dim, 0)


def sum_at_owner(shard, axis, dim):
    parts = in_blocks(shard, dim, lax.axis_size(axis))
    arrived = lax.all_to_all(parts, axis, split_axis=0, concat_axis=0, tiled=True)
    return arrived.astype(jnp.float32).sum(axis=0)


def over_axes(shard, axes):
    return functools.reduce(lax.psum, axes, shard)


def from_everyone(shard, axis):
    peers = lax.axis_size(axis)
    return lax.all_to_all(
        jnp.broadcast_to(shard[None], (peers, *shard.shape)), axis, 0, 0, tiled=True
    )


def in_order(parts, dim):
    parts = jnp.moveaxis(parts, 0, dim)
    lengths = parts.shape
    return parts.reshape(*lengths[:dim], lengths[dim] * lengths[dim + 1], *lengths[dim + 2 :])


def collect(shard, axis, dim):
    parts = from_everyone(shard, axis)
    return in_order(parts, dim)


def scale_rows(mixed_rows, row_sum, row_squares, gain_row, shift_row, full_width):
    mean_rows = row_sum / full_width
    var_rows = row_squares / full_width - mean_rows * mean_rows
    normed = (mixed_rows - mean_rows[:, None]) * lax.rsqrt(var_rows + EPSILON)[:, None]
    return (normed * gain_row + shift_row).astype(jnp.bfloat16)


def sublayer(stream, w_gate, w_up, w_down, gain_row, shift_row):
    columns = w_gate.shape[1]
    paired = jnp.concatenate((w_gate, w_up), axis=1)
    full_width = stream.shape[1] * lax.axis_size(RA)
    summed = lax.psum_scatter(
        jnp.dot(stream, paired, preferred_element_type=jnp.float32).astype(jnp.bfloat16),
        RA,
        scatter_dimension=0,
        tiled=True,
    ).astype(jnp.float32)
    hidden = (jax.nn.silu(summed[:, :columns]) * summed[:, columns:]).astype(jnp.bfloat16)
    partial_value = jnp.dot(
        lax.all_gather(hidden, RA, axis=0, tiled=True), w_down, preferred_element_type=jnp.float32
    )
    branch = sum_at_owner(partial_value.astype(jnp.bfloat16), "cb", 0)
    row_count = branch.shape[0]
    own_rows = lax.dynamic_slice_in_dim(stream, lax.axis_index("cb") * row_count, row_count, 0)
    mixed_rows = RESIDUAL * own_rows.astype(jnp.float32) + branch
    row_sum, row_squares = (
        over_axes(jnp.sum(mixed_rows, axis=1), RA),
        over_axes(jnp.sum(mixed_rows * mixed_rows, axis=1), RA),
    )
    normed = scale_rows(mixed_rows, row_sum, row_squares, gain_row, shift_row, full_width)
    return collect(normed, "cb", 0)


def per_device(inputs, gate_weight, up_weight, down_weight, norm_gain, norm_shift):
    stream = inputs
    for layer_index in range(LAYERS):
        stream = sublayer(
            stream,
            gate_weight[layer_index],
            up_weight[layer_index],
            down_weight[layer_index],
            norm_gain[layer_index],
            norm_shift[layer_index],
        )
    return stream


def solution(mesh):
    finer = Mesh(mesh.devices.reshape(4, 4, mesh.shape["cb"]), ("ra_0", "ra_1", "cb"))
    in_specs = (
        P(None, RA),
        P(None, RA, "cb"),
        P(None, RA, "cb"),
        P(None, "cb", RA),
        P(None, RA),
        P(None, RA),
    )
    out_specs = P(None, RA)
    return jax.shard_map(
        per_device, mesh=finer, in_specs=in_specs, out_specs=out_specs, check_vma=False
    )
```

profile of v0, /device:TPU:1, one launch (start us, length us, event | category | flops | bytes accessed | tf_op | source)
XLA Modules:
  0.0 432.4 jit_solution(12249550608006333865)
XLA Ops:
  6.5 2.0 slice_bitcast_fusion
  8.6 5.8 %fusion = bf16[1536,2816]{0,1:T(8,128)(2,1)} fusion(bf16[1536,256]{1,0:T(8,128)(2,1)S(1)} %copy-done, bf16[256,1408]{1,0:T(8,128)(2,1)S(1)} %get-tuple-element.20, bf16[256,1408]{1,0:T(8,128)(2,1)S(1)} %get-tuple-element.29), kind=kOutput, calls=%fused_computation.2 | convolution fusion | flops 2221801472 | bytes 10878976 | tf_op jit(solution)/shard_map/dot_general | solution.py:63
  14.4 11.5 %copy.11 = bf16[1536,2816]{1,0:T(8,128)(2,1)} copy(bf16[1536,2816]{0,1:T(8,128)(2,1)} %fusion) | data formatting | bytes 17301504
  26.0 88.4 %reduce-scatter.7.cloned.1.call-done = bf16[96,2816]{1,0:T(8,128)(2,1)} async-done(((bf16[1536,2816]{1,0:T(8,128)(2,1)}), bf16[96,2816]{1,0:T(8,128)(2,1)}) %reduce-scatter.7.cloned.1.call-update) | async-done | bytes 540688
  114.4 1.4 copy.12
  115.9 0.2 fusion.8
  116.1 0.9 copy.8
  117.0 52.8 %all-gather.3.cloned.1.call-done = bf16[1536,1408]{1,0:T(8,128)(2,1)} async-done(((bf16[96,1408]{1,0:T(8,128)(2,1)}), bf16[1536,1408]{1,0:T(8,128)(2,1)}) %all-gather.3.cloned.1.call-update) | async-done | bytes 4325392 | tf_op jit(solution)/shard_map/all_gather | solution.py:70
  169.8 4.7 %convolution_convert_fusion.3 = bf16[1536,256]{1,0:T(8,128)(2,1)} fusion(bf16[1536,1408]{1,0:T(8,128)(2,1)} %all-gather.3.cloned.1.call-done, bf16[2,1408,256]{2,1,0:T(8,128)(2,1)} %param.9), kind=kOutput, calls=%fused_computation.4 | convolution fusion | flops 1107689472 | bytes 5832704 | tf_op jit(solution)/shard_map/dot_general | solution.py:69
  174.5 5.3 %all-to-all-start = ((bf16[8,192,256]{2,1,0:T(8,128)(2,1)}), bf16[8,192,256]{2,1,0:T(8,128)(2,1)S(1)}, u32[]{:S(2)}, u32[]{:S(2)}) async-start(bf16[8,192,256]{2,1,0:T(8,128)(2,1)} %bitcast.34), calls=%async_computation | async-start | bytes 1572864 | tf_op jit(solution)/shard_map/all_to_all | solution.py:25
  179.8 12.1 %all-to-all-done = bf16[8,192,256]{2,1,0:T(8,128)(2,1)S(1)} async-done(((bf16[8,192,256]{2,1,0:T(8,128)(2,1)}), bf16[8,192,256]{2,1,0:T(8,128)(2,1)S(1)}, u32[]{:S(2)}, u32[]{:S(2)}) %all-to-all-start) | async-done | bytes 786464 | tf_op jit(solution)/shard_map/all_to_all | solution.py:25
  191.9 0.1 convert_reduce_fusion.1
  192.0 0.2 fusion.13
  192.2 8.4 %all-reduce.3 = (f32[192]{0:T(256)S(1)}, f32[192]{0:T(256)S(1)}) all-reduce(f32[192]{0:T(256)S(1)} %get-tuple-element.8, f32[192]{0:T(256)S(1)} %get-tuple-element.7), channel_id=1, replica_groups=mesh['ra_0'=4,'ra_1'=4,'cb'=8] {'ra_0'}, use_global_device_ids=true, to_apply=%region_6.7 | all-reduce | flops 384 | bytes 3072 | tf_op jit(solution)/shard_map/psum | solution.py:30
  200.6 6.7 %all-reduce.1 = (f32[192]{0:T(256)S(1)}, f32[192]{0:T(256)S(1)}) all-reduce(f32[192]{0:T(256)S(1)} %get-tuple-element.15, f32[192]{0:T(256)S(1)} %get-tuple-element.16), channel_id=1, replica_groups=mesh['ra_0'=4,'ra_1'=4,'cb'=8] {'ra_1'}, use_global_device_ids=true, to_apply=%region_7.8 | all-reduce | flops 384 | bytes 3072 | tf_op jit(solution)/shard_map/psum | solution.py:30
  207.3 0.1 add_convert_fusion.1
  207.5 19.4 %all_to_all.20 = bf16[8,192,256]{2,1,0:T(8,128)(2,1)S(1)} all-to-all(bf16[8,192,256]{2,1,0:T(8,128)(2,1)S(1)} %broadcast_in_dim.4), channel_id=1, replica_groups=mesh['ra_0'=4,'ra_1'=4,'cb'=8] {'cb'}, dimensions={0} | all-to-all | bytes 1572864 | tf_op jit(solution)/shard_map/all_to_all | solution.py:35
  226.9 5.7 %convolution_convert_fusion = bf16[1536,2816]{1,0:T(8,128)(2,1)} fusion(bf16[1536,256]{1,0:T(8,128)(2,1)S(1)} %bitcast.30, bf16[256,1408]{1,0:T(8,128)(2,1)S(1)} %get-tuple-element.19, bf16[256,1408]{1,0:T(8,128)(2,1)S(1)} %get-tuple-element.30), kind=kOutput, calls=%fused_computation | convolution fusion | flops 2221801472 | bytes 10878976 | tf_op jit(solution)/shard_map/dot_general | solution.py:63
  232.7 81.0 %reduce-scatter.9.cloned.1.call-done = bf16[96,2816]{1,0:T(8,128)(2,1)} async-done(((bf16[1536,2816]{1,0:T(8,128)(2,1)}), bf16[96,2816]{1,0:T(8,128)(2,1)}) %reduce-scatter.9.cloned.1.call-update) | async-done | bytes 540688
  313.7 1.4 copy.14
  315.2 0.2 fusion.7
  315.4 0.9 copy.10
  316.3 52.8 %all-gather.5.cloned.1.call-done = bf16[1536,1408]{1,0:T(8,128)(2,1)} async-done(((bf16[96,1408]{1,0:T(8,128)(2,1)}), bf16[1536,1408]{1,0:T(8,128)(2,1)}) %all-gather.5.cloned.1.call-update) | async-done | bytes 4325392 | tf_op jit(solution)/shard_map/all_gather | solution.py:70
  369.1 3.8 convolution_convert_fusion.2
  372.9 17.1 %all_to_all.21 = bf16[8,192,256]{2,1,0:T(8,128)(2,1)S(1)} all-to-all(bf16[8,192,256]{2,1,0:T(8,128)(2,1)S(1)} %bitcast.35), channel_id=1, replica_groups=mesh['ra_0'=4,'ra_1'=4,'cb'=8] {'cb'}, dimensions={0} | all-to-all | bytes 1572864 | tf_op jit(solution)/shard_map/all_to_all | solution.py:25
  390.0 0.1 convert_reduce_fusion
  390.1 0.2 fusion.14
  390.2 8.4 %all-reduce.2 = (f32[192]{0:T(256)S(1)}, f32[192]{0:T(256)S(1)}) all-reduce(f32[192]{0:T(256)S(1)} %get-tuple-element.6, f32[192]{0:T(256)S(1)} %get-tuple-element.5), channel_id=1, replica_groups=mesh['ra_0'=4,'ra_1'=4,'cb'=8] {'ra_0'}, use_global_device_ids=true, to_apply=%region_14.15 | all-reduce | flops 384 | bytes 3072 | tf_op jit(solution)/shard_map/psum | solution.py:30
  398.6 6.8 %all-reduce = (f32[192]{0:T(256)S(1)}, f32[192]{0:T(256)S(1)}) all-reduce(f32[192]{0:T(256)S(1)} %get-tuple-element.13, f32[192]{0:T(256)S(1)} %get-tuple-element.14), channel_id=1, replica_groups=mesh['ra_0'=4,'ra_1'=4,'cb'=8] {'ra_1'}, use_global_device_ids=true, to_apply=%region_15.16 | all-reduce | flops 384 | bytes 3072 | tf_op jit(solution)/shard_map/psum | solution.py:30
  405.4 0.1 add_convert_fusion
  405.6 19.4 %all_to_all.22 = bf16[8,192,256]{2,1,0:T(8,128)(2,1)S(1)} all-to-all(bf16[8,192,256]{2,1,0:T(8,128)(2,1)S(1)} %broadcast_in_dim.5), channel_id=1, replica_groups=mesh['ra_0'=4,'ra_1'=4,'cb'=8] {'cb'}, dimensions={0} | all-to-all | bytes 1572864 | tf_op jit(solution)/shard_map/all_to_all | solution.py:35
  425.0 0.9 copy.16
  (22 shorter events, 0.5 us)
Async XLA Ops:
  6.5 2.1 copy-start
  6.5 107.8 %reduce-scatter.7.cloned.1.call-start = ((), (), s32[]{:S(2)}) async-start(), calls=%async_computation.8 | async-start | bytes 9191424
  25.9 143.9 %all-gather.3.cloned.1.call-start = ((), (), s32[]{:S(2)}) async-start(), calls=%async_computation.6 | async-start | bytes 4595712 | tf_op jit(solution)/shard_map/all_gather | solution.py:70
  174.5 5.3 %copy-start.1 = (f32[2,256]{1,0:T(2,128)S(1)}, f32[2,256]{1,0:T(2,128)}, u32[]{:S(2)}) copy-start(f32[2,256]{1,0:T(2,128)} %param.10) | copy-start | bytes 6148
  174.5 5.3 %copy-start.2 = (f32[2,256]{1,0:T(2,128)S(1)}, f32[2,256]{1,0:T(2,128)}, u32[]{:S(2)}) copy-start(f32[2,256]{1,0:T(2,128)} %param.11) | copy-start | bytes 6148
  174.5 17.4 %all-to-all-start = ((bf16[8,192,256]{2,1,0:T(8,128)(2,1)}), bf16[8,192,256]{2,1,0:T(8,128)(2,1)S(1)}, u32[]{:S(2)}, u32[]{:S(2)}) async-start(bf16[8,192,256]{2,1,0:T(8,128)(2,1)} %bitcast.34), calls=%async_computation | async-start | bytes 1572864 | tf_op jit(solution)/shard_map/all_to_all | solution.py:25
  179.7 133.9 %reduce-scatter.9.cloned.1.call-start = ((), (), s32[]{:S(2)}) async-start(), calls=%async_computation.9 | async-start | bytes 9191424
  232.6 136.5 %all-gather.5.cloned.1.call-start = ((), (), s32[]{:S(2)}) async-start(), calls=%async_computation.7 | async-start | bytes 4595712 | tf_op jit(solution)/shard_map/all_gather | solution.py:70
Sparse Core Ops, SparseCore 0:
  26.1 88.2 reduce-scatter.6
  117.1 52.6 all-gather.2
  232.7 80.9 reduce-scatter.8
  316.4 52.6 all-gather.4
where the time goes:
time: 433 us; the launch traced here: 432 us
  waiting for transfers between devices  287 us (66%)
  blocking collectives  86.1 us (20%)
  matrix products  20 us (5%)
  local copies, waits for them, and re-layouts  19.1 us (4%)
  between operations  13.3 us (3%)
  starting transfers between devices  5.34 us (1%)
    unnamed x6, waiting for transfers between devices  169 us
    all_gather x2, waiting for transfers between devices, sublayer(): lax.all_gather(hidden, RA, axis=0, tiled=True)  106 us
    all_to_all x2, blocking collectives, from_everyone(): lax.all_to_all(jnp.broadcast_to(shard[None], (peers, *shard.shape)), axis...  38.8 us
    psum x4, blocking collectives, over_axes(): return functools.reduce(lax.psum, axes, shard)  30.3 us
    all_to_all x1, blocking collectives, sum_at_owner(): lax.all_to_all(parts, axis, split_axis=0, concat_axis=0, tiled=True)  17.1 us
    unnamed x10, local copies, waits for them, and re-layouts  15.2 us
    all_to_all x1, waiting for transfers between devices, sum_at_owner(): lax.all_to_all(parts, axis, split_axis=0, concat_axis=0, tiled=True)  12.1 us
    dot_general x2, matrix products, sublayer(): jnp.dot(stream, paired, preferred_element_type=jnp.float32)  11.5 us
  transfers between devices with their start and end apart: 5, of which 5 were waited for; matrix products, arithmetic and copies ran while one was open for 0% of the time, Pallas kernels for 0%

commit v1 on v0

v1 whole, which is shorter than its diff:
```python
import functools

import jax
import jax.numpy as jnp
from jax import lax
from jax.experimental import pallas as pl
from jax.experimental.pallas import tpu as pltpu
from jax.sharding import PartitionSpec as P

MESH = pl.DeviceIdType.MESH
BF = jnp.bfloat16
F32 = jnp.float32
RESIDUAL = 0.5
EPSILON = 1e-05

T, D, FF, LAYERS = 1536, 4096, 11264, 2
NC = 3
TC = T // NC
ZB = TC // 4
ZH = ZB // 2
CB_ROWS = TC // 2
YB = TC // 8
YH = YB // 2
R = TC // 32
DB = D // 16
DQ = D // 4
FB = FF // 8
FS = 384
F_LAST = FB - FS

ZA0, ZA1, ZB0, ZB1, ZC0, ZC1 = range(6)
HF0, HF1, HB1, HB0, HG0, HG1 = range(6, 12)
CX = 12
YA0, YA1, YB0, YB1, YC0, YC1 = range(13, 19)
XR = 19
ST = 22
N_RS = 25
XG = 0
YF0, YF1, YK1, YK0, YG0, YG1 = range(3, 9)
DD = 9
N_AG = 13

PERIOD, LAYER_TIME, START = 9.5, 42.0, 18.0
OFFSETS = dict(A=0, B=4.3, C=8.5, D=11.6, E=13.7, F=16.2, G=19.5, H=22.3, I=26.5, J=29.2, K=33.5, L=36.6, M=39.4)


def order():
    timed = []
    for k in range(NC):
        for stage in "KLM":
            timed.append((START - LAYER_TIME + OFFSETS[stage] + 4.0 * k, (stage, -1, k)))
        for layer in range(LAYERS):
            for stage, offset in OFFSETS.items():
                timed.append((START + layer * LAYER_TIME + k * PERIOD + offset, (stage, layer, k)))
    timed.sort(key=lambda item: item[0])
    return [task for _, task in timed]


def kernel(
    x_hbm, wg_hbm, wu_hbm, wd_hbm, gain_hbm, shift_hbm, out_hbm,
    xs, wgu, wd, part, ra, rb, rc, hid, down, core_in, ya, yb, yc, ys, xr, mixed, st, st_in, nb, ov, ga, sh,
    rs_recv, rs_send, ag_recv, ag_send, w_recv, w_send, g_recv, g_send, local,
):
    ra_at, cb_at = lax.axis_index("ra"), lax.axis_index("cb")
    z, x = ra_at // 4, lax.rem(ra_at, 4)
    y, c = cb_at // 2, lax.rem(cb_at, 2)

    def turn(v, d):
        return lax.rem(v + d, 4)

    zp, zo, zm = turn(z, 1), turn(z, 2), turn(z, 3)
    yp, yo, ym = turn(y, 1), turn(y, 2), turn(y, 3)

    def at_z(v):
        return (v * 4 + x, cb_at)

    def at_x(v):
        return (z * 4 + v, cb_at)

    def at_y(v):
        return (ra_at, v * 2 + c)

    other = (ra_at, y * 2 + (1 - c))

    peers = [at_z(zp), at_z(zo), at_z(zm)] + [at_x(turn(x, d)) for d in (1, 2, 3)] + [at_y(yp), at_y(ym), other]
    barrier = pltpu.get_barrier_semaphore()
    for peer in peers:
        pl.semaphore_signal(barrier, inc=1, device_id=peer, device_id_type=MESH)
    pl.semaphore_wait(barrier, len(peers))

    sent = []

    def send(src, dst, send_sem, recv_sem, dev):
        copy = pltpu.make_async_remote_copy(
            src_ref=src, dst_ref=dst, send_sem=send_sem, recv_sem=recv_sem, device_id=dev, device_id_type=MESH
        )
        copy.start()
        sent.append(copy)

    def arrived(dst, recv_sem):
        pltpu.make_async_remote_copy(
            src_ref=dst, dst_ref=dst, send_sem=recv_sem, recv_sem=recv_sem, device_id=other, device_id_type=MESH
        ).wait_recv()

    def f_start(v):
        return pl.multiple_of(jnp.minimum(v * FS, F_LAST), 128)

    def d_cols(v):
        return pl.ds(pl.multiple_of(v * DB, DB), DB)

    def weight_views(l, what, dst, owner):
        units = pl.ds(f_start(dst), FS)
        if what == 0:
            return wg_hbm.at[l, :, units], wgu.at[l, d_cols(owner), pl.ds(0, FS)]
        if what == 1:
            return wu_hbm.at[l, :, units], wgu.at[l, d_cols(owner), pl.ds(FS, FS)]
        return wd_hbm.at[l, units, :], wd.at[l, :, d_cols(owner)]

    own_copies = {}

    def weights_send(l, what):
        for d in (1, 3, 2):
            src, dst = weight_views(l, what, turn(x, d), x)
            send(src, dst, w_send.at[l, what, d - 1], w_recv.at[l, what, d - 1], at_x(turn(x, d)))
        src, dst = weight_views(l, what, x, x)
        own_copies[l, what] = pltpu.make_async_copy(src, dst, local.at[l * 3 + what])
        own_copies[l, what].start()

    def weights_wait(l, what):
        for d in (1, 3, 2):
            _, dst = weight_views(l, what, x, turn(x, 4 - d))
            arrived(dst, w_recv.at[l, what, d - 1])
        own_copies[l, what].wait()

    def gathered(p, k, rows):
        if p < 2:
            return xs.at[p, k, rows, :]
        return ov.at[k, rows, :]

    def y_rows(cc, yy):
        return pl.ds(pl.multiple_of(cc * CB_ROWS + yy * YB, YB), YB)

    def y_half(cc, yy, h):
        return pl.ds(pl.multiple_of(cc * CB_ROWS + yy * YB + h * YH, YH), YH)

    def x_rows(xx):
        return pl.ds(pl.multiple_of(c * CB_ROWS + y * YB + xx * R, R), R)

    in_copies = []
    for k in range(NC):
        rows = pl.ds(pl.multiple_of(k * TC + c * CB_ROWS + y * YB, YB), YB)
        for d in (1, 3, 2):
            send(
                x_hbm.at[rows, :], xs.at[0, k, y_rows(c, y), d_cols(x)],
                ag_send.at[0, k, XG + d - 1], ag_recv.at[0, k, XG + d - 1], at_x(turn(x, d)),
            )
        copy = pltpu.make_async_copy(x_hbm.at[rows, :], xs.at[0, k, y_rows(c, y), d_cols(x)], local.at[6 + k])
        copy.start()
        in_copies.append(copy)
    weights_send(0, 0)
    weights_send(0, 1)
    for i, (src, dst) in enumerate(((gain_hbm, ga), (shift_hbm, sh))):
        for d in (1, 3, 2):
            send(src, dst.at[x], g_send.at[i, d - 1], g_recv.at[i, d - 1], at_x(turn(x, d)))
        copy = pltpu.make_async_copy(src, dst.at[x], local.at[6 + NC + i])
        copy.start()
        own_copies["g", i] = copy
    weights_send(0, 2)

    def stage_a(l, k):
        for j, (cc, yy) in enumerate(((1 - c, y), (1 - c, ym), (1 - c, yp), (1 - c, yo))):
            arrived(gathered(l, k, y_rows(cc, yy)), ag_recv.at[l, k, DD + j])
        if k == 0:
            weights_wait(l, 0)
            weights_wait(l, 1)

        def block(o):
            rows = pl.ds(pl.multiple_of(o * ZB, ZB), ZB)

            def columns(n, carry):
                cols = pl.ds(pl.multiple_of(n * 256, 256), 256)
                value = jnp.dot(xs[l, k, rows, :], wgu[l, :, cols], preferred_element_type=F32).astype(BF)
                part[l, k, o, 0, :, cols] = value[:ZH]
                part[l, k, o, 1, :, cols] = value[ZH:]
                return carry

            lax.fori_loop(0, 2 * FS // 256, columns, 0)

        sems = rs_send.at[l, k], rs_recv.at[l, k]
        block(zo)
        send(part.at[l, k, zo, 0], ra.at[l, k, 0], sems[0].at[ZA0], sems[1].at[ZA0], at_z(zp))
        send(part.at[l, k, zo, 1], ra.at[l, k, 1], sems[0].at[ZA1], sems[1].at[ZA1], at_z(zm))

        def rest(j, carry):
            block(lax.rem(z + 1 + j * 2, 4))
            return carry

        lax.fori_loop(0, 2, rest, 0)
        send(part.at[l, k, zp, 1], rb.at[l, k, 0], sems[0].at[ZB0], sems[1].at[ZB0], at_z(zp))
        send(part.at[l, k, zm, 0], rb.at[l, k, 1], sems[0].at[ZB1], sems[1].at[ZB1], at_z(zm))
        block(z)

    def stage_b(l, k):
        sems = rs_send.at[l, k], rs_recv.at[l, k]
        arrived(ra.at[l, k, 0], sems[1].at[ZA0])
        part[l, k, zp, 0] = (part[l, k, zp, 0].astype(F32) + ra[l, k, 0].astype(F32)).astype(BF)
        send(part.at[l, k, zp, 0], rc.at[l, k, 0], sems[0].at[ZC0], sems[1].at[ZC0], at_z(zp))
        arrived(ra.at[l, k, 1], sems[1].at[ZA1])
        part[l, k, zm, 1] = (part[l, k, zm, 1].astype(F32) + ra[l, k, 1].astype(F32)).astype(BF)
        send(part.at[l, k, zm, 1], rc.at[l, k, 1], sems[0].at[ZC1], sems[1].at[ZC1], at_z(zm))

    def stage_c(l, k):
        sems = rs_send.at[l, k], rs_recv.at[l, k]
        for h in (0, 1):
            arrived(rb.at[l, k, 1 - h], sems[1].at[(ZB1, ZB0)[h]])
            arrived(rc.at[l, k, h], sems[1].at[(ZC0, ZC1)[h]])
            total = part[l, k, z, h].astype(F32) + rc[l, k, h].astype(F32) + rb[l, k, 1 - h].astype(F32)
            gate, up = total[:, :FS], total[:, FS:]
            value = gate * jax.nn.sigmoid(gate) * up
            column = lax.broadcasted_iota(jnp.int32, (ZH, FS), 1)
            value = jnp.where(jnp.logical_and(x == 3, column < 4 * FS - FB), 0.0, value)
            hid[l, k, z, h] = value.astype(BF)
        for h in (0, 1):
            send(hid.at[l, k, z, h], hid.at[l, k, z, h], sems[0].at[(HF0, HF1)[h]], sems[1].at[(HF0, HF1)[h]], at_z(zp))
            g = 1 - h
            send(hid.at[l, k, z, g], hid.at[l, k, z, g], sems[0].at[(HB0, HB1)[g]], sems[1].at[(HB0, HB1)[g]], at_z(zm))

    def stage_d(l, k):
        sems = rs_send.at[l, k], rs_recv.at[l, k]
        arrived(hid.at[l, k, zm, 0], sems[1].at[HF0])
        send(hid.at[l, k, zm, 0], hid.at[l, k, zm, 0], sems[0].at[HG0], sems[1].at[HG0], at_z(zp))
        arrived(hid.at[l, k, zp, 1], sems[1].at[HB1])
        send(hid.at[l, k, zp, 1], hid.at[l, k, zp, 1], sems[0].at[HG1], sems[1].at[HG1], at_z(zm))

    def stage_e(l, k):
        sems = rs_send.at[l, k], rs_recv.at[l, k]
        arrived(hid.at[l, k, zm, 1], sems[1].at[HF1])
        arrived(hid.at[l, k, zp, 0], sems[1].at[HB0])
        arrived(hid.at[l, k, zo, 0], sems[1].at[HG0])
        arrived(hid.at[l, k, zo, 1], sems[1].at[HG1])
        if k == 0:
            weights_wait(l, 2)

        def half(cc):
            def columns(n, carry):
                cols = pl.ds(pl.multiple_of(n * 256, 256), 256)
                lhs = hid[l, k, pl.ds(cc * 2, 2)].reshape(CB_ROWS, FS)
                value = jnp.dot(lhs, wd[l, :, cols], preferred_element_type=F32).astype(BF)
                for yy in range(4):
                    for h in (0, 1):
                        at = yy * YB + h * YH
                        down[l, k, cc, yy, h, :, cols] = value[at:at + YH]
                return carry

            lax.fori_loop(0, DQ // 256, columns, 0)

        half(1 - c)
        send(down.at[l, k, 1 - c], core_in.at[l, k], sems[0].at[CX], sems[1].at[CX], other)
        half(c)

    def stage_f(l, k):
        sems = rs_send.at[l, k], rs_recv.at[l, k]
        arrived(core_in.at[l, k], sems[1].at[CX])

        def add(yy):
            for h in (0, 1):
                down[l, k, c, yy, h] = (
                    down[l, k, c, yy, h].astype(F32) + core_in[l, k, yy, h].astype(F32)
                ).astype(BF)

        add(yo)
        send(down.at[l, k, c, yo, 0], ya.at[l, k, 0], sems[0].at[YA0], sems[1].at[YA0], at_y(yp))
        send(down.at[l, k, c, yo, 1], ya.at[l, k, 1], sems[0].at[YA1], sems[1].at[YA1], at_y(ym))
        add(yp)
        send(down.at[l, k, c, yp, 1], yb.at[l, k, 0], sems[0].at[YB0], sems[1].at[YB0], at_y(yp))
        add(ym)
        send(down.at[l, k, c, ym, 0], yb.at[l, k, 1], sems[0].at[YB1], sems[1].at[YB1], at_y(ym))
        add(y)

    def stage_g(l, k):
        sems = rs_send.at[l, k], rs_recv.at[l, k]
        arrived(ya.at[l, k, 0], sems[1].at[YA0])
        down[l, k, c, yp, 0] = (down[l, k, c, yp, 0].astype(F32) + ya[l, k, 0].astype(F32)).astype(BF)
        send(down.at[l, k, c, yp, 0], yc.at[l, k, 0], sems[0].at[YC0], sems[1].at[YC0], at_y(yp))
        arrived(ya.at[l, k, 1], sems[1].at[YA1])
        down[l, k, c, ym, 1] = (down[l, k, c, ym, 1].astype(F32) + ya[l, k, 1].astype(F32)).astype(BF)
        send(down.at[l, k, c, ym, 1], yc.at[l, k, 1], sems[0].at[YC1], sems[1].at[YC1], at_y(ym))

    def stage_h(l, k):
        sems = rs_send.at[l, k], rs_recv.at[l, k]
        for h in (0, 1):
            arrived(yb.at[l, k, 1 - h], sems[1].at[(YB1, YB0)[h]])
            arrived(yc.at[l, k, h], sems[1].at[(YC0, YC1)[h]])
            total = down[l, k, c, y, h].astype(F32) + yc[l, k, h].astype(F32) + yb[l, k, 1 - h].astype(F32)
            ys[l, k, 2 * h] = total[:R].astype(BF)
            ys[l, k, 2 * h + 1] = total[R:].astype(BF)
        for d in (2, 1, 3):
            send(
                ys.at[l, k, turn(x, d)], xr.at[l, k, d - 1], sems[0].at[XR + d - 1], sems[1].at[XR + d - 1],
                at_x(turn(x, d)),
            )

    def stage_i(l, k):
        sems = rs_send.at[l, k], rs_recv.at[l, k]
        value = RESIDUAL * xs[l, k, x_rows(x), :].astype(F32) + ys[l, k, x].astype(F32)
        for d in (1, 3, 2):
            arrived(xr.at[l, k, d - 1], sems[1].at[XR + d - 1])
            value = value + xr[l, k, d - 1].astype(F32)
        mixed[l, k] = value
        row_sum = jnp.sum(value, axis=1, keepdims=True)
        row_squares = jnp.sum(value * value, axis=1, keepdims=True)
        lane = lax.broadcasted_iota(jnp.int32, (R, 128), 1)
        st[l, k] = jnp.where(lane == 0, row_sum, jnp.where(lane == 1, row_squares, 0.0))
        for d in (2, 1, 3):
            send(
                st.at[l, k], st_in.at[l, k, d - 1], sems[0].at[ST + d - 1], sems[1].at[ST + d - 1],
                at_z(turn(z, d)),
            )

    def stage_j(l, k):
        sems = rs_recv.at[l, k]
        if l == 0 and k == 0:
            for i, dst in enumerate((ga, sh)):
                for d in (1, 3, 2):
                    arrived(dst.at[turn(x, 4 - d)], g_recv.at[i, d - 1])
                own_copies["g", i].wait()
        stats = st[l, k]
        for d in (1, 3, 2):
            arrived(st_in.at[l, k, d - 1], sems.at[ST + d - 1])
            stats = stats + st_in[l, k, d - 1]
        mean = stats[:, 0:1] / D
        var = stats[:, 1:2] / D - mean * mean
        scale = lax.rsqrt(var + EPSILON)
        for q in range(4):
            cols = slice(q * DB, (q + 1) * DB)
            normed = (mixed[l, k, :, cols] - mean) * scale
            value = (normed * ga[q, l:l + 1, :] + sh[q, l:l + 1, :]).astype(BF)
            if l + 1 < LAYERS:
                xs[l + 1, k, x_rows(x), cols] = value
            else:
                nb[k, q] = value
        if l + 1 == LAYERS:
            ov[k, x_rows(x), :] = nb[k, x]
        for d in (2, 1, 3):
            src = xs.at[l + 1, k, x_rows(x), :] if l + 1 < LAYERS else nb.at[k, turn(x, d)]
            send(
                src, gathered(l + 1, k, x_rows(x)), ag_send.at[l + 1, k, XG + d - 1],
                ag_recv.at[l + 1, k, XG + d - 1], at_x(turn(x, d)),
            )

    def stage_k(l, k):
        p = l + 1
        sems = ag_send.at[p, k], ag_recv.at[p, k]
        for d in (1, 3, 2):
            owner = turn(x, 4 - d)
            if p == 0:
                arrived(xs.at[0, k, y_rows(c, y), d_cols(owner)], sems[1].at[XG + d - 1])
            else:
                arrived(gathered(p, k, x_rows(owner)), sems[1].at[XG + d - 1])
        if p == 0:
            in_copies[k].wait()
        for h in (0, 1):
            ref = gathered(p, k, y_half(c, y, h))
            send(ref, ref, sems[0].at[(YF0, YF1)[h]], sems[1].at[(YF0, YF1)[h]], at_y(yp))
            g = 1 - h
            ref = gathered(p, k, y_half(c, y, g))
            send(ref, ref, sems[0].at[(YK0, YK1)[g]], sems[1].at[(YK0, YK1)[g]], at_y(ym))
        ref = gathered(p, k, y_rows(c, y))
        send(ref, ref, sems[0].at[DD], sems[1].at[DD], other)

    def stage_l(l, k):
        p = l + 1
        sems = ag_send.at[p, k], ag_recv.at[p, k]
        ref = gathered(p, k, y_half(c, ym, 0))
        arrived(ref, sems[1].at[YF0])
        send(ref, ref, sems[0].at[YG0], sems[1].at[YG0], at_y(yp))
        ref = gathered(p, k, y_half(c, yp, 1))
        arrived(ref, sems[1].at[YK1])
        send(ref, ref, sems[0].at[YG1], sems[1].at[YG1], at_y(ym))

    def stage_m(l, k):
        p = l + 1
        sems = ag_send.at[p, k], ag_recv.at[p, k]
        for j, (yy, last, slot) in enumerate(((ym, 1, YF1), (yp, 0, YK0))):
            arrived(gathered(p, k, y_half(c, yy, last)), sems[1].at[slot])
            ref = gathered(p, k, y_rows(c, yy))
            send(ref, ref, sems[0].at[DD + 1 + j], sems[1].at[DD + 1 + j], other)
        arrived(gathered(p, k, y_half(c, yo, 0)), sems[1].at[YG0])
        arrived(gathered(p, k, y_half(c, yo, 1)), sems[1].at[YG1])
        ref = gathered(p, k, y_rows(c, yo))
        send(ref, ref, sems[0].at[DD + 3], sems[1].at[DD + 3], other)

    stages = dict(
        A=stage_a, B=stage_b, C=stage_c, D=stage_d, E=stage_e, F=stage_f, G=stage_g, H=stage_h, I=stage_i,
        J=stage_j, K=stage_k, L=stage_l, M=stage_m,
    )
    later_weights = {("A", 0, 0): 0, ("A", 0, 1): 1, ("A", 0, 2): 2}
    for stage, l, k in order():
        stages[stage](l, k)
        if (stage, l, k) in later_weights:
            weights_send(1, later_weights[stage, l, k])

    out_copies = []
    for k in range(NC):
        for j, (cc, yy) in enumerate(((1 - c, y), (1 - c, ym), (1 - c, yp), (1 - c, yo))):
            arrived(gathered(2, k, y_rows(cc, yy)), ag_recv.at[2, k, DD + j])
        copy = pltpu.make_async_copy(ov.at[k], out_hbm.at[pl.ds(k * TC, TC), :], local.at[8 + NC + k])
        copy.start()
        out_copies.append(copy)
    for copy in sent:
        copy.wait_send()
    for copy in out_copies:
        copy.wait()


def solution(mesh):
    dma = pltpu.SemaphoreType.DMA

    def per_device(inputs, gate_weight, up_weight, down_weight, norm_gain, norm_shift):
        any_space = pl.BlockSpec(memory_space=pl.ANY)
        return pl.pallas_call(
            kernel,
            out_shape=jax.ShapeDtypeStruct((T, DB), BF),
            in_specs=[any_space] * 6,
            out_specs=any_space,
            scratch_shapes=[
                pltpu.VMEM((2, NC, TC, DQ), BF),
                pltpu.VMEM((2, DQ, 2 * FS), BF),
                pltpu.VMEM((2, FS, DQ), BF),
                pltpu.VMEM((2, NC, 4, 2, ZH, 2 * FS), BF),
                pltpu.VMEM((2, NC, 2, ZH, 2 * FS), BF),
                pltpu.VMEM((2, NC, 2, ZH, 2 * FS), BF),
                pltpu.VMEM((2, NC, 2, ZH, 2 * FS), BF),
                pltpu.VMEM((2, NC, 4, 2, ZH, FS), BF),
                pltpu.VMEM((2, NC, 2, 4, 2, YH, DQ), BF),
                pltpu.VMEM((2, NC, 4, 2, YH, DQ), BF),
                pltpu.VMEM((2, NC, 2, YH, DQ), BF),
                pltpu.VMEM((2, NC, 2, YH, DQ), BF),
                pltpu.VMEM((2, NC, 2, YH, DQ), BF),
                pltpu.VMEM((2, NC, 4, R, DQ), BF),
                pltpu.VMEM((2, NC, 3, R, DQ), BF),
                pltpu.VMEM((2, NC, R, DQ), F32),
                pltpu.VMEM((2, NC, R, 128), F32),
                pltpu.VMEM((2, NC, 3, R, 128), F32),
                pltpu.VMEM((NC, 4, R, DB), BF),
                pltpu.VMEM((NC, TC, DB), BF),
                pltpu.VMEM((4, 2, DB), F32),
                pltpu.VMEM((4, 2, DB), F32),
                dma((2, NC, N_RS)),
                dma((2, NC, N_RS)),
                dma((3, NC, N_AG)),
                dma((3, NC, N_AG)),
                dma((2, 3, 3)),
                dma((2, 3, 3)),
                dma((2, 3)),
                dma((2, 3)),
                dma((8 + 2 * NC,)),
            ],
            compiler_params=pltpu.CompilerParams(
                collective_id=0, has_side_effects=True, vmem_limit_bytes=62 * 1024 * 1024
            ),
        )(inputs, gate_weight, up_weight, down_weight, norm_gain, norm_shift)

    return jax.shard_map(
        per_device,
        mesh=mesh,
        in_specs=(P(None, "ra"), P(None, "ra", "cb"), P(None, "ra", "cb"), P(None, "cb", "ra"), P(None, "ra"), P(None, "ra")),
        out_specs=P(None, "ra"),
        check_vma=False,
    )
```

time: 433 us -> 178 us (0.41)
  waiting for transfers between devices: 287 us -> 0 us
  Pallas kernels: 0 us -> 176 us
  blocking collectives: 86.1 us -> 0 us
  matrix products: 20 us -> 0 us
  local copies, waits for them, and re-layouts: 19.1 us -> 2.06 us
  between operations: 13.3 us -> 0.01 us
  starting transfers between devices: 5.34 us -> 0 us
    pallas_call x0 -> x1, Pallas kernels: none -> 176 us  [per_device(): pl.pallas_call(kernel, out_shape=jax.ShapeDtypeStruct((T, DB), BF), in_sp...]
    unnamed x6 -> x0, waiting for transfers between devices: 169 us -> none
    all_gather x2 -> x0, waiting for transfers between devices: 106 us -> none  [sublayer(): lax.all_gather(hidden, RA, axis=0, tiled=True)]
    all_to_all x3 -> x0, blocking collectives: 55.8 us -> none  [the longest x2 38.8 us: from_everyone(): lax.all_to_all(jnp.broadcast_to(shard[None], (peers, *shard.shape)), axis...]
    psum x4 -> x0, blocking collectives: 30.3 us -> none  [over_axes(): return functools.reduce(lax.psum, axes, shard)]
    dot_general x4 -> x0, matrix products: 20 us -> none  [the longest x2 11.5 us: sublayer(): jnp.dot(stream, paired, preferred_element_type=jnp.float32)]
    unnamed x10 -> x1, local copies, waits for them, and re-layouts: 15.2 us -> 2.06 us
    all_to_all x1 -> x0, waiting for transfers between devices: 12.1 us -> none  [sum_at_owner(): lax.all_to_all(parts, axis, split_axis=0, concat_axis=0, tiled=True)]
  transfers between devices with their start and end apart: 5 -> 0, of which waited for: 5 -> 0; matrix products, arithmetic and copies ran while one was open for 0% -> 0% of each run, Pallas kernels for 0% -> 0%
where the time goes in v1:
time: 178 us
  Pallas kernels  176 us (99%)
  local copies, waits for them, and re-layouts  2.06 us (1%)
    pallas_call x1, Pallas kernels, per_device(): pl.pallas_call(kernel, out_shape=jax.ShapeDtypeStruct((T, DB), BF), in_sp...  176 us

profile of v1, /device:TPU:1, one launch (start us, length us, event | category | flops | bytes accessed | tf_op | source)
XLA Modules:
  0.0 177.8 jit_solution(14424558552008607529)
XLA Ops:
  0.0 175.8 %shard_map.64 = bf16[1536,256]{1,0:T(8,128)(2,1)} custom-call(bf16[1536,256]{1,0:T(8,128)(2,1)} %x_hbm.1, bf16[2,256,1408]{2,1,0:T(8,128)(2,1)} %wg_hbm.1, bf16[2,256,1408]{2,1,0:T(8,128)(2,1)} %wu_hbm.1, bf16[2,1408,256]{2,1,0:T(8,128)(2,1)} %wd_hbm.1, f32[2,256]{1,0:T(2,128)} %gain_hbm.1, f32[2,256]{1,0:T(2,128)} %shift_hbm.1), custom_call_target="tpu_custom_call" | custom-call | tf_op jit(solution)/shard_map/pallas_call | solution.py:421
  175.8 2.1 %copy.8 = bf16[1536,256]{1,0:T(8,128)(2,1)} copy(bf16[1536,256]{1,0:T(8,128)(2,1)} %shard_map.64) | data formatting | bytes 1572864

commit v2 on v0

v2 whole, which is shorter than its diff:
```python
import jax
import jax.numpy as jnp
from jax import lax
from jax.experimental import pallas as pl
from jax.experimental.pallas import tpu as pltpu
from jax.sharding import PartitionSpec as P

MESH = pl.DeviceIdType.MESH
BF = jnp.bfloat16
F32 = jnp.float32
RESIDUAL = 0.5
EPSILON = 1e-05

T, D, FF, LAYERS = 1536, 4096, 11264, 2
TCORE = T // 2
NC = 3
TC = TCORE // NC
ZB = TC // 4
ZH = ZB // 2
YB = TC // 4
YH = YB // 2
R = TC // 16
DB = D // 16
DQ = D // 4
UT = 128
NJ = 3
NT = 2 * NJ
TILES = FF // 8 // UT
SHARED = 4 * NJ - TILES

ZA0, ZA1, ZB0, ZB1, ZC0, ZC1, HF0, HF1, HB1, HB0, HG0, HG1 = range(12)
N_Z = 12
YA0, YA1, YB0, YB1, YC0, YC1 = range(6)
XR = 6
ST = 9
N_Y = 12
XG = 0
YF0, YF1, YK1, YK0, YG0, YG1 = range(3, 9)
DD = 9
N_AG = 13
WM, WP, WRM, WRP, WOM, WOP, WD = range(7)
N_W = 10

HOP = {1: 1.8, 2: 2.6}
CORE_HOP = 1.0
FROM_HBM = 1.1
LINK = 46.6e3
CORE_LINK = 500e3
TIMES = dict(A=0.5, B=0.1, C=0.2, D=0.05, E=0.9, G=0.12, H=0.15, I=0.25, J=0.3, K=0.06, L=0.06, M=0.03, W=0.1, V=0.05, U=0.08)


SLACK = dict(A=0.5, E=0.5, W=0.7)


def plan():
    tasks = {}
    gu, dn = DB * UT * 2, NJ * UT * DB * 2
    for l in range(LAYERS):
        for j in range(NJ + 1):
            size = 2 * gu if j < NJ else dn
            tasks["W", l, j] = ([], [
                (("wrm", l, j), "x+", size // 2, 1), (("wrp", l, j), "x-", size // 2, 1),
                (("wm", l, j), "x+", size, 1), (("wp", l, j), "x-", size, 1), (("wd", l, j), "c", size, 0),
            ])
            tasks["V", l, j] = ([("wrm", l, j), ("wrp", l, j)], [
                (("wom", l, j), "x+", size // 2, 1), (("wop", l, j), "x-", size // 2, 1)])
            tasks["U", l, j] = ([("wm", l, j), ("wp", l, j), ("wom", l, j), ("wop", l, j)], [(("wu", l, j), "c", 3 * size, 0)])
    zs, hs = ZH * 4 * UT * 2, ZH * 2 * UT * 2
    for k in range(NC):
        for p in range(LAYERS + 1):
            ys = YH * (DQ if p < LAYERS else DB) * 2
            sends = [(("yf", p, k), "y+", ys, 1), (("yk", p, k), "y-", ys, 1), (("yf1", p, k), "y+", ys, 1), (("yk1", p, k), "y-", ys, 1)]
            tasks["K", p - 1, k] = ([("xg", p, k)], sends)
            tasks["L", p - 1, k] = ([("yf", p, k), ("yk", p, k)], [(("yg", p, k), "y+", ys, 1), (("yg1", p, k), "y-", ys, 1)])
        for l in range(LAYERS):
            for j in range(NJ):
                need = [("yg", l, k), ("yg1", l, k), ("yf1", l, k), ("yk1", l, k)] + [("wd", l, j), ("wu", l, j)]
                tasks["A", l, k, j] = (need, [
                    (("za", l, k, j), "z+", zs, 1), (("za1", l, k, j), "z-", zs, 1),
                    (("zb", l, k, j), "z+", zs, 1), (("zb1", l, k, j), "z-", zs, 1)])
                tasks["B", l, k, j] = ([("za", l, k, j), ("za1", l, k, j)], [
                    (("zc", l, k, j), "z+", zs, 1), (("zc1", l, k, j), "z-", zs, 1)])
                tasks["C", l, k, j] = ([(m, l, k, j) for m in ("zb", "zb1", "zc", "zc1")], [
                    (("hf", l, k, j), "z+", hs, 1), (("hk", l, k, j), "z-", hs, 1),
                    (("hf1", l, k, j), "z+", hs, 1), (("hk1", l, k, j), "z-", hs, 1)])
                tasks["D", l, k, j] = ([("hf", l, k, j), ("hk", l, k, j)], [
                    (("hg", l, k, j), "z+", hs, 1), (("hg1", l, k, j), "z-", hs, 1)])
            ys, xsz = YH * DQ * 2, R * DQ * 2
            tasks["E", l, k] = ([(m, l, k, j) for m in ("hf1", "hk1", "hg", "hg1") for j in range(NJ)] + [("wd", l, NJ), ("wu", l, NJ)], [
                (("ya", l, k), "y+", ys, 1), (("ya1", l, k), "y-", ys, 1), (("yb", l, k), "y+", ys, 1), (("yb1", l, k), "y-", ys, 1)])
            tasks["G", l, k] = ([("ya", l, k), ("ya1", l, k)], [(("yc", l, k), "y+", ys, 1), (("yc1", l, k), "y-", ys, 1)])
            three = lambda m, size, axis: [((m, l, k, 2), axis + "+", size, 2), ((m, l, k, 1), axis + "+", size, 1), ((m, l, k, 3), axis + "-", size, 1)]
            tasks["H", l, k] = ([(m, l, k) for m in ("yb", "yb1", "yc", "yc1")], three("xr", xsz, "x"))
            tasks["I", l, k] = ([("xr", l, k, d) for d in (1, 2, 3)], three("st", R * 512, "z"))
            tasks["J", l, k] = ([("st", l, k, d) for d in (1, 2, 3)], [
                (("xg2", l + 1, k), "x+", xsz if l + 1 < LAYERS else xsz // 4, 2),
                (("xg", l + 1, k), "x+", xsz if l + 1 < LAYERS else xsz // 4, 1),
                (("xg3", l + 1, k), "x-", xsz if l + 1 < LAYERS else xsz // 4, 1)])
            tasks["K", l, k][0].extend([("xg2", l + 1, k), ("xg3", l + 1, k)])
    return tasks


def order(report=None):
    tasks = plan()
    maker = {m[0]: t for t, (_, sends) in tasks.items() for m in sends}
    rank = {}

    def rest(task):
        if task not in rank:
            rank[task] = TIMES[task[0]] + max((rest(u) + 2.0 for u in users.get(task, ())), default=0.0)
        return rank[task]

    users = {}
    for t, (needs, _) in tasks.items():
        for m in needs:
            if m in maker:
                users.setdefault(maker[m], set()).add(t)
    arrive, free = {}, {}

    def transmit(sends, now, hbm=0.0):
        for m, link, size, hops in sends:
            if link == "c":
                done = max(now, free.get(link, 0.0)) + size / CORE_LINK
                arrive[m] = done + CORE_HOP + hbm
            else:
                done = max(now, free.get(link, 0.0)) + size * hops / LINK
                arrive[m] = done + HOP[hops] + hbm
            free[link] = done

    now = 3.5
    done, out = set(), []
    x_in = YB * DB * 2
    for k in range(NC):
        transmit([(("xg2", 0, k), "x+", x_in, 2), (("xg", 0, k), "x+", x_in, 1), (("xg3", 0, k), "x-", x_in, 1)], now, FROM_HBM)
        tasks["K", -1, k][0].extend([("xg2", 0, k), ("xg3", 0, k)])
        if k == 0:
            transmit(tasks["W", 0, 0][1], now, FROM_HBM)
            done.add(("W", 0, 0))
    left = [t for t in tasks if t not in done]
    after = {}
    while left:
        ready = []
        for t in left:
            needs = tasks[t][0]
            at = None
            if t[0] == "W":
                before = ("W", t[1], t[2] - 1) if t[2] else ("W", t[1] - 1, NJ)
                if before in done:
                    at = max(free["x+"], free["x-"]) - SLACK["W"]
            elif all(m in arrive for m in needs):
                at = max((arrive[m] for m in needs), default=0.0)
                if t[0] in SLACK:
                    at = max(at, max(free.get(m[1], 0.0) for m in tasks[t][1]) - SLACK[t[0]])
            if at is not None:
                ready.append((at, t))
        at, t = min(ready, key=lambda r: (max(r[0], now), -rest(r[1]), r[1][1:]))
        begin = max(now, at)
        now = begin + TIMES[t[0]]
        transmit(tasks[t][1], now, FROM_HBM if t[0] == "W" else 0.0)
        left.remove(t)
        done.add(t)
        out.append(t)
        if report is not None:
            report.append((begin, now, t))
    return out


def kernel(
    x_hbm, wg_hbm, wu_hbm, wd_hbm, gain_hbm, shift_hbm, out_hbm,
    xs, wgu, wd, rel, rel_d, part, ra, rb, rc, hid, down, ya, yb, yc, ys, xr, mixed, st, st_in, nb, ov, ga, sh,
    z_recv, z_send, y_recv, y_send, ag_recv, ag_send, w_recv, w_send, g_recv, g_send, local,
):
    ra_at, cb_at = lax.axis_index("ra"), lax.axis_index("cb")
    z, x = ra_at // 4, lax.rem(ra_at, 4)
    y, c = cb_at // 2, lax.rem(cb_at, 2)

    def turn(v, d):
        return lax.rem(v + d, 4)

    zp, zo, zm = turn(z, 1), turn(z, 2), turn(z, 3)
    yp, yo, ym = turn(y, 1), turn(y, 2), turn(y, 3)
    xp, xo, xm = turn(x, 1), turn(x, 2), turn(x, 3)

    def at_z(v):
        return (v * 4 + x, cb_at)

    def at_x(v):
        return (z * 4 + v, cb_at)

    def at_y(v):
        return (ra_at, v * 2 + c)

    other = (ra_at, y * 2 + (1 - c))

    peers = [at_z(zp), at_z(zo), at_z(zm), at_x(xp), at_x(xo), at_x(xm), at_y(yp), at_y(ym), other]
    barrier = pltpu.get_barrier_semaphore()
    for peer in peers:
        pl.semaphore_signal(barrier, inc=1, device_id=peer, device_id_type=MESH)
    pl.semaphore_wait(barrier, len(peers))

    waits = []

    def start(src, dst, send_sem, recv_sem, dev):
        copy = pltpu.make_async_remote_copy(
            src_ref=src, dst_ref=dst, send_sem=send_sem, recv_sem=recv_sem, device_id=dev, device_id_type=MESH
        )
        copy.start()
        return copy

    def send(src, dst, sems, slot, dev):
        waits.append(start(src, dst, sems[0].at[slot], sems[1].at[slot], dev).wait_send)

    def described(ref, sem):
        return pltpu.make_async_remote_copy(
            src_ref=ref, dst_ref=ref, send_sem=sem, recv_sem=sem, device_id=other, device_id_type=MESH
        )

    def arrived(dst, recv_sem):
        described(dst, recv_sem).wait_recv()

    def d_cols(v):
        return pl.ds(pl.multiple_of(v * DB, DB), DB)

    def tile_of(v):
        return jnp.minimum(v * NJ, TILES - NJ)

    def units(v, j):
        return pl.ds(pl.multiple_of((tile_of(v) + j) * UT, UT), UT)

    def gu_dst(l, j, cc, owner):
        return wgu.at[l, 2 * j + cc, d_cols(owner), :]

    def gu_half(l, j, cc, owner, what):
        return wgu.at[l, 2 * j + cc, d_cols(owner), pl.ds(what * UT, UT)]

    def d_dst(l, cc, owner):
        return wd.at[l, :, cc, :, d_cols(owner)]

    def d_half(l, cc, owner, h):
        return wd.at[l, :, cc, pl.ds(h * 64, 64), d_cols(owner)]

    local_waits = {}

    def w_sems(l, j):
        return w_send.at[l, j], w_recv.at[l, j]

    def stage_w(l, j):
        sems = w_sems(l, j)
        if j < NJ:
            send(wg_hbm.at[l, :, units(xo, j)], rel.at[l, j, 0], sems, WRM, at_x(xp))
            send(wu_hbm.at[l, :, units(xo, j)], rel.at[l, j, 1], sems, WRP, at_x(xm))
            for dev, dst_x, slot in ((at_x(xp), xp, WM), (at_x(xm), xm, WP)):
                for what, src in enumerate((wg_hbm, wu_hbm)):
                    start(src.at[l, :, units(dst_x, j)], gu_half(l, j, c, x, what), sems[0].at[slot], sems[1].at[slot], dev)
                waits.append(described(gu_dst(l, j, c, x), sems[0].at[slot]).wait_send)
            for what, src in enumerate((wg_hbm, wu_hbm)):
                start(src.at[l, :, units(x, j)], gu_half(l, j, c, x, what), sems[0].at[WD], sems[1].at[WD], other)
            waits.append(described(gu_dst(l, j, c, x), sems[0].at[WD]).wait_send)
            mine = []
            for what, src in enumerate((wg_hbm, wu_hbm)):
                copy = pltpu.make_async_copy(
                    src.at[l, :, units(x, j)], gu_half(l, j, c, x, what), local.at[l * 7 + j * 2 + what]
                )
                copy.start()
                mine.append(copy.wait)
            local_waits[l, j] = mine
        else:
            def src(v, h=None):
                if h is None:
                    return wd_hbm.at[l, pl.ds(tile_of(v), NJ)]
                return wd_hbm.at[l, pl.ds(tile_of(v), NJ), pl.ds(h * 64, 64)]

            send(src(xo, 0), rel_d.at[l, 0], sems, WRM, at_x(xp))
            send(src(xo, 1), rel_d.at[l, 1], sems, WRP, at_x(xm))
            send(src(xp), d_dst(l, c, x), sems, WM, at_x(xp))
            send(src(xm), d_dst(l, c, x), sems, WP, at_x(xm))
            send(src(x), d_dst(l, c, x), sems, WD, other)
            copy = pltpu.make_async_copy(src(x), d_dst(l, c, x), local.at[l * 7 + 6])
            copy.start()
            local_waits[l, j] = [copy.wait]

    def relay_ref(l, j, h):
        return rel.at[l, j, h] if j < NJ else rel_d.at[l, h]

    def w_half(l, j, cc, owner, h):
        return gu_half(l, j, cc, owner, h) if j < NJ else d_half(l, cc, owner, h)

    def w_whole(l, j, cc, owner):
        return gu_dst(l, j, cc, owner) if j < NJ else d_dst(l, cc, owner)

    def stage_v(l, j):
        sems = w_sems(l, j)
        arrived(relay_ref(l, j, 0), sems[1].at[WRM])
        send(relay_ref(l, j, 0), w_half(l, j, c, xm, 0), sems, WOM, at_x(xp))
        arrived(relay_ref(l, j, 1), sems[1].at[WRP])
        send(relay_ref(l, j, 1), w_half(l, j, c, xp, 1), sems, WOP, at_x(xm))

    def stage_u(l, j):
        sems = w_sems(l, j)
        for n, (owner, slot) in enumerate(((xm, WM), (xp, WP))):
            ref = w_whole(l, j, c, owner)
            arrived(ref, sems[1].at[slot])
            send(ref, ref, sems, WD + 1 + n, other)
        arrived(w_half(l, j, c, xo, 0), sems[1].at[WOM])
        arrived(w_half(l, j, c, xo, 1), sems[1].at[WOP])
        ref = w_whole(l, j, c, xo)
        send(ref, ref, sems, WD + 3, other)

    def weights_ready(l, j):
        for wait in local_waits[l, j]:
            wait()
        for n, owner in enumerate((x, xm, xp)):
            arrived(w_whole(l, j, 1 - c, owner), w_recv.at[l, j, WD + n])
        arrived(w_whole(l, j, 1 - c, xo), w_recv.at[l, j, WD + 3])

    def gathered(p, k, at, rows, cc=None):
        if p < 2:
            return xs.at[p, k, pl.ds(pl.multiple_of(at, rows), rows), :]
        base = (c if cc is None else cc) * TCORE + k * TC
        return ov.at[pl.ds(pl.multiple_of(base + at, rows), rows), :]

    def x_rows(v):
        return y * YB + v * R

    in_copies = []

    def input_send(k):
        rows = pl.ds(pl.multiple_of(c * TCORE + k * TC + y * YB, YB), YB)
        dst = xs.at[0, k, pl.ds(pl.multiple_of(y * YB, YB), YB), d_cols(x)]
        for d in (2, 1, 3):
            send(x_hbm.at[rows, :], dst, (ag_send.at[0, k], ag_recv.at[0, k]), XG + d - 1, at_x(turn(x, d)))
        copy = pltpu.make_async_copy(x_hbm.at[rows, :], dst, local.at[14 + k])
        copy.start()
        in_copies.append(copy)

    for k in range(NC):
        input_send(k)
        if k == 0:
            stage_w(0, 0)
    gain_copies = []
    for i, (src, dst) in enumerate(((gain_hbm, ga), (shift_hbm, sh))):
        for d in (1, 3, 2):
            send(src, dst.at[x], (g_send.at[i], g_recv.at[i]), d - 1, at_x(turn(x, d)))
        copy = pltpu.make_async_copy(src, dst.at[x], local.at[14 + NC + i])
        copy.start()
        gain_copies.append(copy)

    def z_sems(l, k, j):
        return z_send.at[l, k, j], z_recv.at[l, k, j]

    def y_sems(l, k):
        return y_send.at[l, k], y_recv.at[l, k]

    def ag_sems(p, k):
        return ag_send.at[p, k], ag_recv.at[p, k]

    def stage_a(l, k, j):
        if j == 0:
            sems = ag_sems(l, k)
            arrived(gathered(l, k, ym * YB + YH, YH), sems[1].at[YF1])
            arrived(gathered(l, k, yp * YB, YH), sems[1].at[YK0])
            arrived(gathered(l, k, yo * YB, YH), sems[1].at[YG0])
            arrived(gathered(l, k, yo * YB + YH, YH), sems[1].at[YG1])
        if k == 0:
            weights_ready(l, j)

        def columns(n, carry):
            cols = pl.ds(pl.multiple_of(n * 256, 256), 256)
            value = jnp.dot(xs[l, k], wgu[l, 2 * j + n], preferred_element_type=F32).astype(BF)
            for o in range(4):
                for h in (0, 1):
                    at = o * ZB + h * ZH
                    part[l, k, j, o, h, :, cols] = value[at:at + ZH]
            return carry

        lax.fori_loop(0, 2, columns, 0)
        sems = z_sems(l, k, j)
        send(part.at[l, k, j, zo, 0], ra.at[l, k, j, 0], sems, ZA0, at_z(zp))
        send(part.at[l, k, j, zo, 1], ra.at[l, k, j, 1], sems, ZA1, at_z(zm))
        send(part.at[l, k, j, zp, 1], rb.at[l, k, j, 0], sems, ZB0, at_z(zp))
        send(part.at[l, k, j, zm, 0], rb.at[l, k, j, 1], sems, ZB1, at_z(zm))

    def stage_b(l, k, j):
        sems = z_sems(l, k, j)
        for h, (to, slot, out) in enumerate(((zp, ZA0, ZC0), (zm, ZA1, ZC1))):
            arrived(ra.at[l, k, j, h], sems[1].at[slot])
            part[l, k, j, to, h] = (part[l, k, j, to, h].astype(F32) + ra[l, k, j, h].astype(F32)).astype(BF)
            send(part.at[l, k, j, to, h], rc.at[l, k, j, h], sems, out, at_z(to))

    def hid_ref(l, k, j, o, h):
        return hid.at[l, k, pl.ds(2 * j, 2), pl.ds(pl.multiple_of(o * ZB + h * ZH, ZH), ZH), :]

    def stage_c(l, k, j):
        sems = z_sems(l, k, j)
        for h in (0, 1):
            arrived(rb.at[l, k, j, 1 - h], sems[1].at[(ZB1, ZB0)[h]])
            arrived(rc.at[l, k, j, h], sems[1].at[(ZC0, ZC1)[h]])
            total = (
                part[l, k, j, z, h].astype(F32) + rc[l, k, j, h].astype(F32) + rb[l, k, j, 1 - h].astype(F32)
            )
            for n in (0, 1):
                gate, up = total[:, n * 256:n * 256 + UT], total[:, n * 256 + UT:(n + 1) * 256]
                value = gate * jax.nn.sigmoid(gate) * up
                if j < SHARED:
                    value = jnp.where(x == 3, jnp.zeros_like(value), value)
                hid[l, k, 2 * j + n, pl.ds(pl.multiple_of(z * ZB + h * ZH, ZH), ZH), :] = value.astype(BF)
        for h in (0, 1):
            ref = hid_ref(l, k, j, z, h)
            send(ref, ref, sems, (HF0, HF1)[h], at_z(zp))
            ref = hid_ref(l, k, j, z, 1 - h)
            send(ref, ref, sems, (HB1, HB0)[h], at_z(zm))

    def stage_d(l, k, j):
        sems = z_sems(l, k, j)
        ref = hid_ref(l, k, j, zm, 0)
        arrived(ref, sems[1].at[HF0])
        send(ref, ref, sems, HG0, at_z(zp))
        ref = hid_ref(l, k, j, zp, 1)
        arrived(ref, sems[1].at[HB1])
        send(ref, ref, sems, HG1, at_z(zm))

    def stage_e(l, k):
        for j in range(NJ):
            sems = z_sems(l, k, j)
            arrived(hid_ref(l, k, j, zm, 1), sems[1].at[HF1])
            arrived(hid_ref(l, k, j, zp, 0), sems[1].at[HB0])
            arrived(hid_ref(l, k, j, zo, 0), sems[1].at[HG0])
            arrived(hid_ref(l, k, j, zo, 1), sems[1].at[HG1])
        if k == 0:
            weights_ready(l, NJ)

        def columns(n, carry):
            cols = pl.ds(pl.multiple_of(n * 256, 256), 256)
            lhs = jnp.concatenate([hid[l, k, t] for t in range(NT)], axis=1)
            rhs = wd[l, :, :, :, cols].reshape(NT * UT, 256)
            value = jnp.dot(lhs, rhs, preferred_element_type=F32).astype(BF)
            for yy in range(4):
                for h in (0, 1):
                    at = yy * YB + h * YH
                    down[l, k, yy, h, :, cols] = value[at:at + YH]
            return carry

        lax.fori_loop(0, DQ // 256, columns, 0)
        sems = y_sems(l, k)
        send(down.at[l, k, yo, 0], ya.at[l, k, 0], sems, YA0, at_y(yp))
        send(down.at[l, k, yo, 1], ya.at[l, k, 1], sems, YA1, at_y(ym))
        send(down.at[l, k, yp, 1], yb.at[l, k, 0], sems, YB0, at_y(yp))
        send(down.at[l, k, ym, 0], yb.at[l, k, 1], sems, YB1, at_y(ym))

    def stage_g(l, k):
        sems = y_sems(l, k)
        for h, (to, slot, out) in enumerate(((yp, YA0, YC0), (ym, YA1, YC1))):
            arrived(ya.at[l, k, h], sems[1].at[slot])
            down[l, k, to, h] = (down[l, k, to, h].astype(F32) + ya[l, k, h].astype(F32)).astype(BF)
            send(down.at[l, k, to, h], yc.at[l, k, h], sems, out, at_y(to))

    def stage_h(l, k):
        sems = y_sems(l, k)
        for h in (0, 1):
            arrived(yb.at[l, k, 1 - h], sems[1].at[(YB1, YB0)[h]])
            arrived(yc.at[l, k, h], sems[1].at[(YC0, YC1)[h]])
            total = down[l, k, y, h].astype(F32) + yc[l, k, h].astype(F32) + yb[l, k, 1 - h].astype(F32)
            ys[l, k, 2 * h] = total[:R].astype(BF)
            ys[l, k, 2 * h + 1] = total[R:].astype(BF)
        for d in (2, 1, 3):
            send(ys.at[l, k, turn(x, d)], xr.at[l, k, d - 1], sems, XR + d - 1, at_x(turn(x, d)))

    def stage_i(l, k):
        sems = y_sems(l, k)
        rows = pl.ds(pl.multiple_of(x_rows(x), R), R)
        value = RESIDUAL * xs[l, k, rows, :].astype(F32) + ys[l, k, x].astype(F32)
        for d in (1, 3, 2):
            arrived(xr.at[l, k, d - 1], sems[1].at[XR + d - 1])
            value = value + xr[l, k, d - 1].astype(F32)
        mixed[l, k] = value
        row_sum = jnp.sum(value, axis=1, keepdims=True)
        row_squares = jnp.sum(value * value, axis=1, keepdims=True)
        lane = lax.broadcasted_iota(jnp.int32, (R, 128), 1)
        st[l, k] = jnp.where(lane == 0, row_sum, jnp.where(lane == 1, row_squares, 0.0))
        for d in (2, 1, 3):
            send(st.at[l, k], st_in.at[l, k, d - 1], sems, ST + d - 1, at_z(turn(z, d)))

    def stage_j(l, k):
        if l == 0 and k == 0:
            for i, dst in enumerate((ga, sh)):
                for d in (1, 3, 2):
                    arrived(dst.at[turn(x, 4 - d)], g_recv.at[i, d - 1])
                gain_copies[i].wait()
        stats = st[l, k]
        for d in (1, 3, 2):
            arrived(st_in.at[l, k, d - 1], y_recv.at[l, k, ST + d - 1])
            stats = stats + st_in[l, k, d - 1]
        mean = stats[:, 0:1] / D
        var = stats[:, 1:2] / D - mean * mean
        scale = lax.rsqrt(var + EPSILON)
        rows = pl.ds(pl.multiple_of(x_rows(x), R), R)
        for q in range(4):
            cols = slice(q * DB, (q + 1) * DB)
            normed = (mixed[l, k, :, cols] - mean) * scale
            value = (normed * ga[q, l:l + 1, :] + sh[q, l:l + 1, :]).astype(BF)
            if l + 1 < LAYERS:
                xs[l + 1, k, rows, cols] = value
            else:
                nb[k, q] = value
        if l + 1 == LAYERS:
            ov[pl.ds(pl.multiple_of(c * TCORE + k * TC + x_rows(x), R), R), :] = nb[k, x]
        dst = gathered(l + 1, k, x_rows(x), R)
        for d in (2, 1, 3):
            src = dst if l + 1 < LAYERS else nb.at[k, turn(x, d)]
            send(src, dst, ag_sems(l + 1, k), XG + d - 1, at_x(turn(x, d)))

    def stage_k(l, k):
        p = l + 1
        sems = ag_sems(p, k)
        for d in (1, 3, 2):
            owner = turn(x, 4 - d)
            if p == 0:
                ref = xs.at[0, k, pl.ds(pl.multiple_of(y * YB, YB), YB), d_cols(owner)]
            else:
                ref = gathered(p, k, x_rows(owner), R)
            arrived(ref, sems[1].at[XG + d - 1])
        if p == 0:
            in_copies[k].wait()
        for h in (0, 1):
            ref = gathered(p, k, y * YB + h * YH, YH)
            send(ref, ref, sems, (YF0, YF1)[h], at_y(yp))
            ref = gathered(p, k, y * YB + (1 - h) * YH, YH)
            send(ref, ref, sems, (YK1, YK0)[h], at_y(ym))
        if p == 2:
            ref = gathered(p, k, y * YB, YB)
            send(ref, ref, sems, DD, other)

    def stage_l(l, k):
        p = l + 1
        sems = ag_sems(p, k)
        ref = gathered(p, k, ym * YB, YH)
        arrived(ref, sems[1].at[YF0])
        send(ref, ref, sems, YG0, at_y(yp))
        ref = gathered(p, k, yp * YB + YH, YH)
        arrived(ref, sems[1].at[YK1])
        send(ref, ref, sems, YG1, at_y(ym))
        if p == 2:
            for n, (at, half, slot) in enumerate(((ym, 1, YF1), (yp, 0, YK0))):
                arrived(gathered(p, k, at * YB + half * YH, YH), sems[1].at[slot])
                ref = gathered(p, k, at * YB, YB)
                send(ref, ref, sems, DD + 1 + n, other)

    def stage_m(l, k):
        p = l + 1
        sems = ag_sems(p, k)
        arrived(gathered(p, k, yo * YB, YH), sems[1].at[YG0])
        arrived(gathered(p, k, yo * YB + YH, YH), sems[1].at[YG1])
        ref = gathered(p, k, yo * YB, YB)
        send(ref, ref, sems, DD + 3, other)

    stages = dict(
        A=stage_a, B=stage_b, C=stage_c, D=stage_d, E=stage_e, G=stage_g, H=stage_h, I=stage_i, J=stage_j,
        K=stage_k, L=stage_l, W=stage_w, V=stage_v, U=stage_u,
    )
    for stage, *key in order():
        stages[stage](*key)

    for k in range(NC):
        stage_m(1, k)
    out_waits = []
    for k in range(NC):
        for n, yy in enumerate((y, ym, yp, yo)):
            arrived(gathered(2, k, yy * YB, YB, 1 - c), ag_recv.at[2, k, DD + n])
    for cc in range(2):
        rows = pl.ds(cc * TCORE, TCORE)
        copy = pltpu.make_async_copy(ov.at[rows, :], out_hbm.at[rows, :], local.at[16 + NC + cc])
        copy.start()
        out_waits.append(copy.wait)
    for wait in waits:
        wait()
    for wait in out_waits:
        wait()


def solution(mesh):
    dma = pltpu.SemaphoreType.DMA

    def per_device(inputs, gate_weight, up_weight, down_weight, norm_gain, norm_shift):
        any_space = pl.BlockSpec(memory_space=pl.ANY)
        return pl.pallas_call(
            kernel,
            out_shape=jax.ShapeDtypeStruct((T, DB), BF),
            in_specs=[any_space] * 6,
            out_specs=any_space,
            scratch_shapes=[
                pltpu.VMEM((2, NC, TC, DQ), BF),
                pltpu.VMEM((2, NT, DQ, 2 * UT), BF),
                pltpu.VMEM((2, NJ, 2, UT, DQ), BF),
                pltpu.VMEM((2, NJ, 2, DB, UT), BF),
                pltpu.VMEM((2, 2, NJ, UT // 2, DB), BF),
                pltpu.VMEM((2, NC, NJ, 4, 2, ZH, 4 * UT), BF),
                pltpu.VMEM((2, NC, NJ, 2, ZH, 4 * UT), BF),
                pltpu.VMEM((2, NC, NJ, 2, ZH, 4 * UT), BF),
                pltpu.VMEM((2, NC, NJ, 2, ZH, 4 * UT), BF),
                pltpu.VMEM((2, NC, NT, TC, UT), BF),
                pltpu.VMEM((2, NC, 4, 2, YH, DQ), BF),
                pltpu.VMEM((2, NC, 2, YH, DQ), BF),
                pltpu.VMEM((2, NC, 2, YH, DQ), BF),
                pltpu.VMEM((2, NC, 2, YH, DQ), BF),
                pltpu.VMEM((2, NC, 4, R, DQ), BF),
                pltpu.VMEM((2, NC, 3, R, DQ), BF),
                pltpu.VMEM((2, NC, R, DQ), F32),
                pltpu.VMEM((2, NC, R, 128), F32),
                pltpu.VMEM((2, NC, 3, R, 128), F32),
                pltpu.VMEM((NC, 4, R, DB), BF),
                pltpu.VMEM((T, DB), BF),
                pltpu.VMEM((4, 2, DB), F32),
                pltpu.VMEM((4, 2, DB), F32),
                dma((2, NC, NJ, N_Z)),
                dma((2, NC, NJ, N_Z)),
                dma((2, NC, N_Y)),
                dma((2, NC, N_Y)),
                dma((3, NC, N_AG)),
                dma((3, NC, N_AG)),
                dma((2, NJ + 1, N_W)),
                dma((2, NJ + 1, N_W)),
                dma((2, 3)),
                dma((2, 3)),
                dma((18 + NC,)),
            ],
            compiler_params=pltpu.CompilerParams(
                collective_id=0, has_side_effects=True, vmem_limit_bytes=62 * 1024 * 1024
            ),
        )(inputs, gate_weight, up_weight, down_weight.reshape(LAYERS, TILES, UT, DB), norm_gain, norm_shift)

    return jax.shard_map(
        per_device,
        mesh=mesh,
        in_specs=(P(None, "ra"), P(None, "ra", "cb"), P(None, "ra", "cb"), P(None, "cb", "ra"), P(None, "ra"), P(None, "ra")),
        out_specs=P(None, "ra"),
        check_vma=False,
    )
```

time: 433 us -> 170 us (0.39)
  waiting for transfers between devices: 287 us -> 0 us
  Pallas kernels: 0 us -> 168 us
  blocking collectives: 86.1 us -> 0 us
  matrix products: 20 us -> 0 us
  local copies, waits for them, and re-layouts: 19.1 us -> 2.06 us
  between operations: 13.3 us -> 0.01 us
  starting transfers between devices: 5.34 us -> 0 us
    unnamed x6 -> x0, waiting for transfers between devices: 169 us -> none
    pallas_call x0 -> x1, Pallas kernels: none -> 168 us  [per_device(): pl.pallas_call(kernel, out_shape=jax.ShapeDtypeStruct((T, DB), BF), in_sp...]
    all_gather x2 -> x0, waiting for transfers between devices: 106 us -> none  [sublayer(): lax.all_gather(hidden, RA, axis=0, tiled=True)]
    all_to_all x3 -> x0, blocking collectives: 55.8 us -> none  [the longest x2 38.8 us: from_everyone(): lax.all_to_all(jnp.broadcast_to(shard[None], (peers, *shard.shape)), axis...]
    psum x4 -> x0, blocking collectives: 30.3 us -> none  [over_axes(): return functools.reduce(lax.psum, axes, shard)]
    dot_general x4 -> x0, matrix products: 20 us -> none  [the longest x2 11.5 us: sublayer(): jnp.dot(stream, paired, preferred_element_type=jnp.float32)]
    unnamed x10 -> x1, local copies, waits for them, and re-layouts: 15.2 us -> 2.06 us
    all_to_all x1 -> x0, waiting for transfers between devices: 12.1 us -> none  [sum_at_owner(): lax.all_to_all(parts, axis, split_axis=0, concat_axis=0, tiled=True)]
  transfers between devices with their start and end apart: 5 -> 0, of which waited for: 5 -> 0; matrix products, arithmetic and copies ran while one was open for 0% -> 0% of each run, Pallas kernels for 0% -> 0%
where the time goes in v2:
time: 170 us
  Pallas kernels  168 us (99%)
  local copies, waits for them, and re-layouts  2.06 us (1%)
    pallas_call x1, Pallas kernels, per_device(): pl.pallas_call(kernel, out_shape=jax.ShapeDtypeStruct((T, DB), BF), in_sp...  168 us

profile of v2, /device:TPU:1, one launch (start us, length us, event | category | flops | bytes accessed | tf_op | source)
XLA Modules:
  0.0 169.6 jit_solution(12648138742396458777)
XLA Ops:
  0.0 167.6 %shard_map.64 = bf16[1536,256]{1,0:T(8,128)(2,1)} custom-call(bf16[1536,256]{1,0:T(8,128)(2,1)} %x_hbm.1, bf16[2,256,1408]{2,1,0:T(8,128)(2,1)} %wg_hbm.1, bf16[2,256,1408]{2,1,0:T(8,128)(2,1)} %wu_hbm.1, bf16[2,11,128,256]{3,2,1,0:T(8,128)(2,1)} %bitcast.1, f32[2,256]{1,0:T(2,128)} %gain_hbm.1, f32[2,256]{1,0:T(2,128)} %shift_hbm.1), custom_call_target="tpu_custom_call" | custom-call | tf_op jit(solution)/shard_map/pallas_call | solution.py:585
  167.6 2.1 %copy.8 = bf16[1536,256]{1,0:T(8,128)(2,1)} copy(bf16[1536,256]{1,0:T(8,128)(2,1)} %shard_map.64) | data formatting | bytes 1572864

commit v3 on v0

v3 whole, which is shorter than its diff:
```python
import jax
import jax.numpy as jnp
from jax import lax
from jax.experimental import pallas as pl
from jax.experimental.pallas import tpu as pltpu
from jax.sharding import PartitionSpec as P

MESH = pl.DeviceIdType.MESH
BF = jnp.bfloat16
F32 = jnp.float32
RESIDUAL = 0.5
EPSILON = 1e-05

T, D, FF, LAYERS = 1536, 4096, 11264, 2
NC = 6
TC = T // NC
ZB = TC // 4
ZH = ZB // 2
YB = TC // 4
YH = YB // 2
R = TC // 16
DB = D // 16
DQ = D // 4
UT = 128
NJ = 3
NT = 2 * NJ
TILES = FF // 8 // UT
SHARED = 4 * NJ - TILES

GROUPS = {(l, k): [(0, 1), (1, 2), (2, 3)] if l + k == 0 else [(0, 3)] for l in range(LAYERS) for k in range(NC)}

SLOTS = {}


def slots(*names):
    for name in names:
        SLOTS.setdefault(name, len(SLOTS))


for l in range(LAYERS):
    for k in range(NC):
        for g in range(len(GROUPS[l, k])):
            for m in ("za", "zb", "zc", "hf", "hk", "hg"):
                slots((m, l, k, g, 0), (m, l, k, g, 1))
        for m in ("ya", "yb", "yc"):
            slots((m, l, k, 0), (m, l, k, 1))
        for m in ("xr", "st"):
            slots((m, l, k, 1), (m, l, k, 2), (m, l, k, 3))
    for j in range(NJ + 1):
        slots(("wr", l, j, 0), ("wr", l, j, 1))
        for cc in range(2):
            slots(("wm", l, j, cc), ("wp", l, j, cc), ("wo", l, j, cc, 0), ("wo", l, j, cc, 1), ("wd", l, j, cc))
for k in range(NC):
    for p in range(LAYERS + 1):
        slots(("xg", p, k, 1), ("xg", p, k, 2), ("xg", p, k, 3))
        for m in ("yf", "yk", "yg"):
            slots((m, p, k, 0), (m, p, k, 1))
    slots(*(("dd", k, n) for n in range(4)))
slots(*(("gain", i, d) for i in range(2) for d in (1, 2, 3)))
N_SLOTS = len(SLOTS)

HOP = {1: 1.9, 2: 2.7}
CORE_HOP = 1.0
FROM_HBM = 1.1
LINK = 92e3
CORE_LINK = 500e3
START = 3.5
TIMES = dict(B=0.1, C=0.2, D=0.06, E=0.9, G=0.15, H=0.15, I=0.25, J=0.35, K=0.08, L=0.06, M=0.05, W=0.12, V=0.06)
SLACK = dict(A=0.5, E=0.5, W=0.7)


def time_of(task):
    if task[0] in "ABC" and task[0] != "":
        first, last = GROUPS[task[1], task[2]][task[3]]
        return {"A": 0.4, "B": 0.08, "C": 0.1}[task[0]] * (last - first) + 0.05
    return TIMES[task[0]]


def plan():
    tasks = {}
    for l in range(LAYERS):
        for j in range(NJ + 1):
            size = 2 * (2 * DB * UT * 2 if j < NJ else NJ * UT * DB * 2)
            tasks["W", l, j] = ([], [
                (("wr", l, j, 0), "x+", size // 2, 1), (("wr", l, j, 1), "x-", size // 2, 1),
                (("wm", l, j), "x+", size, 1), (("wp", l, j), "x-", size, 1), (("wd", l, j), "c", size // 2, 0),
            ])
            tasks["V", l, j] = ([("wr", l, j, 0), ("wr", l, j, 1)], [
                (("wo", l, j, 0), "x+", size // 2, 1), (("wo", l, j, 1), "x-", size // 2, 1)])

    def ring(one, two, keys, size, axis):
        return [((m, *keys, h), axis + "+-"[h ^ (m == two and 0)], size, 1) for m in (one, two) for h in (0, 1)]

    def pair(m, keys, size, axis):
        return [((m, *keys, 0), axis + "+", size, 1), ((m, *keys, 1), axis + "-", size, 1)]

    def three(m, keys, size, axis):
        return [((m, *keys, 2), axis + "+", size, 2), ((m, *keys, 1), axis + "+", size, 1), ((m, *keys, 3), axis + "-", size, 1)]

    def gather(one, two, keys, size, axis):
        return [
            ((one, *keys, 0), axis + "+", size, 1), ((two, *keys, 1), axis + "-", size, 1),
            ((one, *keys, 1), axis + "+", size, 1), ((two, *keys, 0), axis + "-", size, 1)]

    for k in range(NC):
        for p in range(LAYERS + 1):
            size = YH * (DQ if p < LAYERS else DB) * 2
            tasks["K", p - 1, k] = ([("xg", p, k, d) for d in (1, 2, 3)], gather("yf", "yk", (p, k), size, "y"))
            tasks["L", p - 1, k] = ([("yf", p, k, 0), ("yk", p, k, 1)], pair("yg", (p, k), size, "y"))
        tasks["M", LAYERS - 1, k] = ([("yg", LAYERS, k, h) for h in (0, 1)], [(("dd", k), "c", 2 * size, 0)])
        for l in range(LAYERS):
            for g, (first, last) in enumerate(GROUPS[l, k]):
                zs, hs = ZH * 4 * UT * 2 * (last - first), ZH * 2 * UT * 2 * (last - first)
                keys = (l, k, g)
                need = [("yg", l, k, h) for h in (0, 1)] + [("yf", l, k, 1), ("yk", l, k, 0)]
                for j in range(first, last):
                    need += [("wm", l, j), ("wp", l, j), ("wo", l, j, 0), ("wo", l, j, 1), ("wd", l, j)]
                tasks["A", *keys] = (need, pair("za", keys, zs, "z") + pair("zb", keys, zs, "z"))
                tasks["B", *keys] = ([("za", *keys, h) for h in (0, 1)], pair("zc", keys, zs, "z"))
                tasks["C", *keys] = ([(m, *keys, h) for m in ("zb", "zc") for h in (0, 1)], gather("hf", "hk", keys, hs, "z"))
                tasks["D", *keys] = ([("hf", *keys, 0), ("hk", *keys, 1)], pair("hg", keys, hs, "z"))
            need = [(m, l, k, g, h) for g in range(len(GROUPS[l, k])) for m, h in (("hf", 1), ("hk", 0), ("hg", 0), ("hg", 1))]
            need += [("wm", l, NJ), ("wp", l, NJ), ("wo", l, NJ, 0), ("wo", l, NJ, 1), ("wd", l, NJ)]
            ys, xsz = YH * DQ * 2, R * DQ * 2
            tasks["E", l, k] = (need, pair("ya", (l, k), ys, "y") + pair("yb", (l, k), ys, "y"))
            tasks["G", l, k] = ([("ya", l, k, h) for h in (0, 1)], pair("yc", (l, k), ys, "y"))
            tasks["H", l, k] = ([(m, l, k, h) for m in ("yb", "yc") for h in (0, 1)], three("xr", (l, k), xsz, "x"))
            tasks["I", l, k] = ([("xr", l, k, d) for d in (1, 2, 3)], three("st", (l, k), R * 512, "z"))
            tasks["J", l, k] = ([("st", l, k, d) for d in (1, 2, 3)], three("xg", (l + 1, k), xsz if l + 1 < LAYERS else xsz // 4, "x"))
    return tasks


def order(report=None):
    tasks = plan()
    maker = {m[0]: t for t, (_, sends) in tasks.items() for m in sends}
    users = {}
    for t, (needs, _) in tasks.items():
        for m in needs:
            if m in maker:
                users.setdefault(maker[m], set()).add(t)
    rank = {}

    def rest(task):
        if task not in rank:
            rank[task] = time_of(task) + max((rest(u) + 2.0 for u in users.get(task, ())), default=0.0)
        return rank[task]

    arrive, free = {}, {}

    def transmit(sends, now, more=0.0):
        for m, link, size, hops in sends:
            done = max(now, free.get(link, 0.0)) + (size * hops / LINK if hops else size / CORE_LINK)
            arrive[m] = done + (HOP[hops] if hops else CORE_HOP) + more
            free[link] = done

    now = START
    done, out = set(), []
    for k in range(NC):
        x_in = YB * DB * 2
        transmit([(("xg", 0, k, 2), "x+", x_in, 2), (("xg", 0, k, 1), "x+", x_in, 1), (("xg", 0, k, 3), "x-", x_in, 1)], now, FROM_HBM)
        if k == 0:
            transmit(tasks["W", 0, 0][1], now, FROM_HBM)
            done.add(("W", 0, 0))
    left = [t for t in tasks if t not in done]
    while left:
        ready = []
        for t in left:
            needs, sends = tasks[t]
            at = None
            if t[0] == "W":
                before = ("W", t[1], t[2] - 1) if t[2] else ("W", t[1] - 1, NJ)
                if before in done:
                    at = max(free["x+"], free["x-"]) - SLACK["W"]
            elif all(m in arrive for m in needs):
                at = max(arrive[m] for m in needs)
                if t[0] in SLACK:
                    at = max(at, max(free.get(m[1], 0.0) for m in sends) - SLACK[t[0]])
            if at is not None:
                ready.append((at, t))
        at, t = min(ready, key=lambda r: (max(r[0], now), r[1][0] == "W", r[1][1:3], -rest(r[1])))
        begin = max(now, at)
        now = begin + time_of(t)
        transmit(tasks[t][1], now, FROM_HBM if t[0] == "W" else 0.0)
        left.remove(t)
        done.add(t)
        out.append(t)
        if report is not None:
            report.append((begin, now, t))
    return out


def kernel(
    x_hbm, wg_hbm, wu_hbm, wd_hbm, gain_hbm, shift_hbm, out_hbm,
    xs, wgu, wd, rel, rel_d, part, ra, rb, rc, hid, down, ya, yb, yc, ys, xr, mixed, st, st_in, nb, ov, ga, sh,
    recv, sent, local, go,
):
    ra_at, cb_at = lax.axis_index("ra"), lax.axis_index("cb")
    z, x = ra_at // 4, lax.rem(ra_at, 4)
    y, c = cb_at // 2, lax.rem(cb_at, 2)

    def turn(v, d):
        return lax.rem(v + d, 4)

    zp, zo, zm = turn(z, 1), turn(z, 2), turn(z, 3)
    yp, yo, ym = turn(y, 1), turn(y, 2), turn(y, 3)
    xp, xo, xm = turn(x, 1), turn(x, 2), turn(x, 3)

    def at_z(v):
        return (v * 4 + x, cb_at)

    def at_x(v):
        return (z * 4 + v, cb_at)

    def at_x_main(v):
        return (z * 4 + v, y * 2 + 1)

    def at_y(v):
        return (ra_at, v * 2 + c)

    other = (ra_at, y * 2 + (1 - c))

    peers = [at_z(zp), at_z(zo), at_z(zm), at_x(xp), at_x(xo), at_x(xm), at_y(yp), at_y(ym), other]
    peers += [(z * 4 + xp, y * 2 + (1 - c)), (z * 4 + xm, y * 2 + (1 - c))]
    barrier = pltpu.get_barrier_semaphore()
    for peer in peers:
        pl.semaphore_signal(barrier, inc=1, device_id=peer, device_id_type=MESH)
    pl.semaphore_wait(barrier, len(peers))

    def start(src, dst, name, dev):
        copy = pltpu.make_async_remote_copy(
            src_ref=src, dst_ref=dst, send_sem=sent.at[SLOTS[name]], recv_sem=recv.at[SLOTS[name]],
            device_id=dev, device_id_type=MESH,
        )
        copy.start()
        return copy

    def described(ref, name):
        return pltpu.make_async_remote_copy(
            src_ref=ref, dst_ref=ref, send_sem=sent.at[SLOTS[name]], recv_sem=recv.at[SLOTS[name]],
            device_id=other, device_id_type=MESH,
        )

    def arrived(dst, name):
        described(dst, name).wait_recv()

    def d_cols(v):
        return pl.ds(pl.multiple_of(v * DB, DB), DB)

    def tile_of(v):
        return jnp.minimum(v * NJ, TILES - NJ)

    def units(v, j):
        return pl.ds(pl.multiple_of((tile_of(v) + j) * UT, UT), UT)

    def gu_half(l, j, cc, owner, what):
        return wgu.at[l, 2 * j + cc, d_cols(owner), pl.ds(what * UT, UT)]

    def relay_ref(l, j, h):
        return rel.at[l, j, h] if j < NJ else rel_d.at[l, h]

    def w_half(l, j, cc, owner, h):
        if j < NJ:
            return gu_half(l, j, cc, owner, h)
        return wd.at[l, :, cc, pl.ds(h * 64, 64), d_cols(owner)]

    def w_whole(l, j, cc, owner):
        return wgu.at[l, 2 * j + cc, d_cols(owner), :] if j < NJ else wd.at[l, :, cc, :, d_cols(owner)]

    def program(core):
        waits = []

        def send(src, dst, name, dev):
            waits.append(start(src, dst, name, dev).wait_send)

        local_waits = {}

        def stage_w(l, j):
            if j < NJ:
                sources = (wg_hbm, wu_hbm)
                send(wg_hbm.at[l, :, units(xo, j)], rel.at[l, j, 0], ("wr", l, j, 0), at_x(xp))
                send(wu_hbm.at[l, :, units(xo, j)], rel.at[l, j, 1], ("wr", l, j, 1), at_x(xm))
                for dst_x, m in ((xp, "wm"), (xm, "wp")):
                    for what, src in enumerate(sources):
                        start(
                            src.at[l, :, units(dst_x, j)], gu_half(l, j, core, x, what), (m, l, j, core), at_x_main(dst_x)
                        )
                    waits.append(described(w_whole(l, j, core, x), (m, l, j, core)).wait_send)
                if core == 0:
                    for what, src in enumerate(sources):
                        start(src.at[l, :, units(x, j)], gu_half(l, j, core, x, what), ("wd", l, j, core), other)
                    waits.append(described(w_whole(l, j, core, x), ("wd", l, j, core)).wait_send)
                else:
                    mine = []
                    for what, src in enumerate(sources):
                        copy = pltpu.make_async_copy(
                            src.at[l, :, units(x, j)], gu_half(l, j, core, x, what), local.at[l * 7 + j * 2 + what]
                        )
                        copy.start()
                        mine.append(copy.wait)
                    local_waits[l, j] = mine
            else:
                def src(v, h=None):
                    if h is None:
                        return wd_hbm.at[l, pl.ds(tile_of(v), NJ)]
                    return wd_hbm.at[l, pl.ds(tile_of(v), NJ), pl.ds(h * 64, 64)]

                send(src(xo, 0), rel_d.at[l, 0], ("wr", l, j, 0), at_x(xp))
                send(src(xo, 1), rel_d.at[l, 1], ("wr", l, j, 1), at_x(xm))
                send(src(xp), w_whole(l, j, core, x), ("wm", l, j, core), at_x_main(xp))
                send(src(xm), w_whole(l, j, core, x), ("wp", l, j, core), at_x_main(xm))
                if core == 0:
                    send(src(x), w_whole(l, j, core, x), ("wd", l, j, core), other)
                else:
                    copy = pltpu.make_async_copy(src(x), w_whole(l, j, core, x), local.at[l * 7 + 6])
                    copy.start()
                    local_waits[l, j] = [copy.wait]

        def stage_v(l, j):
            for h, (to, owner) in enumerate(((xp, xm), (xm, xp))):
                arrived(relay_ref(l, j, h), ("wr", l, j, h))
                send(relay_ref(l, j, h), w_half(l, j, core, owner, h), ("wo", l, j, core, h), at_x_main(to))

        if core == 0:
            stage_w(0, 0)
            for stage, *key in order():
                if stage == "W":
                    pl.semaphore_wait(go, 1)
                    stage_w(*key)
                elif stage == "V":
                    stage_v(*key)
            for k in range(NC):
                for n, yy in enumerate((y, ym, yp, yo)):
                    arrived(ov.at[pl.ds(pl.multiple_of(k * TC + yy * YB, YB), YB), :], ("dd", k, n))
            copy = pltpu.make_async_copy(ov, out_hbm, local.at[0])
            copy.start()
            for wait in waits:
                wait()
            copy.wait()
            return

        def weights_ready(l, j):
            for wait in local_waits[l, j]:
                wait()
            arrived(w_whole(l, j, 0, x), ("wd", l, j, 0))
            for cc in range(2):
                arrived(w_whole(l, j, cc, xm), ("wm", l, j, cc))
                arrived(w_whole(l, j, cc, xp), ("wp", l, j, cc))
                arrived(w_half(l, j, cc, xo, 0), ("wo", l, j, cc, 0))
                arrived(w_half(l, j, cc, xo, 1), ("wo", l, j, cc, 1))

        def gathered(p, k, at, rows):
            if p < LAYERS:
                return xs.at[p, k, pl.ds(pl.multiple_of(at, rows), rows), :]
            return ov.at[pl.ds(pl.multiple_of(k * TC + at, rows), rows), :]

        def x_rows(v):
            return y * YB + v * R

        in_copies = []

        def input_send(k):
            rows = pl.ds(pl.multiple_of(k * TC + y * YB, YB), YB)
            dst = xs.at[0, k, pl.ds(pl.multiple_of(y * YB, YB), YB), d_cols(x)]
            for d in (2, 1, 3):
                send(x_hbm.at[rows, :], dst, ("xg", 0, k, d), at_x(turn(x, d)))
            copy = pltpu.make_async_copy(x_hbm.at[rows, :], dst, local.at[14 + k])
            copy.start()
            in_copies.append(copy)

        input_send(0)
        stage_w(0, 0)
        for k in range(1, NC):
            input_send(k)
        gain_copies = []
        for i, (src, dst) in enumerate(((gain_hbm, ga), (shift_hbm, sh))):
            for d in (1, 3, 2):
                send(src, dst.at[x], ("gain", i, d), at_x(turn(x, d)))
            copy = pltpu.make_async_copy(src, dst.at[x], local.at[14 + NC + i])
            copy.start()
            gain_copies.append(copy)

        gates_ready = set()

        def stage_a(l, k, g):
            first, last = GROUPS[l, k][g]
            if g == 0:
                arrived(gathered(l, k, ym * YB + YH, YH), ("yf", l, k, 1))
                arrived(gathered(l, k, yp * YB, YH), ("yk", l, k, 0))
                arrived(gathered(l, k, yo * YB, YH), ("yg", l, k, 0))
                arrived(gathered(l, k, yo * YB + YH, YH), ("yg", l, k, 1))
            for j in range(first, last):
                if (l, j) not in gates_ready:
                    weights_ready(l, j)
                    gates_ready.add((l, j))

            def tiles(j, carry):
                for n in (0, 1):
                    value = jnp.dot(xs[l, k], wgu[l, 2 * j + n], preferred_element_type=F32).astype(BF)
                    for o in range(4):
                        for h in (0, 1):
                            at = o * ZB + h * ZH
                            part[l, k, j, o, h, :, n * 256:(n + 1) * 256] = value[at:at + ZH]
                return carry

            lax.fori_loop(first, last, tiles, 0)
            js = pl.ds(first, last - first)
            send(part.at[l, k, js, zo, 0], ra.at[l, k, js, 0], ("za", l, k, g, 0), at_z(zp))
            send(part.at[l, k, js, zo, 1], ra.at[l, k, js, 1], ("za", l, k, g, 1), at_z(zm))
            send(part.at[l, k, js, zp, 1], rb.at[l, k, js, 0], ("zb", l, k, g, 0), at_z(zp))
            send(part.at[l, k, js, zm, 0], rb.at[l, k, js, 1], ("zb", l, k, g, 1), at_z(zm))

        def stage_b(l, k, g):
            first, last = GROUPS[l, k][g]
            js = pl.ds(first, last - first)
            for h, to in enumerate((zp, zm)):
                arrived(ra.at[l, k, js, h], ("za", l, k, g, h))
                for j in range(first, last):
                    part[l, k, j, to, h] = (part[l, k, j, to, h].astype(F32) + ra[l, k, j, h].astype(F32)).astype(BF)
                send(part.at[l, k, js, to, h], rc.at[l, k, js, h], ("zc", l, k, g, h), at_z(to))

        def hid_ref(l, k, g, o, h):
            first, last = GROUPS[l, k][g]
            rows = pl.ds(pl.multiple_of(o * ZB + h * ZH, ZH), ZH)
            return hid.at[l, k, pl.ds(2 * first, 2 * (last - first)), rows, :]

        def stage_c(l, k, g):
            first, last = GROUPS[l, k][g]
            js = pl.ds(first, last - first)
            for h in (0, 1):
                arrived(rb.at[l, k, js, 1 - h], ("zb", l, k, g, 1 - h))
                arrived(rc.at[l, k, js, h], ("zc", l, k, g, h))
                for j in range(first, last):
                    total = (
                        part[l, k, j, z, h].astype(F32) + rc[l, k, j, h].astype(F32) + rb[l, k, j, 1 - h].astype(F32)
                    )
                    for n in (0, 1):
                        gate, up = total[:, n * 256:n * 256 + UT], total[:, n * 256 + UT:(n + 1) * 256]
                        value = gate * jax.nn.sigmoid(gate) * up
                        if j < SHARED:
                            value = jnp.where(x == 3, jnp.zeros_like(value), value)
                        hid[l, k, 2 * j + n, pl.ds(pl.multiple_of(z * ZB + h * ZH, ZH), ZH), :] = value.astype(BF)
                if h == 0:
                    ref = hid_ref(l, k, g, z, 0)
                    send(ref, ref, ("hf", l, k, g, 0), at_z(zp))
            ref = hid_ref(l, k, g, z, 1)
            send(ref, ref, ("hk", l, k, g, 1), at_z(zm))
            send(ref, ref, ("hf", l, k, g, 1), at_z(zp))
            ref = hid_ref(l, k, g, z, 0)
            send(ref, ref, ("hk", l, k, g, 0), at_z(zm))

        def stage_d(l, k, g):
            for h, (owner, m, to) in enumerate(((zm, "hf", zp), (zp, "hk", zm))):
                ref = hid_ref(l, k, g, owner, h)
                arrived(ref, (m, l, k, g, h))
                send(ref, ref, ("hg", l, k, g, h), at_z(to))

        def stage_e(l, k):
            for g in range(len(GROUPS[l, k])):
                arrived(hid_ref(l, k, g, zm, 1), ("hf", l, k, g, 1))
                arrived(hid_ref(l, k, g, zp, 0), ("hk", l, k, g, 0))
                arrived(hid_ref(l, k, g, zo, 0), ("hg", l, k, g, 0))
                arrived(hid_ref(l, k, g, zo, 1), ("hg", l, k, g, 1))
            if (l, NJ) not in gates_ready:
                weights_ready(l, NJ)
                gates_ready.add((l, NJ))

            def columns(n, carry):
                lhs = jnp.concatenate([hid[l, k, t] for t in range(NT)], axis=1)
                for i in (0, 1):
                    cols = pl.ds(pl.multiple_of(n * 512 + i * 256, 256), 256)
                    rhs = wd[l, :, :, :, cols].reshape(NT * UT, 256)
                    value = jnp.dot(lhs, rhs, preferred_element_type=F32).astype(BF)
                    for yy in range(4):
                        for h in (0, 1):
                            at = yy * YB + h * YH
                            down[l, k, yy, h, :, cols] = value[at:at + YH]
                return carry

            lax.fori_loop(0, DQ // 512, columns, 0)
            send(down.at[l, k, yo, 0], ya.at[l, k, 0], ("ya", l, k, 0), at_y(yp))
            send(down.at[l, k, yo, 1], ya.at[l, k, 1], ("ya", l, k, 1), at_y(ym))
            send(down.at[l, k, yp, 1], yb.at[l, k, 0], ("yb", l, k, 0), at_y(yp))
            send(down.at[l, k, ym, 0], yb.at[l, k, 1], ("yb", l, k, 1), at_y(ym))

        def stage_g(l, k):
            for h, to in enumerate((yp, ym)):
                arrived(ya.at[l, k, h], ("ya", l, k, h))
                down[l, k, to, h] = (down[l, k, to, h].astype(F32) + ya[l, k, h].astype(F32)).astype(BF)
                send(down.at[l, k, to, h], yc.at[l, k, h], ("yc", l, k, h), at_y(to))

        def stage_h(l, k):
            for h in (0, 1):
                arrived(yb.at[l, k, 1 - h], ("yb", l, k, 1 - h))
                arrived(yc.at[l, k, h], ("yc", l, k, h))
                total = down[l, k, y, h].astype(F32) + yc[l, k, h].astype(F32) + yb[l, k, 1 - h].astype(F32)
                ys[l, k, 2 * h] = total[:R].astype(BF)
                ys[l, k, 2 * h + 1] = total[R:].astype(BF)
            for d in (2, 1, 3):
                send(ys.at[l, k, turn(x, d)], xr.at[l, k, d - 1], ("xr", l, k, d), at_x(turn(x, d)))

        def stage_i(l, k):
            rows = pl.ds(pl.multiple_of(x_rows(x), R), R)
            value = RESIDUAL * xs[l, k, rows, :].astype(F32) + ys[l, k, x].astype(F32)
            for d in (1, 3, 2):
                arrived(xr.at[l, k, d - 1], ("xr", l, k, d))
                value = value + xr[l, k, d - 1].astype(F32)
            mixed[l, k] = value
            row_sum = jnp.sum(value, axis=1, keepdims=True)
            row_squares = jnp.sum(value * value, axis=1, keepdims=True)
            lane = lax.broadcasted_iota(jnp.int32, (R, 128), 1)
            st[l, k] = jnp.where(lane == 0, row_sum, jnp.where(lane == 1, row_squares, 0.0))
            for d in (2, 1, 3):
                send(st.at[l, k], st_in.at[l, k, d - 1], ("st", l, k, d), at_z(turn(z, d)))

        def stage_j(l, k):
            if l == 0 and k == 0:
                for i, dst in enumerate((ga, sh)):
                    for d in (1, 3, 2):
                        arrived(dst.at[turn(x, 4 - d)], ("gain", i, d))
                    gain_copies[i].wait()
            stats = st[l, k]
            for d in (1, 3, 2):
                arrived(st_in.at[l, k, d - 1], ("st", l, k, d))
                stats = stats + st_in[l, k, d - 1]
            mean = stats[:, 0:1] / D
            var = stats[:, 1:2] / D - mean * mean
            scale = lax.rsqrt(var + EPSILON)
            rows = pl.ds(pl.multiple_of(x_rows(x), R), R)
            for q in range(4):
                cols = slice(q * DB, (q + 1) * DB)
                normed = (mixed[l, k, :, cols] - mean) * scale
                value = (normed * ga[q, l:l + 1, :] + sh[q, l:l + 1, :]).astype(BF)
                if l + 1 < LAYERS:
                    xs[l + 1, k, rows, cols] = value
                else:
                    nb[k, q] = value
            if l + 1 == LAYERS:
                ov[pl.ds(pl.multiple_of(k * TC + x_rows(x), R), R), :] = nb[k, x]
            dst = gathered(l + 1, k, x_rows(x), R)
            for d in (2, 1, 3):
                src = dst if l + 1 < LAYERS else nb.at[k, turn(x, d)]
                send(src, dst, ("xg", l + 1, k, d), at_x(turn(x, d)))

        def stage_k(l, k):
            p = l + 1
            for d in (1, 3, 2):
                owner = turn(x, 4 - d)
                if p == 0:
                    ref = xs.at[0, k, pl.ds(pl.multiple_of(y * YB, YB), YB), d_cols(owner)]
                else:
                    ref = gathered(p, k, x_rows(owner), R)
                arrived(ref, ("xg", p, k, d))
            if p == 0:
                in_copies[k].wait()
            for h in (0, 1):
                ref = gathered(p, k, y * YB + h * YH, YH)
                send(ref, ref, ("yf", p, k, h), at_y(yp))
                ref = gathered(p, k, y * YB + (1 - h) * YH, YH)
                send(ref, ref, ("yk", p, k, 1 - h), at_y(ym))
            if p == LAYERS:
                ref = gathered(p, k, y * YB, YB)
                send(ref, ref, ("dd", k, 0), other)

        def stage_l(l, k):
            p = l + 1
            for h, (owner, m, to) in enumerate(((ym, "yf", yp), (yp, "yk", ym))):
                ref = gathered(p, k, owner * YB + h * YH, YH)
                arrived(ref, (m, p, k, h))
                send(ref, ref, ("yg", p, k, h), at_y(to))
            if p == LAYERS:
                for n, (owner, m, h) in enumerate(((ym, "yf", 1), (yp, "yk", 0))):
                    arrived(gathered(p, k, owner * YB + h * YH, YH), (m, p, k, h))
                    ref = gathered(p, k, owner * YB, YB)
                    send(ref, ref, ("dd", k, 1 + n), other)

        def stage_m(l, k):
            p = l + 1
            for h in (0, 1):
                arrived(gathered(p, k, yo * YB + h * YH, YH), ("yg", p, k, h))
            ref = gathered(p, k, yo * YB, YB)
            send(ref, ref, ("dd", k, 3), other)

        def stage_w_both(l, j):
            pl.semaphore_signal(go, inc=1, device_id=other, device_id_type=MESH)
            stage_w(l, j)

        stages = dict(
            A=stage_a, B=stage_b, C=stage_c, D=stage_d, E=stage_e, G=stage_g, H=stage_h, I=stage_i, J=stage_j,
            K=stage_k, L=stage_l, M=stage_m, W=stage_w_both, V=stage_v,
        )
        for stage, *key in order():
            stages[stage](*key)
        copy = pltpu.make_async_copy(ov, out_hbm, local.at[16 + NC])
        copy.start()
        for wait in waits:
            wait()
        copy.wait()

    @pl.when(c == 0)
    def _():
        program(0)

    @pl.when(c == 1)
    def _():
        program(1)


def solution(mesh):
    dma = pltpu.SemaphoreType.DMA

    def per_device(inputs, gate_weight, up_weight, down_weight, norm_gain, norm_shift):
        any_space = pl.BlockSpec(memory_space=pl.ANY)
        return pl.pallas_call(
            kernel,
            out_shape=jax.ShapeDtypeStruct((T, DB), BF),
            in_specs=[any_space] * 6,
            out_specs=any_space,
            scratch_shapes=[
                pltpu.VMEM((2, NC, TC, DQ), BF),
                pltpu.VMEM((2, NT, DQ, 2 * UT), BF),
                pltpu.VMEM((2, NJ, 2, UT, DQ), BF),
                pltpu.VMEM((2, NJ, 2, DB, UT), BF),
                pltpu.VMEM((2, 2, NJ, UT // 2, DB), BF),
                pltpu.VMEM((2, NC, NJ, 4, 2, ZH, 4 * UT), BF),
                pltpu.VMEM((2, NC, NJ, 2, ZH, 4 * UT), BF),
                pltpu.VMEM((2, NC, NJ, 2, ZH, 4 * UT), BF),
                pltpu.VMEM((2, NC, NJ, 2, ZH, 4 * UT), BF),
                pltpu.VMEM((2, NC, NT, TC, UT), BF),
                pltpu.VMEM((2, NC, 4, 2, YH, DQ), BF),
                pltpu.VMEM((2, NC, 2, YH, DQ), BF),
                pltpu.VMEM((2, NC, 2, YH, DQ), BF),
                pltpu.VMEM((2, NC, 2, YH, DQ), BF),
                pltpu.VMEM((2, NC, 4, R, DQ), BF),
                pltpu.VMEM((2, NC, 3, R, DQ), BF),
                pltpu.VMEM((2, NC, R, DQ), F32),
                pltpu.VMEM((2, NC, R, 128), F32),
                pltpu.VMEM((2, NC, 3, R, 128), F32),
                pltpu.VMEM((NC, 4, R, DB), BF),
                pltpu.VMEM((T, DB), BF),
                pltpu.VMEM((4, 2, DB), F32),
                pltpu.VMEM((4, 2, DB), F32),
                dma((N_SLOTS,)),
                dma((N_SLOTS,)),
                dma((17 + NC,)),
                pltpu.SemaphoreType.REGULAR,
            ],
            compiler_params=pltpu.CompilerParams(
                collective_id=0, has_side_effects=True, vmem_limit_bytes=63 * 1024 * 1024
            ),
        )(inputs, gate_weight, up_weight, down_weight.reshape(LAYERS, TILES, UT, DB), norm_gain, norm_shift)

    return jax.shard_map(
        per_device,
        mesh=mesh,
        in_specs=(P(None, "ra"), P(None, "ra", "cb"), P(None, "ra", "cb"), P(None, "cb", "ra"), P(None, "ra"), P(None, "ra")),
        out_specs=P(None, "ra"),
        check_vma=False,
    )
```

time: 433 us -> 150 us (0.35)
  waiting for transfers between devices: 287 us -> 0 us
  Pallas kernels: 0 us -> 147 us
  blocking collectives: 86.1 us -> 0 us
  matrix products: 20 us -> 0 us
  local copies, waits for them, and re-layouts: 19.1 us -> 2.06 us
  between operations: 13.3 us -> 0.01 us
  starting transfers between devices: 5.34 us -> 0 us
    unnamed x6 -> x0, waiting for transfers between devices: 169 us -> none
    pallas_call x0 -> x1, Pallas kernels: none -> 147 us  [per_device(): pl.pallas_call(kernel, out_shape=jax.ShapeDtypeStruct((T, DB), BF), in_sp...]
    all_gather x2 -> x0, waiting for transfers between devices: 106 us -> none  [sublayer(): lax.all_gather(hidden, RA, axis=0, tiled=True)]
    all_to_all x3 -> x0, blocking collectives: 55.8 us -> none  [the longest x2 38.8 us: from_everyone(): lax.all_to_all(jnp.broadcast_to(shard[None], (peers, *shard.shape)), axis...]
    psum x4 -> x0, blocking collectives: 30.3 us -> none  [over_axes(): return functools.reduce(lax.psum, axes, shard)]
    dot_general x4 -> x0, matrix products: 20 us -> none  [the longest x2 11.5 us: sublayer(): jnp.dot(stream, paired, preferred_element_type=jnp.float32)]
    unnamed x10 -> x1, local copies, waits for them, and re-layouts: 15.2 us -> 2.06 us
    all_to_all x1 -> x0, waiting for transfers between devices: 12.1 us -> none  [sum_at_owner(): lax.all_to_all(parts, axis, split_axis=0, concat_axis=0, tiled=True)]
  transfers between devices with their start and end apart: 5 -> 0, of which waited for: 5 -> 0; matrix products, arithmetic and copies ran while one was open for 0% -> 0% of each run, Pallas kernels for 0% -> 0%
where the time goes in v3:
time: 150 us
  Pallas kernels  147 us (98%)
  local copies, waits for them, and re-layouts  2.06 us (1%)
    pallas_call x1, Pallas kernels, per_device(): pl.pallas_call(kernel, out_shape=jax.ShapeDtypeStruct((T, DB), BF), in_sp...  147 us

profile of v3, /device:TPU:1, one launch (start us, length us, event | category | flops | bytes accessed | tf_op | source)
XLA Modules:
  0.0 149.6 jit_solution(13835490475507969950)
XLA Ops:
  0.0 147.5 %shard_map.64 = bf16[1536,256]{1,0:T(8,128)(2,1)} custom-call(bf16[1536,256]{1,0:T(8,128)(2,1)} %x_hbm.1, bf16[2,256,1408]{2,1,0:T(8,128)(2,1)} %wg_hbm.1, bf16[2,256,1408]{2,1,0:T(8,128)(2,1)} %wu_hbm.1, bf16[2,11,128,256]{3,2,1,0:T(8,128)(2,1)} %bitcast.1, f32[2,256]{1,0:T(2,128)} %gain_hbm.1, f32[2,256]{1,0:T(2,128)} %shift_hbm.1), custom_call_target="tpu_custom_call" | custom-call | tf_op jit(solution)/shard_map/pallas_call | solution.py:613
  147.5 2.1 %copy.8 = bf16[1536,256]{1,0:T(8,128)(2,1)} copy(bf16[1536,256]{1,0:T(8,128)(2,1)} %shard_map.64) | data formatting | bytes 1572864

commit v4 on v3

v4 whole, which is shorter than its diff:
```python
import jax
import jax.numpy as jnp
from jax import lax
from jax.experimental import pallas as pl
from jax.experimental.pallas import tpu as pltpu
from jax.sharding import PartitionSpec as P

MESH = pl.DeviceIdType.MESH
BF = jnp.bfloat16
F32 = jnp.float32
RESIDUAL = 0.5
EPSILON = 1e-05

T, D, FF, LAYERS = 1536, 4096, 11264, 2
NC = 6
TC = T // NC
ZB = TC // 4
ZH = ZB // 2
YB = TC // 4
YH = YB // 2
R = TC // 16
DB = D // 16
DQ = D // 4
UT = 128
NJ = 3
NT = 2 * NJ
TILES = FF // 8 // UT
SHARED = 4 * NJ - TILES

GROUPS = {(l, k): [(0, 1), (1, 2), (2, 3)] for l in range(LAYERS) for k in range(NC)}

SLOTS = {}


def slots(*names):
    for name in names:
        SLOTS.setdefault(name, len(SLOTS))


for l in range(LAYERS):
    for k in range(NC):
        for g in range(len(GROUPS[l, k])):
            for m in ("za", "zb", "zc", "hf", "hk", "hg"):
                slots((m, l, k, g, 0), (m, l, k, g, 1))
        for m in ("ya", "yb", "yc"):
            slots((m, l, k, 0), (m, l, k, 1))
        for m in ("xr", "st"):
            slots((m, l, k, 1), (m, l, k, 2), (m, l, k, 3))
    for j in range(NJ + 1):
        slots(("wr", l, j, 0), ("wr", l, j, 1))
        for cc in range(2):
            slots(("wm", l, j, cc), ("wp", l, j, cc), ("wo", l, j, cc, 0), ("wo", l, j, cc, 1), ("wd", l, j, cc))
for k in range(NC):
    for p in range(LAYERS + 1):
        slots(("xg", p, k, 1), ("xg", p, k, 2), ("xg", p, k, 3))
        for m in ("yf", "yk", "yg"):
            slots((m, p, k, 0), (m, p, k, 1))
    slots(*(("dd", k, n) for n in range(4)), *(("xq", k, d) for d in (1, 2, 3)))
slots(*(("gain", i, d) for i in range(4) for d in (1, 2, 3)))
N_SLOTS = len(SLOTS)
N_SENT = 320
WAIT_LATER = 30

HOP = {1: 1.9, 2: 2.7}
CORE_HOP = 1.0
FROM_HBM = 1.1
LINK = 92e3
CORE_LINK = 500e3
START = 3.5
TIMES = dict(D=0.06, E=0.9, G=0.15, H=0.15, I=0.25, J=0.35, Q=0.08, K=0.08, L=0.06, M=0.05, W=0.12, V=0.06, X=0.05)
SLACK = dict(A=1.5, E=0.5, W=0.5, X=1.0)
FILL = [
    [("X", 0, 1), ("X", 0, 2), ("W", 0, 1), ("W", 0, 2), ("X", 0, 3), ("X", 0, 4), ("X", 0, 5), ("W", 0, 3)],
    [("W", 1, j) for j in range(NJ + 1)],
]
NOT_BEFORE = {("W", 1, 1): 0.0, ("W", 1, 2): 55.0, ("W", 1, 3): 60.0}
SUM_AXIS, UNIT_AXIS = "zx", "xz"


def time_of(task):
    if task[0] in "ABC":
        first, last = GROUPS[task[1], task[2]][task[3]]
        return {"A": 0.43, "B": 0.1, "C": 0.1}[task[0]] * (last - first) + 0.05
    return TIMES[task[0]]


def pair(m, keys, size, axis):
    return [((m, *keys, 0), axis + "+", size, 1), ((m, *keys, 1), axis + "-", size, 1)]


def three(m, keys, size, axis):
    return [((m, *keys, 2), axis + "+", size, 2), ((m, *keys, 1), axis + "+", size, 1), ((m, *keys, 3), axis + "-", size, 1)]


def both_ways(one, two, keys, size, axis):
    return [
        ((one, *keys, 0), axis + "+", size, 1), ((two, *keys, 1), axis + "-", size, 1),
        ((one, *keys, 1), axis + "+", size, 1), ((two, *keys, 0), axis + "-", size, 1)]


def plan():
    tasks = {}
    for l in range(LAYERS):
        axis = UNIT_AXIS[l]
        for j in range(NJ + 1):
            size = 2 * (2 * DB * UT * 2 if j < NJ else NJ * UT * DB * 2)
            tasks["W", l, j] = ([], pair("wr", (l, j), size // 2, axis) + [
                (("wm", l, j), axis + "+", size, 1), (("wp", l, j), axis + "-", size, 1), (("wd", l, j), "c", size // 2, 0)])
            tasks["V", l, j] = ([("wr", l, j, 0), ("wr", l, j, 1)], pair("wo", (l, j), size // 2, axis))
    block = YB * DB * 2
    for k in range(NC):
        tasks["X", 0, k] = ([], three("xg", (0, k), block, "x"))
        tasks["Q", 0, k] = ([("xq", k, d) for d in (1, 2, 3)], three("xg", (1, k), block, "z"))
        for p in range(LAYERS + 1):
            size = YH * (DQ if p < LAYERS else DB) * 2
            tasks["K", p - 1, k] = ([("xg", p, k, d) for d in (1, 2, 3)], both_ways("yf", "yk", (p, k), size, "y"))
            tasks["L", p - 1, k] = ([("yf", p, k, 0), ("yk", p, k, 1)], pair("yg", (p, k), size, "y"))
        tasks["M", LAYERS - 1, k] = ([("yg", LAYERS, k, h) for h in (0, 1)], [(("dd", k), "c", 2 * size, 0)])
        for l in range(LAYERS):
            axis, other_axis = SUM_AXIS[l], UNIT_AXIS[l]
            for g, (first, last) in enumerate(GROUPS[l, k]):
                zs, hs = ZH * 4 * UT * 2 * (last - first), ZH * 2 * UT * 2 * (last - first)
                keys = (l, k, g)
                need = [("yg", l, k, h) for h in (0, 1)] + [("yf", l, k, 1), ("yk", l, k, 0)]
                for j in range(first, last):
                    need += [("wm", l, j), ("wp", l, j), ("wo", l, j, 0), ("wo", l, j, 1), ("wd", l, j)]
                tasks["A", *keys] = (need, pair("za", keys, zs, axis) + pair("zb", keys, zs, axis))
                tasks["B", *keys] = ([("za", *keys, h) for h in (0, 1)], pair("zc", keys, zs, axis))
                tasks["C", *keys] = ([(m, *keys, h) for m in ("zb", "zc") for h in (0, 1)], both_ways("hf", "hk", keys, hs, axis))
                tasks["D", *keys] = ([("hf", *keys, 0), ("hk", *keys, 1)], pair("hg", keys, hs, axis))
            need = [(m, l, k, g, h) for g in range(len(GROUPS[l, k])) for m, h in (("hf", 1), ("hk", 0), ("hg", 0), ("hg", 1))]
            need += [("wm", l, NJ), ("wp", l, NJ), ("wo", l, NJ, 0), ("wo", l, NJ, 1), ("wd", l, NJ)]
            ys, xsz = YH * DQ * 2, R * DQ * 2
            tasks["E", l, k] = (need, pair("ya", (l, k), ys, "y") + pair("yb", (l, k), ys, "y"))
            tasks["G", l, k] = ([("ya", l, k, h) for h in (0, 1)], pair("yc", (l, k), ys, "y"))
            tasks["H", l, k] = ([(m, l, k, h) for m in ("yb", "yc") for h in (0, 1)], three("xr", (l, k), xsz, other_axis))
            tasks["I", l, k] = ([("xr", l, k, d) for d in (1, 2, 3)], three("st", (l, k), R * 512, axis))
            out = ("xq", (k,)) if l + 1 < LAYERS else ("xg", (l + 1, k))
            tasks["J", l, k] = ([("st", l, k, d) for d in (1, 2, 3)], three(*out, xsz // 4, other_axis))
    return tasks


def order(report=None):
    tasks = plan()
    maker = {m[0]: t for t, (_, sends) in tasks.items() for m in sends}
    users = {}
    for t, (needs, _) in tasks.items():
        for m in needs:
            if m in maker:
                users.setdefault(maker[m], set()).add(t)
    rank = {}

    def rest(task):
        if task not in rank:
            rank[task] = time_of(task) + max((rest(u) + 2.0 for u in users.get(task, ())), default=0.0)
        return rank[task]

    arrive, free = {}, {}

    def transmit(task, now):
        more = FROM_HBM if task[0] in "WX" else 0.0
        for m, link, size, hops in tasks[task][1]:
            done = max(now, free.get(link, 0.0)) + (size * hops / LINK if hops else size / CORE_LINK)
            arrive[m] = done + (HOP[hops] if hops else CORE_HOP) + more
            free[link] = done

    now = START
    fill = [list(tasks_of) for tasks_of in FILL]
    out = [("X", 0, 0), ("W", 0, 0)]
    for t in out:
        transmit(t, now)
    left = [t for t in tasks if t not in out]
    while left:
        ready = []
        for t in left:
            needs, sends = tasks[t]
            at = None
            if t[0] in "WX":
                if any(queue and queue[0] == t for queue in fill):
                    at = max(free.get(m[1], 0.0) for m in sends if m[1] != "c") - SLACK[t[0]]
                    at = max(at, NOT_BEFORE.get(t, 0.0))
            elif all(m in arrive for m in needs):
                at = max(arrive[m] for m in needs)
                if t[0] in SLACK:
                    at = max(at, max(free.get(m[1], 0.0) for m in sends) - SLACK[t[0]])
            if at is not None:
                ready.append((at, t))
        at, t = min(ready, key=lambda r: (max(r[0], now), r[1][0] in "WX", r[1][1:3], -rest(r[1])))
        begin = max(now, at)
        now = begin + time_of(t)
        for queue in fill:
            if queue and queue[0] == t:
                queue.pop(0)
        transmit(t, now)
        left.remove(t)
        out.append(t)
        if report is not None:
            report.append((begin, now, t))
    return out


def kernel(
    x_hbm, wg_hbm, wu_hbm, wd_hbm, gain_hbm, shift_hbm, out_hbm,
    xs, wgu, wd, rel, rel_d, part, ra, rb, rc, hid, down, ya, yb, yc, ys, xr, mixed, st, st_in, nb, ov, gains,
    recv, sent, local, go,
):
    ra_at, cb_at = lax.axis_index("ra"), lax.axis_index("cb")
    z, x = ra_at // 4, lax.rem(ra_at, 4)
    y, c = cb_at // 2, lax.rem(cb_at, 2)

    def turn(v, d):
        return lax.rem(v + d, 4)

    zp, zo, zm = turn(z, 1), turn(z, 2), turn(z, 3)
    yp, yo, ym = turn(y, 1), turn(y, 2), turn(y, 3)
    xp, xo, xm = turn(x, 1), turn(x, 2), turn(x, 3)

    def at_z(v):
        return (v * 4 + x, cb_at)

    def at_x(v):
        return (z * 4 + v, cb_at)

    def at_sum(l, v):
        return at_z(v) if SUM_AXIS[l] == "z" else at_x(v)

    def at_unit(l, v):
        return at_x(v) if UNIT_AXIS[l] == "x" else at_z(v)

    def at_unit_main(l, v):
        return (z * 4 + v, y * 2 + 1) if UNIT_AXIS[l] == "x" else (v * 4 + x, y * 2 + 1)

    sums = [(zp, zo, zm, z), (xp, xo, xm, x)]
    unit_at = [(xp, xo, xm, x), (zp, zo, zm, z)]

    def at_y(v):
        return (ra_at, v * 2 + c)

    other = (ra_at, y * 2 + (1 - c))

    peers = [at_z(zp), at_z(zo), at_z(zm), at_x(xp), at_x(xo), at_x(xm), at_y(yp), at_y(ym), other]
    peers += [(z * 4 + xp, y * 2 + (1 - c)), (z * 4 + xm, y * 2 + (1 - c))]
    peers += [(zp * 4 + x, y * 2 + (1 - c)), (zm * 4 + x, y * 2 + (1 - c))]
    barrier = pltpu.get_barrier_semaphore()
    for peer in peers:
        pl.semaphore_signal(barrier, inc=1, device_id=peer, device_id_type=MESH)
    pl.semaphore_wait(barrier, len(peers))

    def arrived(dst, name):
        pltpu.make_async_remote_copy(
            src_ref=dst, dst_ref=dst, send_sem=sent.at[0], recv_sem=recv.at[SLOTS[name]],
            device_id=other, device_id_type=MESH,
        ).wait_recv()

    def d_cols(v):
        return pl.ds(pl.multiple_of(v * DB, DB), DB)

    def tile_of(v):
        return jnp.minimum(v * NJ, TILES - NJ)

    def units(v, j):
        return pl.ds(pl.multiple_of((tile_of(v) + j) * UT, UT), UT)

    def gu_half(l, j, cc, owner, what):
        return wgu.at[l, 2 * j + cc, d_cols(owner), pl.ds(what * UT, UT)]

    def relay_ref(l, j, h):
        return rel.at[l, j, h] if j < NJ else rel_d.at[l, h]

    def w_half(l, j, cc, owner, h):
        if j < NJ:
            return gu_half(l, j, cc, owner, h)
        return wd.at[l, :, cc, pl.ds(h * 64, 64), d_cols(owner)]

    def w_whole(l, j, cc, owner):
        return wgu.at[l, 2 * j + cc, d_cols(owner), :] if j < NJ else wd.at[l, :, cc, :, d_cols(owner)]

    def program(core):
        waits = []
        local_waits = {}

        def send(src, dst, name, dev):
            pltpu.make_async_remote_copy(
                src_ref=src, dst_ref=dst, send_sem=sent.at[len(waits)], recv_sem=recv.at[SLOTS[name]],
                device_id=dev, device_id_type=MESH,
            ).start()

        def all_sent(like):
            waits.append(
                pltpu.make_async_remote_copy(
                    src_ref=like, dst_ref=like, send_sem=sent.at[len(waits)], recv_sem=recv.at[0],
                    device_id=other, device_id_type=MESH,
                ).wait_send
            )

        done = []

        def wait_sent(keep):
            while len(waits) - len(done) > keep:
                waits[len(done)]()
                done.append(True)

        def stage_w(l, j):
            up, opposite, back, me = unit_at[l]
            if j < NJ:
                sources = (wg_hbm, wu_hbm)
                send(wg_hbm.at[l, :, units(opposite, j)], rel.at[l, j, 0], ("wr", l, j, 0), at_unit(l, up))
                send(wu_hbm.at[l, :, units(opposite, j)], rel.at[l, j, 1], ("wr", l, j, 1), at_unit(l, back))
                for what, src in enumerate(sources):
                    for to, m in ((up, "wm"), (back, "wp")):
                        send(
                            src.at[l, :, units(to, j)], gu_half(l, j, core, me, what), (m, l, j, core), at_unit_main(l, to)
                        )
                if core == 0:
                    for what, src in enumerate(sources):
                        send(src.at[l, :, units(me, j)], gu_half(l, j, core, me, what), ("wd", l, j, core), other)
                else:
                    mine = []
                    for what, src in enumerate(sources):
                        copy = pltpu.make_async_copy(
                            src.at[l, :, units(me, j)], gu_half(l, j, core, me, what), local.at[l * 7 + j * 2 + what]
                        )
                        copy.start()
                        mine.append(copy.wait)
                    local_waits[l, j] = mine
                all_sent(wgu.at[l, 0:4 - core, 0:DB, :])
            else:
                def src(v, h=None):
                    if h is None:
                        return wd_hbm.at[l, pl.ds(tile_of(v), NJ)]
                    return wd_hbm.at[l, pl.ds(tile_of(v), NJ), pl.ds(h * 64, 64)]

                send(src(opposite, 0), rel_d.at[l, 0], ("wr", l, j, 0), at_unit(l, up))
                send(src(opposite, 1), rel_d.at[l, 1], ("wr", l, j, 1), at_unit(l, back))
                send(src(up), w_whole(l, j, core, me), ("wm", l, j, core), at_unit_main(l, up))
                send(src(back), w_whole(l, j, core, me), ("wp", l, j, core), at_unit_main(l, back))
                if core == 0:
                    send(src(me), w_whole(l, j, core, me), ("wd", l, j, core), other)
                else:
                    copy = pltpu.make_async_copy(src(me), w_whole(l, j, core, me), local.at[l * 7 + 6])
                    copy.start()
                    local_waits[l, j] = [copy.wait]
                all_sent(wgu.at[l, 0:4 - core, 0:NJ * UT, :])

        def stage_v(l, j):
            up, _, back, _ = unit_at[l]
            for h, (to, owner) in enumerate(((up, back), (back, up))):
                arrived(relay_ref(l, j, h), ("wr", l, j, h))
                send(relay_ref(l, j, h), w_half(l, j, core, owner, h), ("wo", l, j, core, h), at_unit_main(l, to))
            all_sent(wgu.at[l, 0, 0:DB if j < NJ else NJ * UT, :])

        if core == 0:
            for i, (stage, *key) in enumerate([t for t in order() if t[0] in "WV"]):
                if stage == "W":
                    if i:
                        pl.semaphore_wait(go, 1)
                    stage_w(*key)
                else:
                    stage_v(*key)
            for k in range(NC):
                for n, yy in enumerate((y, ym, yp, yo)):
                    arrived(ov.at[pl.ds(pl.multiple_of(k * TC + yy * YB, YB), YB), :], ("dd", k, n))
            copy = pltpu.make_async_copy(ov, out_hbm, local.at[0])
            copy.start()
            wait_sent(0)
            copy.wait()
            return

        def weights_ready(l, j):
            up, opposite, back, me = unit_at[l]
            for wait in local_waits[l, j]:
                wait()
            arrived(w_whole(l, j, 0, me), ("wd", l, j, 0))
            for cc in range(2):
                arrived(w_whole(l, j, cc, back), ("wm", l, j, cc))
                arrived(w_whole(l, j, cc, up), ("wp", l, j, cc))
                arrived(w_half(l, j, cc, opposite, 0), ("wo", l, j, cc, 0))
                arrived(w_half(l, j, cc, opposite, 1), ("wo", l, j, cc, 1))

        def gathered(p, k, at, rows):
            if p < LAYERS:
                return xs.at[p, k, pl.ds(pl.multiple_of(at, rows), rows), :]
            return ov.at[pl.ds(pl.multiple_of(k * TC + at, rows), rows), :]

        def part_rows(v):
            return y * YB + v * R

        in_copies = {}
        y_block = pl.ds(pl.multiple_of(y * YB, YB), YB)

        def stage_x(l, k):
            rows = pl.ds(pl.multiple_of(k * TC + y * YB, YB), YB)
            dst = xs.at[0, k, y_block, d_cols(x)]
            for d in (2, 1, 3):
                send(x_hbm.at[rows, :], dst, ("xg", 0, k, d), at_x(turn(x, d)))
            all_sent(ov.at[0:3 * YB, :])
            in_copies[k] = pltpu.make_async_copy(x_hbm.at[rows, :], dst, local.at[14 + k])
            in_copies[k].start()

        gain_copies = []

        def gains_send():
            for i, (src, axis) in enumerate(((gain_hbm, 0), (shift_hbm, 0), (gain_hbm, 1), (shift_hbm, 1))):
                me = unit_at[axis][3]
                for d in (1, 3, 2):
                    send(src, gains.at[i, me], ("gain", i, d), at_unit(axis, turn(me, d)))
                all_sent(gains.at[i, 0:3])
                copy = pltpu.make_async_copy(src, gains.at[i, me], local.at[14 + NC + i])
                copy.start()
                gain_copies.append(copy)

        seen = set()

        def stage_a(l, k, g):
            first, last = GROUPS[l, k][g]
            if g == 0:
                arrived(gathered(l, k, ym * YB + YH, YH), ("yf", l, k, 1))
                arrived(gathered(l, k, yp * YB, YH), ("yk", l, k, 0))
                arrived(gathered(l, k, yo * YB, YH), ("yg", l, k, 0))
                arrived(gathered(l, k, yo * YB + YH, YH), ("yg", l, k, 1))
            for j in range(first, last):
                if (l, j) not in seen:
                    weights_ready(l, j)
                    seen.add((l, j))

            def tiles(j, carry):
                for n in (0, 1):
                    value = jnp.dot(xs[l, k], wgu[l, 2 * j + n], preferred_element_type=F32).astype(BF)
                    for o in range(4):
                        for h in (0, 1):
                            at = o * ZB + h * ZH
                            part[l, k, j, o, h, :, n * 256:(n + 1) * 256] = value[at:at + ZH]
                return carry

            lax.fori_loop(first, last, tiles, 0)
            js = pl.ds(first, last - first)
            up, opposite, back, _ = sums[l]
            send(part.at[l, k, js, opposite, 0], ra.at[l, k, js, 0], ("za", l, k, g, 0), at_sum(l, up))
            send(part.at[l, k, js, opposite, 1], ra.at[l, k, js, 1], ("za", l, k, g, 1), at_sum(l, back))
            send(part.at[l, k, js, up, 1], rb.at[l, k, js, 0], ("zb", l, k, g, 0), at_sum(l, up))
            send(part.at[l, k, js, back, 0], rb.at[l, k, js, 1], ("zb", l, k, g, 1), at_sum(l, back))
            all_sent(part.at[l, k, js, 0:2])

        def stage_b(l, k, g):
            first, last = GROUPS[l, k][g]
            js = pl.ds(first, last - first)
            up, _, back, _ = sums[l]
            for h, to in enumerate((up, back)):
                arrived(ra.at[l, k, js, h], ("za", l, k, g, h))
                for j in range(first, last):
                    part[l, k, j, to, h] = (part[l, k, j, to, h].astype(F32) + ra[l, k, j, h].astype(F32)).astype(BF)
                send(part.at[l, k, js, to, h], rc.at[l, k, js, h], ("zc", l, k, g, h), at_sum(l, to))
            all_sent(part.at[l, k, js, 0])

        def hid_ref(l, k, g, o, h):
            first, last = GROUPS[l, k][g]
            rows = pl.ds(pl.multiple_of(o * ZB + h * ZH, ZH), ZH)
            return hid.at[l, k, pl.ds(2 * first, 2 * (last - first)), rows, :]

        def stage_c(l, k, g):
            first, last = GROUPS[l, k][g]
            js = pl.ds(first, last - first)
            up, _, back, me = sums[l]
            for h in (0, 1):
                arrived(rb.at[l, k, js, 1 - h], ("zb", l, k, g, 1 - h))
                arrived(rc.at[l, k, js, h], ("zc", l, k, g, h))
                for j in range(first, last):
                    total = (
                        part[l, k, j, me, h].astype(F32) + rc[l, k, j, h].astype(F32) + rb[l, k, j, 1 - h].astype(F32)
                    )
                    for n in (0, 1):
                        gate, lift = total[:, n * 256:n * 256 + UT], total[:, n * 256 + UT:(n + 1) * 256]
                        value = gate * jax.nn.sigmoid(gate) * lift
                        if j < SHARED:
                            value = jnp.where(unit_at[l][3] == 3, jnp.zeros_like(value), value)
                        hid[l, k, 2 * j + n, pl.ds(pl.multiple_of(me * ZB + h * ZH, ZH), ZH), :] = value.astype(BF)
                if h == 0:
                    ref = hid_ref(l, k, g, me, 0)
                    send(ref, ref, ("hf", l, k, g, 0), at_sum(l, up))
            ref = hid_ref(l, k, g, me, 1)
            send(ref, ref, ("hk", l, k, g, 1), at_sum(l, back))
            send(ref, ref, ("hf", l, k, g, 1), at_sum(l, up))
            ref = hid_ref(l, k, g, me, 0)
            send(ref, ref, ("hk", l, k, g, 0), at_sum(l, back))
            all_sent(hid.at[l, k, pl.ds(2 * first, 2 * (last - first)), 0:4 * ZH, :])

        def stage_d(l, k, g):
            first, last = GROUPS[l, k][g]
            up, _, back, _ = sums[l]
            for h, (owner, m, to) in enumerate(((back, "hf", up), (up, "hk", back))):
                ref = hid_ref(l, k, g, owner, h)
                arrived(ref, (m, l, k, g, h))
                send(ref, ref, ("hg", l, k, g, h), at_sum(l, to))
            all_sent(hid.at[l, k, pl.ds(2 * first, 2 * (last - first)), 0:2 * ZH, :])

        def stage_e(l, k):
            up, opposite, back, _ = sums[l]
            for g in range(len(GROUPS[l, k])):
                arrived(hid_ref(l, k, g, back, 1), ("hf", l, k, g, 1))
                arrived(hid_ref(l, k, g, up, 0), ("hk", l, k, g, 0))
                arrived(hid_ref(l, k, g, opposite, 0), ("hg", l, k, g, 0))
                arrived(hid_ref(l, k, g, opposite, 1), ("hg", l, k, g, 1))
            if (l, NJ) not in seen:
                weights_ready(l, NJ)
                seen.add((l, NJ))

            def columns(n, carry):
                lhs = jnp.concatenate([hid[l, k, t] for t in range(NT)], axis=1)
                for i in (0, 1):
                    cols = pl.ds(pl.multiple_of(n * 512 + i * 256, 256), 256)
                    rhs = wd[l, :, :, :, cols].reshape(NT * UT, 256)
                    value = jnp.dot(lhs, rhs, preferred_element_type=F32).astype(BF)
                    for yy in range(4):
                        for h in (0, 1):
                            at = yy * YB + h * YH
                            down[l, k, yy, h, :, cols] = value[at:at + YH]
                return carry

            lax.fori_loop(0, DQ // 512, columns, 0)
            send(down.at[l, k, yo, 0], ya.at[l, k, 0], ("ya", l, k, 0), at_y(yp))
            send(down.at[l, k, yo, 1], ya.at[l, k, 1], ("ya", l, k, 1), at_y(ym))
            send(down.at[l, k, yp, 1], yb.at[l, k, 0], ("yb", l, k, 0), at_y(yp))
            send(down.at[l, k, ym, 0], yb.at[l, k, 1], ("yb", l, k, 1), at_y(ym))
            all_sent(down.at[l, k, 0:2])

        def stage_g(l, k):
            for h, to in enumerate((yp, ym)):
                arrived(ya.at[l, k, h], ("ya", l, k, h))
                down[l, k, to, h] = (down[l, k, to, h].astype(F32) + ya[l, k, h].astype(F32)).astype(BF)
                send(down.at[l, k, to, h], yc.at[l, k, h], ("yc", l, k, h), at_y(to))
            all_sent(down.at[l, k, 0])

        def stage_h(l, k):
            for h in (0, 1):
                arrived(yb.at[l, k, 1 - h], ("yb", l, k, 1 - h))
                arrived(yc.at[l, k, h], ("yc", l, k, h))
                total = down[l, k, y, h].astype(F32) + yc[l, k, h].astype(F32) + yb[l, k, 1 - h].astype(F32)
                ys[l, k, 2 * h] = total[:R].astype(BF)
                ys[l, k, 2 * h + 1] = total[R:].astype(BF)
            me = unit_at[l][3]
            for d in (2, 1, 3):
                send(ys.at[l, k, turn(me, d)], xr.at[l, k, d - 1], ("xr", l, k, d), at_unit(l, turn(me, d)))
            all_sent(ys.at[l, k, 0:3])

        def stage_i(l, k):
            me = unit_at[l][3]
            rows = pl.ds(pl.multiple_of(part_rows(me), R), R)
            value = RESIDUAL * xs[l, k, rows, :].astype(F32) + ys[l, k, me].astype(F32)
            for d in (1, 3, 2):
                arrived(xr.at[l, k, d - 1], ("xr", l, k, d))
                value = value + xr[l, k, d - 1].astype(F32)
            mixed[l, k] = value
            row_sum = jnp.sum(value, axis=1, keepdims=True)
            row_squares = jnp.sum(value * value, axis=1, keepdims=True)
            lane = lax.broadcasted_iota(jnp.int32, (R, 128), 1)
            st[l, k] = jnp.where(lane == 0, row_sum, jnp.where(lane == 1, row_squares, 0.0))
            for d in (2, 1, 3):
                send(st.at[l, k], st_in.at[l, k, d - 1], ("st", l, k, d), at_sum(l, turn(sums[l][3], d)))
            all_sent(st_in.at[l, k])

        def stage_j(l, k):
            me = unit_at[l][3]
            if ("gain", l) not in seen:
                seen.add(("gain", l))
                for i in (2 * l, 2 * l + 1):
                    for d in (1, 3, 2):
                        arrived(gains.at[i, turn(me, 4 - d)], ("gain", i, d))
                    gain_copies[i].wait()
            stats = st[l, k]
            for d in (1, 3, 2):
                arrived(st_in.at[l, k, d - 1], ("st", l, k, d))
                stats = stats + st_in[l, k, d - 1]
            mean = stats[:, 0:1] / D
            var = stats[:, 1:2] / D - mean * mean
            scale = lax.rsqrt(var + EPSILON)
            for q in range(4):
                cols = slice(q * DB, (q + 1) * DB)
                normed = (mixed[l, k, :, cols] - mean) * scale
                nb[l, k, q] = (normed * gains[2 * l, q, l:l + 1, :] + gains[2 * l + 1, q, l:l + 1, :]).astype(BF)

            if l + 1 < LAYERS:
                dst = xs.at[1, k, pl.ds(pl.multiple_of(part_rows(me), R), R), d_cols(z)]
            else:
                dst = gathered(LAYERS, k, part_rows(me), R)
            dst[...] = nb[l, k, me]
            for d in (2, 1, 3):
                name = ("xq", k, d) if l + 1 < LAYERS else ("xg", LAYERS, k, d)
                send(nb.at[l, k, turn(me, d)], dst, name, at_unit(l, turn(me, d)))
            all_sent(nb.at[l, k, 0:3])

        def stage_q(l, k):
            for d in (1, 3, 2):
                rows = pl.ds(pl.multiple_of(part_rows(turn(x, 4 - d)), R), R)
                arrived(xs.at[1, k, rows, d_cols(z)], ("xq", k, d))
            ref = xs.at[1, k, y_block, d_cols(z)]
            for d in (2, 1, 3):
                send(ref, ref, ("xg", 1, k, d), at_z(turn(z, d)))
            all_sent(ov.at[0:3 * YB, :])

        def stage_k(l, k):
            p = l + 1
            for d in (1, 3, 2):
                owner = turn(x if p == 0 else z, 4 - d)
                if p < LAYERS:
                    ref = xs.at[p, k, y_block, d_cols(owner)]
                else:
                    ref = gathered(p, k, part_rows(owner), R)
                arrived(ref, ("xg", p, k, d))
            if p == 0:
                in_copies[k].wait()
            for h in (0, 1):
                ref = gathered(p, k, y * YB + h * YH, YH)
                send(ref, ref, ("yf", p, k, h), at_y(yp))
                ref = gathered(p, k, y * YB + (1 - h) * YH, YH)
                send(ref, ref, ("yk", p, k, 1 - h), at_y(ym))
            if p == LAYERS:
                ref = gathered(p, k, y * YB, YB)
                send(ref, ref, ("dd", k, 0), other)
                all_sent(ov.at[0:6 * YH, :])
            else:
                all_sent(xs.at[p, k, 0:4 * YH, :])

        def stage_l(l, k):
            p = l + 1
            for h, (owner, m, to) in enumerate(((ym, "yf", yp), (yp, "yk", ym))):
                ref = gathered(p, k, owner * YB + h * YH, YH)
                arrived(ref, (m, p, k, h))
                send(ref, ref, ("yg", p, k, h), at_y(to))
            if p == LAYERS:
                for n, (owner, m, h) in enumerate(((ym, "yf", 1), (yp, "yk", 0))):
                    arrived(gathered(p, k, owner * YB + h * YH, YH), (m, p, k, h))
                    ref = gathered(p, k, owner * YB, YB)
                    send(ref, ref, ("dd", k, 1 + n), other)
                all_sent(ov.at[0:6 * YH, :])
            else:
                all_sent(xs.at[p, k, 0:2 * YH, :])

        def stage_m(l, k):
            p = l + 1
            for h in (0, 1):
                arrived(gathered(p, k, yo * YB + h * YH, YH), ("yg", p, k, h))
            ref = gathered(p, k, yo * YB, YB)
            send(ref, ref, ("dd", k, 3), other)
            all_sent(ov.at[0:YB, :])

        def stage_w_both(l, j):
            if l + j == 0:
                stage_w(l, j)
                gains_send()
                return
            pl.semaphore_signal(go, inc=1, device_id=other, device_id_type=MESH)
            stage_w(l, j)

        stages = dict(
            A=stage_a, B=stage_b, C=stage_c, D=stage_d, E=stage_e, G=stage_g, H=stage_h, I=stage_i, J=stage_j,
            K=stage_k, L=stage_l, M=stage_m, Q=stage_q, W=stage_w_both, V=stage_v, X=stage_x,
        )
        for stage, *key in order():
            stages[stage](*key)
            wait_sent(WAIT_LATER)
        copy = pltpu.make_async_copy(ov, out_hbm, local.at[18 + NC])
        copy.start()
        wait_sent(0)
        copy.wait()

    @pl.when(c == 0)
    def _():
        program(0)

    @pl.when(c == 1)
    def _():
        program(1)


def solution(mesh):
    dma = pltpu.SemaphoreType.DMA

    def per_device(inputs, gate_weight, up_weight, down_weight, norm_gain, norm_shift):
        any_space = pl.BlockSpec(memory_space=pl.ANY)
        return pl.pallas_call(
            kernel,
            out_shape=jax.ShapeDtypeStruct((T, DB), BF),
            in_specs=[any_space] * 6,
            out_specs=any_space,
            scratch_shapes=[
                pltpu.VMEM((2, NC, TC, DQ), BF),
                pltpu.VMEM((2, NT, DQ, 2 * UT), BF),
                pltpu.VMEM((2, NJ, 2, UT, DQ), BF),
                pltpu.VMEM((2, NJ, 2, DB, UT), BF),
                pltpu.VMEM((2, 2, NJ, UT // 2, DB), BF),
                pltpu.VMEM((2, NC, NJ, 4, 2, ZH, 4 * UT), BF),
                pltpu.VMEM((2, NC, NJ, 2, ZH, 4 * UT), BF),
                pltpu.VMEM((2, NC, NJ, 2, ZH, 4 * UT), BF),
                pltpu.VMEM((2, NC, NJ, 2, ZH, 4 * UT), BF),
                pltpu.VMEM((2, NC, NT, TC, UT), BF),
                pltpu.VMEM((2, NC, 4, 2, YH, DQ), BF),
                pltpu.VMEM((2, NC, 2, YH, DQ), BF),
                pltpu.VMEM((2, NC, 2, YH, DQ), BF),
                pltpu.VMEM((2, NC, 2, YH, DQ), BF),
                pltpu.VMEM((2, NC, 4, R, DQ), BF),
                pltpu.VMEM((2, NC, 3, R, DQ), BF),
                pltpu.VMEM((2, NC, R, DQ), F32),
                pltpu.VMEM((2, NC, R, 128), F32),
                pltpu.VMEM((2, NC, 3, R, 128), F32),
                pltpu.VMEM((2, NC, 4, R, DB), BF),
                pltpu.VMEM((T, DB), BF),
                pltpu.VMEM((4, 4, 2, DB), F32),
                dma((N_SLOTS,)),
                dma((N_SENT,)),
                dma((19 + NC,)),
                pltpu.SemaphoreType.REGULAR,
            ],
            compiler_params=pltpu.CompilerParams(
                collective_id=0, has_side_effects=True, vmem_limit_bytes=63 * 1024 * 1024
            ),
        )(inputs, gate_weight, up_weight, down_weight.reshape(LAYERS, TILES, UT, DB), norm_gain, norm_shift)

    return jax.shard_map(
        per_device,
        mesh=mesh,
        in_specs=(P(None, "ra"), P(None, "ra", "cb"), P(None, "ra", "cb"), P(None, "cb", "ra"), P(None, "ra"), P(None, "ra")),
        out_specs=P(None, "ra"),
        check_vma=False,
    )
```

time: 150 us -> 144 us (0.960)
  Pallas kernels: 147 us -> 141 us
    pallas_call x1, Pallas kernels: 147 us -> 141 us  [per_device(): pl.pallas_call(kernel, out_shape=jax.ShapeDtypeStruct((T, DB), BF), in_sp...]
where the time goes in v4:
time: 144 us; the launch traced here: 143 us
  Pallas kernels  141 us (98%)
  local copies, waits for them, and re-layouts  2.06 us (1%)
    pallas_call x1, Pallas kernels, per_device(): pl.pallas_call(kernel, out_shape=jax.ShapeDtypeStruct((T, DB), BF), in_sp...  141 us

profile of v4, /device:TPU:1, one launch (start us, length us, event | category | flops | bytes accessed | tf_op | source)
XLA Modules:
  0.0 143.5 jit_solution(15350900753516137204)
XLA Ops:
  0.0 141.4 %shard_map.64 = bf16[1536,256]{1,0:T(8,128)(2,1)} custom-call(bf16[1536,256]{1,0:T(8,128)(2,1)} %x_hbm.1, bf16[2,256,1408]{2,1,0:T(8,128)(2,1)} %wg_hbm.1, bf16[2,256,1408]{2,1,0:T(8,128)(2,1)} %wu_hbm.1, bf16[2,11,128,256]{3,2,1,0:T(8,128)(2,1)} %bitcast.1, f32[2,256]{1,0:T(2,128)} %gain_hbm.1, f32[2,256]{1,0:T(2,128)} %shift_hbm.1), custom_call_target="tpu_custom_call" | custom-call | tf_op jit(solution)/shard_map/pallas_call | solution.py:680
  141.4 2.1 %copy.8 = bf16[1536,256]{1,0:T(8,128)(2,1)} copy(bf16[1536,256]{1,0:T(8,128)(2,1)} %shard_map.64) | data formatting | bytes 1572864

commit v5 on v4

--- a/solution.py
+++ b/solution.py
@@ -37,28 +37,16 @@
         SLOTS.setdefault(name, len(SLOTS))
 
 
+for k in range(NC):
+    for g in range(max(len(GROUPS[l, k]) for l in range(LAYERS))):
+        slots(("za", k, g), ("zc", k, g), ("h0", k, g))
+    slots(*((m, k) for m in ("h1", "ya", "yc", "xr", "st", "xq", "xg", "y0", "y1", "y2")))
 for l in range(LAYERS):
-    for k in range(NC):
-        for g in range(len(GROUPS[l, k])):
-            for m in ("za", "zb", "zc", "hf", "hk", "hg"):
-                slots((m, l, k, g, 0), (m, l, k, g, 1))
-        for m in ("ya", "yb", "yc"):
-            slots((m, l, k, 0), (m, l, k, 1))
-        for m in ("xr", "st"):
-            slots((m, l, k, 1), (m, l, k, 2), (m, l, k, 3))
     for j in range(NJ + 1):
-        slots(("wr", l, j, 0), ("wr", l, j, 1))
-        for cc in range(2):
-            slots(("wm", l, j, cc), ("wp", l, j, cc), ("wo", l, j, cc, 0), ("wo", l, j, cc, 1), ("wd", l, j, cc))
-for k in range(NC):
-    for p in range(LAYERS + 1):
-        slots(("xg", p, k, 1), ("xg", p, k, 2), ("xg", p, k, 3))
-        for m in ("yf", "yk", "yg"):
-            slots((m, p, k, 0), (m, p, k, 1))
-    slots(*(("dd", k, n) for n in range(4)), *(("xq", k, d) for d in (1, 2, 3)))
-slots(*(("gain", i, d) for i in range(4) for d in (1, 2, 3)))
+        slots(("wr", l, j), ("w", l, j))
+slots(("dd",), ("gain",))
 N_SLOTS = len(SLOTS)
-N_SENT = 320
+N_SENT = 40
 WAIT_LATER = 30
 
 HOP = {1: 1.9, 2: 2.7}
@@ -281,14 +269,14 @@
 
         def send(src, dst, name, dev):
             pltpu.make_async_remote_copy(
-                src_ref=src, dst_ref=dst, send_sem=sent.at[len(waits)], recv_sem=recv.at[SLOTS[name]],
+                src_ref=src, dst_ref=dst, send_sem=sent.at[len(waits) % N_SENT], recv_sem=recv.at[SLOTS[name]],
                 device_id=dev, device_id_type=MESH,
             ).start()
 
         def all_sent(like):
             waits.append(
                 pltpu.make_async_remote_copy(
-                    src_ref=like, dst_ref=like, send_sem=sent.at[len(waits)], recv_sem=recv.at[0],
+                    src_ref=like, dst_ref=like, send_sem=sent.at[len(waits) % N_SENT], recv_sem=recv.at[0],
                     device_id=other, device_id_type=MESH,
                 ).wait_send
             )
@@ -304,16 +292,16 @@
             up, opposite, back, me = unit_at[l]
             if j < NJ:
                 sources = (wg_hbm, wu_hbm)
-                send(wg_hbm.at[l, :, units(opposite, j)], rel.at[l, j, 0], ("wr", l, j, 0), at_unit(l, up))
-                send(wu_hbm.at[l, :, units(opposite, j)], rel.at[l, j, 1], ("wr", l, j, 1), at_unit(l, back))
+                send(wg_hbm.at[l, :, units(opposite, j)], rel.at[l, j, 0], ("wr", l, j), at_unit(l, up))
+                send(wu_hbm.at[l, :, units(opposite, j)], rel.at[l, j, 1], ("wr", l, j), at_unit(l, back))
                 for what, src in enumerate(sources):
-                    for to, m in ((up, "wm"), (back, "wp")):
+                    for to in (up, back):
                         send(
-                            src.at[l, :, units(to, j)], gu_half(l, j, core, me, what), (m, l, j, core), at_unit_main(l, to)
+                            src.at[l, :, units(to, j)], gu_half(l, j, core, me, what), ("w", l, j), at_unit_main(l, to)
                         )
                 if core == 0:
                     for what, src in enumerate(sources):
-                        send(src.at[l, :, units(me, j)], gu_half(l, j, core, me, what), ("wd", l, j, core), other)
+                        send(src.at[l, :, units(me, j)], gu_half(l, j, core, me, what), ("w", l, j), other)
                 else:
                     mine = []
                     for what, src in enumerate(sources):
@@ -330,12 +318,12 @@
                         return wd_hbm.at[l, pl.ds(tile_of(v), NJ)]
                     return wd_hbm.at[l, pl.ds(tile_of(v), NJ), pl.ds(h * 64, 64)]
 
-                send(src(opposite, 0), rel_d.at[l, 0], ("wr", l, j, 0), at_unit(l, up))
-                send(src(opposite, 1), rel_d.at[l, 1], ("wr", l, j, 1), at_unit(l, back))
-                send(src(up), w_whole(l, j, core, me), ("wm", l, j, core), at_unit_main(l, up))
-                send(src(back), w_whole(l, j, core, me), ("wp", l, j, core), at_unit_main(l, back))
+                send(src(opposite, 0), rel_d.at[l, 0], ("wr", l, j), at_unit(l, up))
+                send(src(opposite, 1), rel_d.at[l, 1], ("wr", l, j), at_unit(l, back))
+                send(src(up), w_whole(l, j, core, me), ("w", l, j), at_unit_main(l, up))
+                send(src(back), w_whole(l, j, core, me), ("w", l, j), at_unit_main(l, back))
                 if core == 0:
-                    send(src(me), w_whole(l, j, core, me), ("wd", l, j, core), other)
+                    send(src(me), w_whole(l, j, core, me), ("w", l, j), other)
                 else:
                     copy = pltpu.make_async_copy(src(me), w_whole(l, j, core, me), local.at[l * 7 + 6])
                     copy.start()
@@ -344,9 +332,9 @@
 
         def stage_v(l, j):
             up, _, back, _ = unit_at[l]
+            arrived(rel.at[l, j] if j < NJ else rel_d.at[l], ("wr", l, j))
             for h, (to, owner) in enumerate(((up, back), (back, up))):
-                arrived(relay_ref(l, j, h), ("wr", l, j, h))
-                send(relay_ref(l, j, h), w_half(l, j, core, owner, h), ("wo", l, j, core, h), at_unit_main(l, to))
+                send(relay_ref(l, j, h), w_half(l, j, core, owner, h), ("w", l, j), at_unit_main(l, to))
             all_sent(wgu.at[l, 0, 0:DB if j < NJ else NJ * UT, :])
 
         if core == 0:
@@ -357,9 +345,7 @@
                     stage_w(*key)
                 else:
                     stage_v(*key)
-            for k in range(NC):
-                for n, yy in enumerate((y, ym, yp, yo)):
-                    arrived(ov.at[pl.ds(pl.multiple_of(k * TC + yy * YB, YB), YB), :], ("dd", k, n))
+            arrived(ov, ("dd",))
             copy = pltpu.make_async_copy(ov, out_hbm, local.at[0])
             copy.start()
             wait_sent(0)
@@ -367,15 +353,9 @@
             return
 
         def weights_ready(l, j):
-            up, opposite, back, me = unit_at[l]
             for wait in local_waits[l, j]:
                 wait()
-            arrived(w_whole(l, j, 0, me), ("wd", l, j, 0))
-            for cc in range(2):
-                arrived(w_whole(l, j, cc, back), ("wm", l, j, cc))
-                arrived(w_whole(l, j, cc, up), ("wp", l, j, cc))
-                arrived(w_half(l, j, cc, opposite, 0), ("wo", l, j, cc, 0))
-                arrived(w_half(l, j, cc, opposite, 1), ("wo", l, j, cc, 1))
+            arrived(wgu.at[l, 0:2, 0:7 * DB // 2, :] if j < NJ else wgu.at[l, 0:3, 0:7 * UT, :], ("w", l, j))
 
         def gathered(p, k, at, rows):
             if p < LAYERS:
@@ -392,7 +372,7 @@
             rows = pl.ds(pl.multiple_of(k * TC + y * YB, YB), YB)
             dst = xs.at[0, k, y_block, d_cols(x)]
             for d in (2, 1, 3):
-                send(x_hbm.at[rows, :], dst, ("xg", 0, k, d), at_x(turn(x, d)))
+                send(x_hbm.at[rows, :], dst, ("xg", k), at_x(turn(x, d)))
             all_sent(ov.at[0:3 * YB, :])
             in_copies[k] = pltpu.make_async_copy(x_hbm.at[rows, :], dst, local.at[14 + k])
             in_copies[k].start()
@@ -403,7 +383,7 @@
             for i, (src, axis) in enumerate(((gain_hbm, 0), (shift_hbm, 0), (gain_hbm, 1), (shift_hbm, 1))):
                 me = unit_at[axis][3]
                 for d in (1, 3, 2):
-                    send(src, gains.at[i, me], ("gain", i, d), at_unit(axis, turn(me, d)))
+                    send(src, gains.at[i, me], ("gain",), at_unit(axis, turn(me, d)))
                 all_sent(gains.at[i, 0:3])
                 copy = pltpu.make_async_copy(src, gains.at[i, me], local.at[14 + NC + i])
                 copy.start()
@@ -414,10 +394,8 @@
         def stage_a(l, k, g):
             first, last = GROUPS[l, k][g]
             if g == 0:
-                arrived(gathered(l, k, ym * YB + YH, YH), ("yf", l, k, 1))
-                arrived(gathered(l, k, yp * YB, YH), ("yk", l, k, 0))
-                arrived(gathered(l, k, yo * YB, YH), ("yg", l, k, 0))
-                arrived(gathered(l, k, yo * YB + YH, YH), ("yg", l, k, 1))
+                arrived(xs.at[l, k, 0:YB, :], ("y1", k))
+                arrived(xs.at[l, k, 0:YB, :], ("y2", k))
             for j in range(first, last):
                 if (l, j) not in seen:
                     weights_ready(l, j)
@@ -435,21 +413,21 @@
             lax.fori_loop(first, last, tiles, 0)
             js = pl.ds(first, last - first)
             up, opposite, back, _ = sums[l]
-            send(part.at[l, k, js, opposite, 0], ra.at[l, k, js, 0], ("za", l, k, g, 0), at_sum(l, up))
-            send(part.at[l, k, js, opposite, 1], ra.at[l, k, js, 1], ("za", l, k, g, 1), at_sum(l, back))
-            send(part.at[l, k, js, up, 1], rb.at[l, k, js, 0], ("zb", l, k, g, 0), at_sum(l, up))
-            send(part.at[l, k, js, back, 0], rb.at[l, k, js, 1], ("zb", l, k, g, 1), at_sum(l, back))
+            send(part.at[l, k, js, opposite, 0], ra.at[l, k, js, 0], ("za", k, g), at_sum(l, up))
+            send(part.at[l, k, js, opposite, 1], ra.at[l, k, js, 1], ("za", k, g), at_sum(l, back))
+            send(part.at[l, k, js, up, 1], rb.at[l, k, js, 0], ("zc", k, g), at_sum(l, up))
+            send(part.at[l, k, js, back, 0], rb.at[l, k, js, 1], ("zc", k, g), at_sum(l, back))
             all_sent(part.at[l, k, js, 0:2])
 
         def stage_b(l, k, g):
             first, last = GROUPS[l, k][g]
             js = pl.ds(first, last - first)
             up, _, back, _ = sums[l]
+            arrived(ra.at[l, k, js], ("za", k, g))
             for h, to in enumerate((up, back)):
-                arrived(ra.at[l, k, js, h], ("za", l, k, g, h))
                 for j in range(first, last):
                     part[l, k, j, to, h] = (part[l, k, j, to, h].astype(F32) + ra[l, k, j, h].astype(F32)).astype(BF)
-                send(part.at[l, k, js, to, h], rc.at[l, k, js, h], ("zc", l, k, g, h), at_sum(l, to))
+                send(part.at[l, k, js, to, h], rc.at[l, k, js, h], ("zc", k, g), at_sum(l, to))
             all_sent(part.at[l, k, js, 0])
 
         def hid_ref(l, k, g, o, h):
@@ -461,9 +439,8 @@
             first, last = GROUPS[l, k][g]
             js = pl.ds(first, last - first)
             up, _, back, me = sums[l]
+            arrived(part.at[l, k, js, 0:2], ("zc", k, g))
             for h in (0, 1):
-                arrived(rb.at[l, k, js, 1 - h], ("zb", l, k, g, 1 - h))
-                arrived(rc.at[l, k, js, h], ("zc", l, k, g, h))
                 for j in range(first, last):
                     total = (
                         part[l, k, j, me, h].astype(F32) + rc[l, k, j, h].astype(F32) + rb[l, k, j, 1 - h].astype(F32)
@@ -476,30 +453,25 @@
                         hid[l, k, 2 * j + n, pl.ds(pl.multiple_of(me * ZB + h * ZH, ZH), ZH), :] = value.astype(BF)
                 if h == 0:
                     ref = hid_ref(l, k, g, me, 0)
-                    send(ref, ref, ("hf", l, k, g, 0), at_sum(l, up))
+                    send(ref, ref, ("h0", k, g), at_sum(l, up))
             ref = hid_ref(l, k, g, me, 1)
-            send(ref, ref, ("hk", l, k, g, 1), at_sum(l, back))
-            send(ref, ref, ("hf", l, k, g, 1), at_sum(l, up))
+            send(ref, ref, ("h0", k, g), at_sum(l, back))
+            send(ref, ref, ("h1", k), at_sum(l, up))
             ref = hid_ref(l, k, g, me, 0)
-            send(ref, ref, ("hk", l, k, g, 0), at_sum(l, back))
+            send(ref, ref, ("h1", k), at_sum(l, back))
             all_sent(hid.at[l, k, pl.ds(2 * first, 2 * (last - first)), 0:4 * ZH, :])
 
         def stage_d(l, k, g):
             first, last = GROUPS[l, k][g]
             up, _, back, _ = sums[l]
-            for h, (owner, m, to) in enumerate(((back, "hf", up), (up, "hk", back))):
+            arrived(hid.at[l, k, pl.ds(2 * first, 2 * (last - first)), 0:2 * ZH, :], ("h0", k, g))
+            for h, (owner, to) in enumerate(((back, up), (up, back))):
                 ref = hid_ref(l, k, g, owner, h)
-                arrived(ref, (m, l, k, g, h))
-                send(ref, ref, ("hg", l, k, g, h), at_sum(l, to))
+                send(ref, ref, ("h1", k), at_sum(l, to))
             all_sent(hid.at[l, k, pl.ds(2 * first, 2 * (last - first)), 0:2 * ZH, :])
 
         def stage_e(l, k):
-            up, opposite, back, _ = sums[l]
-            for g in range(len(GROUPS[l, k])):
-                arrived(hid_ref(l, k, g, back, 1), ("hf", l, k, g, 1))
-                arrived(hid_ref(l, k, g, up, 0), ("hk", l, k, g, 0))
-                arrived(hid_ref(l, k, g, opposite, 0), ("hg", l, k, g, 0))
-                arrived(hid_ref(l, k, g, opposite, 1), ("hg", l, k, g, 1))
+            arrived(hid.at[l, k, :, 0:4 * ZH, :], ("h1", k))
             if (l, NJ) not in seen:
                 weights_ready(l, NJ)
                 seen.add((l, NJ))
@@ -517,37 +489,36 @@
                 return carry
 
             lax.fori_loop(0, DQ // 512, columns, 0)
-            send(down.at[l, k, yo, 0], ya.at[l, k, 0], ("ya", l, k, 0), at_y(yp))
-            send(down.at[l, k, yo, 1], ya.at[l, k, 1], ("ya", l, k, 1), at_y(ym))
-            send(down.at[l, k, yp, 1], yb.at[l, k, 0], ("yb", l, k, 0), at_y(yp))
-            send(down.at[l, k, ym, 0], yb.at[l, k, 1], ("yb", l, k, 1), at_y(ym))
+            send(down.at[l, k, yo, 0], ya.at[l, k, 0], ("ya", k), at_y(yp))
+            send(down.at[l, k, yo, 1], ya.at[l, k, 1], ("ya", k), at_y(ym))
+            send(down.at[l, k, yp, 1], yb.at[l, k, 0], ("yc", k), at_y(yp))
+            send(down.at[l, k, ym, 0], yb.at[l, k, 1], ("yc", k), at_y(ym))
             all_sent(down.at[l, k, 0:2])
 
         def stage_g(l, k):
+            arrived(ya.at[l, k], ("ya", k))
             for h, to in enumerate((yp, ym)):
-                arrived(ya.at[l, k, h], ("ya", l, k, h))
                 down[l, k, to, h] = (down[l, k, to, h].astype(F32) + ya[l, k, h].astype(F32)).astype(BF)
-                send(down.at[l, k, to, h], yc.at[l, k, h], ("yc", l, k, h), at_y(to))
+                send(down.at[l, k, to, h], yc.at[l, k, h], ("yc", k), at_y(to))
             all_sent(down.at[l, k, 0])
 
         def stage_h(l, k):
+            arrived(down.at[l, k, 0:2], ("yc", k))
             for h in (0, 1):
-                arrived(yb.at[l, k, 1 - h], ("yb", l, k, 1 - h))
-                arrived(yc.at[l, k, h], ("yc", l, k, h))
                 total = down[l, k, y, h].astype(F32) + yc[l, k, h].astype(F32) + yb[l, k, 1 - h].astype(F32)
                 ys[l, k, 2 * h] = total[:R].astype(BF)
                 ys[l, k, 2 * h + 1] = total[R:].astype(BF)
             me = unit_at[l][3]
             for d in (2, 1, 3):
-                send(ys.at[l, k, turn(me, d)], xr.at[l, k, d - 1], ("xr", l, k, d), at_unit(l, turn(me, d)))
+                send(ys.at[l, k, turn(me, d)], xr.at[l, k, d - 1], ("xr", k), at_unit(l, turn(me, d)))
             all_sent(ys.at[l, k, 0:3])
 
         def stage_i(l, k):
             me = unit_at[l][3]
             rows = pl.ds(pl.multiple_of(part_rows(me), R), R)
             value = RESIDUAL * xs[l, k, rows, :].astype(F32) + ys[l, k, me].astype(F32)
+            arrived(xr.at[l, k], ("xr", k))
             for d in (1, 3, 2):
-                arrived(xr.at[l, k, d - 1], ("xr", l, k, d))
                 value = value + xr[l, k, d - 1].astype(F32)
             mixed[l, k] = value
             row_sum = jnp.sum(value, axis=1, keepdims=True)
@@ -555,20 +526,19 @@
             lane = lax.broadcasted_iota(jnp.int32, (R, 128), 1)
             st[l, k] = jnp.where(lane == 0, row_sum, jnp.where(lane == 1, row_squares, 0.0))
             for d in (2, 1, 3):
-                send(st.at[l, k], st_in.at[l, k, d - 1], ("st", l, k, d), at_sum(l, turn(sums[l][3], d)))
+                send(st.at[l, k], st_in.at[l, k, d - 1], ("st", k), at_sum(l, turn(sums[l][3], d)))
             all_sent(st_in.at[l, k])
 
         def stage_j(l, k):
             me = unit_at[l][3]
-            if ("gain", l) not in seen:
-                seen.add(("gain", l))
-                for i in (2 * l, 2 * l + 1):
-                    for d in (1, 3, 2):
-                        arrived(gains.at[i, turn(me, 4 - d)], ("gain", i, d))
-                    gain_copies[i].wait()
+            if ("gain",) not in seen:
+                seen.add(("gain",))
+                arrived(gains.at[0:3], ("gain",))
+                for copy in gain_copies:
+                    copy.wait()
             stats = st[l, k]
+            arrived(st_in.at[l, k], ("st", k))
             for d in (1, 3, 2):
-                arrived(st_in.at[l, k, d - 1], ("st", l, k, d))
                 stats = stats + st_in[l, k, d - 1]
             mean = stats[:, 0:1] / D
             var = stats[:, 1:2] / D - mean * mean
@@ -584,63 +554,55 @@
                 dst = gathered(LAYERS, k, part_rows(me), R)
             dst[...] = nb[l, k, me]
             for d in (2, 1, 3):
-                name = ("xq", k, d) if l + 1 < LAYERS else ("xg", LAYERS, k, d)
+                name = ("xq", k) if l + 1 < LAYERS else ("xg", k)
                 send(nb.at[l, k, turn(me, d)], dst, name, at_unit(l, turn(me, d)))
             all_sent(nb.at[l, k, 0:3])
 
         def stage_q(l, k):
-            for d in (1, 3, 2):
-                rows = pl.ds(pl.multiple_of(part_rows(turn(x, 4 - d)), R), R)
-                arrived(xs.at[1, k, rows, d_cols(z)], ("xq", k, d))
+            arrived(nb.at[0, k, 0:3], ("xq", k))
             ref = xs.at[1, k, y_block, d_cols(z)]
             for d in (2, 1, 3):
-                send(ref, ref, ("xg", 1, k, d), at_z(turn(z, d)))
+                send(ref, ref, ("xg", k), at_z(turn(z, d)))
             all_sent(ov.at[0:3 * YB, :])
 
         def stage_k(l, k):
             p = l + 1
-            for d in (1, 3, 2):
-                owner = turn(x if p == 0 else z, 4 - d)
-                if p < LAYERS:
-                    ref = xs.at[p, k, y_block, d_cols(owner)]
-                else:
-                    ref = gathered(p, k, part_rows(owner), R)
-                arrived(ref, ("xg", p, k, d))
+            arrived(ov.at[0:3 * YB, :] if p < LAYERS else nb.at[1, k, 0:3], ("xg", k))
             if p == 0:
                 in_copies[k].wait()
             for h in (0, 1):
                 ref = gathered(p, k, y * YB + h * YH, YH)
-                send(ref, ref, ("yf", p, k, h), at_y(yp))
+                send(ref, ref, (("y0", "y1")[h], k), at_y(yp))
                 ref = gathered(p, k, y * YB + (1 - h) * YH, YH)
-                send(ref, ref, ("yk", p, k, 1 - h), at_y(ym))
+                send(ref, ref, (("y0", "y1")[h], k), at_y(ym))
             if p == LAYERS:
                 ref = gathered(p, k, y * YB, YB)
-                send(ref, ref, ("dd", k, 0), other)
+                send(ref, ref, ("dd",), other)
                 all_sent(ov.at[0:6 * YH, :])
             else:
                 all_sent(xs.at[p, k, 0:4 * YH, :])
 
         def stage_l(l, k):
             p = l + 1
-            for h, (owner, m, to) in enumerate(((ym, "yf", yp), (yp, "yk", ym))):
+            halves = (lambda n: xs.at[p, k, 0:n * YH, :]) if p < LAYERS else (lambda n: ov.at[0:n * YH, :])
+            arrived(halves(2), ("y0", k))
+            for h, (owner, to) in enumerate(((ym, yp), (yp, ym))):
                 ref = gathered(p, k, owner * YB + h * YH, YH)
-                arrived(ref, (m, p, k, h))
-                send(ref, ref, ("yg", p, k, h), at_y(to))
+                send(ref, ref, ("y2", k), at_y(to))
             if p == LAYERS:
-                for n, (owner, m, h) in enumerate(((ym, "yf", 1), (yp, "yk", 0))):
-                    arrived(gathered(p, k, owner * YB + h * YH, YH), (m, p, k, h))
+                arrived(halves(2), ("y1", k))
+                for owner in (ym, yp):
                     ref = gathered(p, k, owner * YB, YB)
-                    send(ref, ref, ("dd", k, 1 + n), other)
+                    send(ref, ref, ("dd",), other)
                 all_sent(ov.at[0:6 * YH, :])
             else:
                 all_sent(xs.at[p, k, 0:2 * YH, :])
 
         def stage_m(l, k):
             p = l + 1
-            for h in (0, 1):
-                arrived(gathered(p, k, yo * YB + h * YH, YH), ("yg", p, k, h))
+            arrived(ov.at[0:YB, :], ("y2", k))
             ref = gathered(p, k, yo * YB, YB)
-            send(ref, ref, ("dd", k, 3), other)
+            send(ref, ref, ("dd",), other)
             all_sent(ov.at[0:YB, :])
 
         def stage_w_both(l, j):

time: 144 us -> 137 us (0.951)
  Pallas kernels: 141 us -> 134 us
    pallas_call x1, Pallas kernels: 141 us -> 134 us  [per_device(): pl.pallas_call(kernel, out_shape=jax.ShapeDtypeStruct((T, DB), BF), in_sp...]
where the time goes in v5:
time: 137 us
  Pallas kernels  134 us (98%)
  local copies, waits for them, and re-layouts  2.06 us (2%)
    pallas_call x1, Pallas kernels, per_device(): pl.pallas_call(kernel, out_shape=jax.ShapeDtypeStruct((T, DB), BF), in_sp...  134 us

profile of v5, /device:TPU:1, one launch (start us, length us, event | category | flops | bytes accessed | tf_op | source)
XLA Modules:
  0.0 136.5 jit_solution(17354642942011860952)
XLA Ops:
  0.0 134.5 %shard_map.64 = bf16[1536,256]{1,0:T(8,128)(2,1)} custom-call(bf16[1536,256]{1,0:T(8,128)(2,1)} %x_hbm.1, bf16[2,256,1408]{2,1,0:T(8,128)(2,1)} %wg_hbm.1, bf16[2,256,1408]{2,1,0:T(8,128)(2,1)} %wu_hbm.1, bf16[2,11,128,256]{3,2,1,0:T(8,128)(2,1)} %bitcast.1, f32[2,256]{1,0:T(2,128)} %gain_hbm.1, f32[2,256]{1,0:T(2,128)} %shift_hbm.1), custom_call_target="tpu_custom_call" | custom-call | tf_op jit(solution)/shard_map/pallas_call | solution.py:642
  134.5 2.1 %copy.8 = bf16[1536,256]{1,0:T(8,128)(2,1)} copy(bf16[1536,256]{1,0:T(8,128)(2,1)} %shard_map.64) | data formatting | bytes 1572864

commit v6 on v5

--- a/solution.py
+++ b/solution.py
@@ -27,7 +27,7 @@
 TILES = FF // 8 // UT
 SHARED = 4 * NJ - TILES
 
-GROUPS = {(l, k): [(0, 1), (1, 2), (2, 3)] for l in range(LAYERS) for k in range(NC)}
+GROUPS = {(l, k): [(0, 1), (1, 2), (2, 3)] if l == 0 else [(0, 1), (1, 3)] for l in range(LAYERS) for k in range(NC)}
 
 SLOTS = {}
 
@@ -44,147 +44,49 @@
 for l in range(LAYERS):
     for j in range(NJ + 1):
         slots(("wr", l, j), ("w", l, j))
-slots(("dd",), ("gain",))
+slots(("gain",), *(("dd", k) for k in range(NC)))
 N_SLOTS = len(SLOTS)
 N_SENT = 40
 WAIT_LATER = 30
 
-HOP = {1: 1.9, 2: 2.7}
-CORE_HOP = 1.0
-FROM_HBM = 1.1
-LINK = 92e3
-CORE_LINK = 500e3
-START = 3.5
-TIMES = dict(D=0.06, E=0.9, G=0.15, H=0.15, I=0.25, J=0.35, Q=0.08, K=0.08, L=0.06, M=0.05, W=0.12, V=0.06, X=0.05)
-SLACK = dict(A=1.5, E=0.5, W=0.5, X=1.0)
-FILL = [
-    [("X", 0, 1), ("X", 0, 2), ("W", 0, 1), ("W", 0, 2), ("X", 0, 3), ("X", 0, 4), ("X", 0, 5), ("W", 0, 3)],
-    [("W", 1, j) for j in range(NJ + 1)],
+SUM_AXIS, UNIT_AXIS = "zx", "xz"
+ORDER = [
+    ("X", 0, 0), ("W", 0, 0), ("W", 1, 0), ("W", 1, 1), ("S", 0, 0), ("X", 0, 2), ("X", 0, 3), ("X", 0, 4),
+    ("W", 1, 2), ("X", 0, 1), ("V", 0, 0), ("X", 0, 5), ("K", -1, 0), ("S", 0, 2), ("S", 0, 3), ("W", 0, 1),
+    ("L", -1, 0), ("K", -1, 2), ("S", 0, 4), ("K", -1, 3), ("A", 0, 0, 0), ("V", 1, 0), ("L", -1, 2), ("V", 0, 1),
+    ("W", 0, 2), ("L", -1, 3), ("K", -1, 4), ("B", 0, 0, 0), ("S", 0, 1), ("A", 0, 2, 0), ("A", 0, 2, 1),
+    ("A", 0, 0, 1), ("L", -1, 4), ("C", 0, 0, 0), ("A", 0, 3, 0), ("A", 0, 3, 1), ("V", 0, 2), ("B", 0, 2, 0),
+    ("B", 0, 0, 1), ("B", 0, 2, 1), ("A", 0, 4, 1), ("S", 0, 5), ("W", 0, 3), ("D", 0, 0, 0), ("K", -1, 1),
+    ("A", 0, 4, 0), ("A", 0, 0, 2), ("A", 0, 2, 2), ("C", 0, 2, 1), ("C", 0, 0, 1), ("B", 0, 0, 2), ("B", 0, 3, 0),
+    ("L", -1, 1), ("B", 0, 2, 2), ("C", 0, 2, 0), ("A", 0, 3, 2), ("V", 0, 3), ("D", 0, 2, 1), ("C", 0, 0, 2),
+    ("K", -1, 5), ("D", 0, 0, 1), ("B", 0, 3, 1), ("C", 0, 2, 2), ("A", 0, 4, 2), ("D", 0, 2, 0), ("D", 0, 0, 2),
+    ("B", 0, 3, 2), ("A", 0, 1, 0), ("L", -1, 5), ("D", 0, 2, 2), ("C", 0, 3, 1), ("C", 0, 3, 0), ("A", 0, 1, 2),
+    ("B", 0, 4, 2), ("B", 0, 4, 0), ("E", 0, 0), ("C", 0, 3, 2), ("B", 0, 1, 0), ("E", 0, 2), ("D", 0, 3, 0),
+    ("B", 0, 4, 1), ("B", 0, 1, 2), ("D", 0, 3, 1), ("A", 0, 1, 1), ("G", 0, 0), ("C", 0, 4, 2), ("D", 0, 3, 2),
+    ("A", 0, 5, 2), ("C", 0, 4, 0), ("G", 0, 2), ("A", 0, 5, 0), ("C", 0, 4, 1), ("B", 0, 1, 1), ("C", 0, 1, 2),
+    ("C", 0, 1, 0), ("H", 0, 0), ("A", 0, 5, 1), ("E", 0, 3), ("B", 0, 5, 0), ("H", 0, 2), ("D", 0, 4, 1),
+    ("D", 0, 4, 0), ("C", 0, 1, 1), ("D", 0, 4, 2), ("B", 0, 5, 2), ("I", 0, 0), ("B", 0, 5, 1), ("D", 0, 1, 0),
+    ("D", 0, 1, 2), ("G", 0, 3), ("D", 0, 1, 1), ("C", 0, 5, 0), ("E", 0, 4), ("C", 0, 5, 2), ("C", 0, 5, 1),
+    ("I", 0, 2), ("J", 0, 0), ("E", 0, 1), ("H", 0, 3), ("D", 0, 5, 0), ("D", 0, 5, 2), ("D", 0, 5, 1), ("G", 0, 4),
+    ("Q", 0, 0), ("J", 0, 2), ("G", 0, 1), ("E", 0, 5), ("I", 0, 3), ("H", 0, 4), ("Q", 0, 2), ("K", 0, 0),
+    ("H", 0, 1), ("V", 1, 2), ("G", 0, 5), ("J", 0, 3), ("I", 0, 4), ("V", 1, 1), ("L", 0, 0), ("K", 0, 2),
+    ("I", 0, 1), ("H", 0, 5), ("Q", 0, 3), ("J", 0, 4), ("A", 1, 0, 0), ("L", 0, 2), ("A", 1, 0, 1), ("K", 0, 3),
+    ("I", 0, 5), ("J", 0, 1), ("B", 1, 0, 0), ("Q", 0, 4), ("A", 1, 2, 0), ("B", 1, 0, 1), ("A", 1, 2, 1),
+    ("L", 0, 3), ("J", 0, 5), ("Q", 0, 1), ("C", 1, 0, 0), ("B", 1, 2, 0), ("K", 0, 4), ("C", 1, 0, 1),
+    ("B", 1, 2, 1), ("A", 1, 3, 1), ("Q", 0, 5), ("W", 1, 3), ("D", 1, 0, 1), ("L", 0, 4), ("K", 0, 1),
+    ("A", 1, 3, 0), ("C", 1, 2, 1), ("B", 1, 3, 1), ("C", 1, 2, 0), ("A", 1, 4, 0), ("B", 1, 3, 0), ("K", 0, 5),
+    ("A", 1, 4, 1), ("L", 0, 1), ("B", 1, 4, 0), ("D", 1, 2, 0), ("C", 1, 3, 1), ("D", 1, 2, 1), ("V", 1, 3),
+    ("C", 1, 3, 0), ("L", 0, 5), ("D", 1, 0, 0), ("B", 1, 4, 1), ("A", 1, 1, 0), ("C", 1, 4, 0), ("A", 1, 1, 1),
+    ("A", 1, 5, 0), ("D", 1, 3, 1), ("D", 1, 3, 0), ("A", 1, 5, 1), ("C", 1, 4, 1), ("B", 1, 1, 0), ("E", 1, 2),
+    ("E", 1, 0), ("B", 1, 1, 1), ("E", 1, 3), ("D", 1, 4, 0), ("B", 1, 5, 1), ("D", 1, 4, 1), ("G", 1, 2),
+    ("C", 1, 1, 0), ("G", 1, 0), ("B", 1, 5, 0), ("C", 1, 1, 1), ("G", 1, 3), ("C", 1, 5, 1), ("E", 1, 4),
+    ("C", 1, 5, 0), ("D", 1, 1, 0), ("H", 1, 2), ("D", 1, 1, 1), ("H", 1, 3), ("H", 1, 0), ("D", 1, 5, 1),
+    ("D", 1, 5, 0), ("G", 1, 4), ("E", 1, 1), ("I", 1, 2), ("E", 1, 5), ("I", 1, 3), ("H", 1, 4), ("I", 1, 0),
+    ("G", 1, 1), ("J", 1, 2), ("G", 1, 5), ("J", 1, 3), ("J", 1, 0), ("H", 1, 1), ("I", 1, 4), ("K", 1, 2),
+    ("H", 1, 5), ("K", 1, 3), ("J", 1, 4), ("I", 1, 1), ("L", 1, 2), ("K", 1, 0), ("L", 1, 3), ("I", 1, 5),
+    ("L", 1, 0), ("M", 1, 3), ("M", 1, 2), ("J", 1, 1), ("K", 1, 4), ("J", 1, 5), ("M", 1, 0), ("L", 1, 4),
+    ("K", 1, 1), ("K", 1, 5), ("L", 1, 1), ("M", 1, 4), ("L", 1, 5), ("M", 1, 1), ("M", 1, 5),
 ]
-NOT_BEFORE = {("W", 1, 1): 0.0, ("W", 1, 2): 55.0, ("W", 1, 3): 60.0}
-SUM_AXIS, UNIT_AXIS = "zx", "xz"
-
-
-def time_of(task):
-    if task[0] in "ABC":
-        first, last = GROUPS[task[1], task[2]][task[3]]
-        return {"A": 0.43, "B": 0.1, "C": 0.1}[task[0]] * (last - first) + 0.05
-    return TIMES[task[0]]
-
-
-def pair(m, keys, size, axis):
-    return [((m, *keys, 0), axis + "+", size, 1), ((m, *keys, 1), axis + "-", size, 1)]
-
-
-def three(m, keys, size, axis):
-    return [((m, *keys, 2), axis + "+", size, 2), ((m, *keys, 1), axis + "+", size, 1), ((m, *keys, 3), axis + "-", size, 1)]
-
-
-def both_ways(one, two, keys, size, axis):
-    return [
-        ((one, *keys, 0), axis + "+", size, 1), ((two, *keys, 1), axis + "-", size, 1),
-        ((one, *keys, 1), axis + "+", size, 1), ((two, *keys, 0), axis + "-", size, 1)]
-
-
-def plan():
-    tasks = {}
-    for l in range(LAYERS):
-        axis = UNIT_AXIS[l]
-        for j in range(NJ + 1):
-            size = 2 * (2 * DB * UT * 2 if j < NJ else NJ * UT * DB * 2)
-            tasks["W", l, j] = ([], pair("wr", (l, j), size // 2, axis) + [
-                (("wm", l, j), axis + "+", size, 1), (("wp", l, j), axis + "-", size, 1), (("wd", l, j), "c", size // 2, 0)])
-            tasks["V", l, j] = ([("wr", l, j, 0), ("wr", l, j, 1)], pair("wo", (l, j), size // 2, axis))
-    block = YB * DB * 2
-    for k in range(NC):
-        tasks["X", 0, k] = ([], three("xg", (0, k), block, "x"))
-        tasks["Q", 0, k] = ([("xq", k, d) for d in (1, 2, 3)], three("xg", (1, k), block, "z"))
-        for p in range(LAYERS + 1):
-            size = YH * (DQ if p < LAYERS else DB) * 2
-            tasks["K", p - 1, k] = ([("xg", p, k, d) for d in (1, 2, 3)], both_ways("yf", "yk", (p, k), size, "y"))
-            tasks["L", p - 1, k] = ([("yf", p, k, 0), ("yk", p, k, 1)], pair("yg", (p, k), size, "y"))
-        tasks["M", LAYERS - 1, k] = ([("yg", LAYERS, k, h) for h in (0, 1)], [(("dd", k), "c", 2 * size, 0)])
-        for l in range(LAYERS):
-            axis, other_axis = SUM_AXIS[l], UNIT_AXIS[l]
-            for g, (first, last) in enumerate(GROUPS[l, k]):
-                zs, hs = ZH * 4 * UT * 2 * (last - first), ZH * 2 * UT * 2 * (last - first)
-                keys = (l, k, g)
-                need = [("yg", l, k, h) for h in (0, 1)] + [("yf", l, k, 1), ("yk", l, k, 0)]
-                for j in range(first, last):
-                    need += [("wm", l, j), ("wp", l, j), ("wo", l, j, 0), ("wo", l, j, 1), ("wd", l, j)]
-                tasks["A", *keys] = (need, pair("za", keys, zs, axis) + pair("zb", keys, zs, axis))
-                tasks["B", *keys] = ([("za", *keys, h) for h in (0, 1)], pair("zc", keys, zs, axis))
-                tasks["C", *keys] = ([(m, *keys, h) for m in ("zb", "zc") for h in (0, 1)], both_ways("hf", "hk", keys, hs, axis))
-                tasks["D", *keys] = ([("hf", *keys, 0), ("hk", *keys, 1)], pair("hg", keys, hs, axis))
-            need = [(m, l, k, g, h) for g in range(len(GROUPS[l, k])) for m, h in (("hf", 1), ("hk", 0), ("hg", 0), ("hg", 1))]
-            need += [("wm", l, NJ), ("wp", l, NJ), ("wo", l, NJ, 0), ("wo", l, NJ, 1), ("wd", l, NJ)]
-            ys, xsz = YH * DQ * 2, R * DQ * 2
-            tasks["E", l, k] = (need, pair("ya", (l, k), ys, "y") + pair("yb", (l, k), ys, "y"))
-            tasks["G", l, k] = ([("ya", l, k, h) for h in (0, 1)], pair("yc", (l, k), ys, "y"))
-            tasks["H", l, k] = ([(m, l, k, h) for m in ("yb", "yc") for h in (0, 1)], three("xr", (l, k), xsz, other_axis))
-            tasks["I", l, k] = ([("xr", l, k, d) for d in (1, 2, 3)], three("st", (l, k), R * 512, axis))
-            out = ("xq", (k,)) if l + 1 < LAYERS else ("xg", (l + 1, k))
-            tasks["J", l, k] = ([("st", l, k, d) for d in (1, 2, 3)], three(*out, xsz // 4, other_axis))
-    return tasks
-
-
-def order(report=None):
-    tasks = plan()
-    maker = {m[0]: t for t, (_, sends) in tasks.items() for m in sends}
-    users = {}
-    for t, (needs, _) in tasks.items():
-        for m in needs:
-            if m in maker:
-                users.setdefault(maker[m], set()).add(t)
-    rank = {}
-
-    def rest(task):
-        if task not in rank:
-            rank[task] = time_of(task) + max((rest(u) + 2.0 for u in users.get(task, ())), default=0.0)
-        return rank[task]
-
-    arrive, free = {}, {}
-
-    def transmit(task, now):
-        more = FROM_HBM if task[0] in "WX" else 0.0
-        for m, link, size, hops in tasks[task][1]:
-            done = max(now, free.get(link, 0.0)) + (size * hops / LINK if hops else size / CORE_LINK)
-            arrive[m] = done + (HOP[hops] if hops else CORE_HOP) + more
-            free[link] = done
-
-    now = START
-    fill = [list(tasks_of) for tasks_of in FILL]
-    out = [("X", 0, 0), ("W", 0, 0)]
-    for t in out:
-        transmit(t, now)
-    left = [t for t in tasks if t not in out]
-    while left:
-        ready = []
-        for t in left:
-            needs, sends = tasks[t]
-            at = None
-            if t[0] in "WX":
-                if any(queue and queue[0] == t for queue in fill):
-                    at = max(free.get(m[1], 0.0) for m in sends if m[1] != "c") - SLACK[t[0]]
-                    at = max(at, NOT_BEFORE.get(t, 0.0))
-            elif all(m in arrive for m in needs):
-                at = max(arrive[m] for m in needs)
-                if t[0] in SLACK:
-                    at = max(at, max(free.get(m[1], 0.0) for m in sends) - SLACK[t[0]])
-            if at is not None:
-                ready.append((at, t))
-        at, t = min(ready, key=lambda r: (max(r[0], now), r[1][0] in "WX", r[1][1:3], -rest(r[1])))
-        begin = max(now, at)
-        now = begin + time_of(t)
-        for queue in fill:
-            if queue and queue[0] == t:
-                queue.pop(0)
-        transmit(t, now)
-        left.remove(t)
-        out.append(t)
-        if report is not None:
-            report.append((begin, now, t))
-    return out
 
 
 def kernel(
@@ -338,18 +240,22 @@
             all_sent(wgu.at[l, 0, 0:DB if j < NJ else NJ * UT, :])
 
         if core == 0:
-            for i, (stage, *key) in enumerate([t for t in order() if t[0] in "WV"]):
+            for i, (stage, *key) in enumerate([t for t in ORDER if t[0] in "WV"]):
                 if stage == "W":
                     if i:
                         pl.semaphore_wait(go, 1)
                     stage_w(*key)
                 else:
                     stage_v(*key)
-            arrived(ov, ("dd",))
-            copy = pltpu.make_async_copy(ov, out_hbm, local.at[0])
-            copy.start()
+            copies = []
+            for k in range(NC):
+                rows = pl.ds(k * TC, TC)
+                arrived(ov.at[rows, :], ("dd", k))
+                copies.append(pltpu.make_async_copy(ov.at[rows, :], out_hbm.at[rows, :], local.at[k]))
+                copies[-1].start()
             wait_sent(0)
-            copy.wait()
+            for copy in copies:
+                copy.wait()
             return
 
         def weights_ready(l, j):
@@ -366,16 +272,28 @@
             return y * YB + v * R
 
         in_copies = {}
+        out_copies = []
         y_block = pl.ds(pl.multiple_of(y * YB, YB), YB)
 
         def stage_x(l, k):
+            def half(h):
+                rows = pl.ds(pl.multiple_of(k * TC + y * YB + h * YH, YH), YH)
+                return x_hbm.at[rows, :], xs.at[0, k, pl.ds(pl.multiple_of(y * YB + h * YH, YH), YH), d_cols(x)]
+
+            for h, name in enumerate((("xq", k), ("xg", k))):
+                send(*half(h), name, at_x(xp))
+                send(*half(1 - h), name, at_x(xm))
+            all_sent(ov.at[0:2 * YB, :])
             rows = pl.ds(pl.multiple_of(k * TC + y * YB, YB), YB)
-            dst = xs.at[0, k, y_block, d_cols(x)]
-            for d in (2, 1, 3):
-                send(x_hbm.at[rows, :], dst, ("xg", k), at_x(turn(x, d)))
-            all_sent(ov.at[0:3 * YB, :])
-            in_copies[k] = pltpu.make_async_copy(x_hbm.at[rows, :], dst, local.at[14 + k])
+            in_copies[k] = pltpu.make_async_copy(x_hbm.at[rows, :], xs.at[0, k, y_block, d_cols(x)], local.at[14 + k])
             in_copies[k].start()
+
+        def stage_s(l, k):
+            arrived(ov.at[0:YB, :], ("xq", k))
+            for h, (owner, to) in enumerate(((xm, xp), (xp, xm))):
+                ref = xs.at[0, k, pl.ds(pl.multiple_of(y * YB + h * YH, YH), YH), d_cols(owner)]
+                send(ref, ref, ("xg", k), at_x(to))
+            all_sent(ov.at[0:YB, :])
 
         gain_copies = []
 
@@ -393,7 +311,8 @@
 
         def stage_a(l, k, g):
             first, last = GROUPS[l, k][g]
-            if g == 0:
+            if ("x", l, k) not in seen:
+                seen.add(("x", l, k))
                 arrived(xs.at[l, k, 0:YB, :], ("y1", k))
                 arrived(xs.at[l, k, 0:YB, :], ("y2", k))
             for j in range(first, last):
@@ -402,12 +321,12 @@
                     seen.add((l, j))
 
             def tiles(j, carry):
-                for n in (0, 1):
-                    value = jnp.dot(xs[l, k], wgu[l, 2 * j + n], preferred_element_type=F32).astype(BF)
-                    for o in range(4):
-                        for h in (0, 1):
-                            at = o * ZB + h * ZH
-                            part[l, k, j, o, h, :, n * 256:(n + 1) * 256] = value[at:at + ZH]
+                rhs = jnp.concatenate([wgu[l, 2 * j], wgu[l, 2 * j + 1]], axis=1)
+                value = jnp.dot(xs[l, k], rhs, preferred_element_type=F32).astype(BF)
+                for o in range(4):
+                    for h in (0, 1):
+                        at = o * ZB + h * ZH
+                        part[l, k, j, o, h] = value[at:at + ZH]
                 return carry
 
             lax.fori_loop(first, last, tiles, 0)
@@ -478,14 +397,13 @@
 
             def columns(n, carry):
                 lhs = jnp.concatenate([hid[l, k, t] for t in range(NT)], axis=1)
-                for i in (0, 1):
-                    cols = pl.ds(pl.multiple_of(n * 512 + i * 256, 256), 256)
-                    rhs = wd[l, :, :, :, cols].reshape(NT * UT, 256)
-                    value = jnp.dot(lhs, rhs, preferred_element_type=F32).astype(BF)
-                    for yy in range(4):
-                        for h in (0, 1):
-                            at = yy * YB + h * YH
-                            down[l, k, yy, h, :, cols] = value[at:at + YH]
+                cols = pl.ds(pl.multiple_of(n * 512, 512), 512)
+                rhs = wd[l, :, :, :, cols].reshape(NT * UT, 512)
+                value = jnp.dot(lhs, rhs, preferred_element_type=F32).astype(BF)
+                for yy in range(4):
+                    for h in (0, 1):
+                        at = yy * YB + h * YH
+                        down[l, k, yy, h, :, cols] = value[at:at + YH]
                 return carry
 
             lax.fori_loop(0, DQ // 512, columns, 0)
@@ -567,7 +485,8 @@
 
         def stage_k(l, k):
             p = l + 1
-            arrived(ov.at[0:3 * YB, :] if p < LAYERS else nb.at[1, k, 0:3], ("xg", k))
+            got = (ov.at[0:2 * YB, :], ov.at[0:3 * YB, :], nb.at[1, k, 0:3])[p]
+            arrived(got, ("xg", k))
             if p == 0:
                 in_copies[k].wait()
             for h in (0, 1):
@@ -577,7 +496,7 @@
                 send(ref, ref, (("y0", "y1")[h], k), at_y(ym))
             if p == LAYERS:
                 ref = gathered(p, k, y * YB, YB)
-                send(ref, ref, ("dd",), other)
+                send(ref, ref, ("dd", k), other)
                 all_sent(ov.at[0:6 * YH, :])
             else:
                 all_sent(xs.at[p, k, 0:4 * YH, :])
@@ -593,7 +512,7 @@
                 arrived(halves(2), ("y1", k))
                 for owner in (ym, yp):
                     ref = gathered(p, k, owner * YB, YB)
-                    send(ref, ref, ("dd",), other)
+                    send(ref, ref, ("dd", k), other)
                 all_sent(ov.at[0:6 * YH, :])
             else:
                 all_sent(xs.at[p, k, 0:2 * YH, :])
@@ -602,8 +521,11 @@
             p = l + 1
             arrived(ov.at[0:YB, :], ("y2", k))
             ref = gathered(p, k, yo * YB, YB)
-            send(ref, ref, ("dd",), other)
+            send(ref, ref, ("dd", k), other)
             all_sent(ov.at[0:YB, :])
+            rows = pl.ds(k * TC, TC)
+            out_copies.append(pltpu.make_async_copy(ov.at[rows, :], out_hbm.at[rows, :], local.at[14 + k]))
+            out_copies[-1].start()
 
         def stage_w_both(l, j):
             if l + j == 0:
@@ -615,15 +537,14 @@
 
         stages = dict(
             A=stage_a, B=stage_b, C=stage_c, D=stage_d, E=stage_e, G=stage_g, H=stage_h, I=stage_i, J=stage_j,
-            K=stage_k, L=stage_l, M=stage_m, Q=stage_q, W=stage_w_both, V=stage_v, X=stage_x,
+            K=stage_k, L=stage_l, M=stage_m, Q=stage_q, W=stage_w_both, V=stage_v, X=stage_x, S=stage_s,
         )
-        for stage, *key in order():
+        for stage, *key in ORDER:
             stages[stage](*key)
             wait_sent(WAIT_LATER)
-        copy = pltpu.make_async_copy(ov, out_hbm, local.at[18 + NC])
-        copy.start()
         wait_sent(0)
-        copy.wait()
+        for copy in out_copies:
+            copy.wait()
 
     @pl.when(c == 0)
     def _():

time: 137 us -> 131 us (0.956)
  Pallas kernels: 134 us -> 129 us
    pallas_call x1, Pallas kernels: 134 us -> 129 us  [per_device(): pl.pallas_call(kernel, out_shape=jax.ShapeDtypeStruct((T, DB), BF), in_sp...]
where the time goes in v6:
time: 131 us
  Pallas kernels  129 us (98%)
  local copies, waits for them, and re-layouts  2.06 us (2%)
    pallas_call x1, Pallas kernels, per_device(): pl.pallas_call(kernel, out_shape=jax.ShapeDtypeStruct((T, DB), BF), in_sp...  129 us

profile of v6, /device:TPU:1, one launch (start us, length us, event | category | flops | bytes accessed | tf_op | source)
XLA Modules:
  0.0 130.8 jit_solution(4668946328514926673)
XLA Ops:
  0.0 128.8 %shard_map.64 = bf16[1536,256]{1,0:T(8,128)(2,1)} custom-call(bf16[1536,256]{1,0:T(8,128)(2,1)} %x_hbm.1, bf16[2,256,1408]{2,1,0:T(8,128)(2,1)} %wg_hbm.1, bf16[2,256,1408]{2,1,0:T(8,128)(2,1)} %wu_hbm.1, bf16[2,11,128,256]{3,2,1,0:T(8,128)(2,1)} %bitcast.1, f32[2,256]{1,0:T(2,128)} %gain_hbm.1, f32[2,256]{1,0:T(2,128)} %shift_hbm.1), custom_call_target="tpu_custom_call" | custom-call | tf_op jit(solution)/shard_map/pallas_call | solution.py:563
  128.8 2.1 %copy.8 = bf16[1536,256]{1,0:T(8,128)(2,1)} copy(bf16[1536,256]{1,0:T(8,128)(2,1)} %shard_map.64) | data formatting | bytes 1572864

commit v7 on v6

--- a/solution.py
+++ b/solution.py
@@ -27,7 +27,7 @@
 TILES = FF // 8 // UT
 SHARED = 4 * NJ - TILES
 
-GROUPS = {(l, k): [(0, 1), (1, 2), (2, 3)] if l == 0 else [(0, 1), (1, 3)] for l in range(LAYERS) for k in range(NC)}
+GROUPS = {(l, k): [(0, 1), (1, 2), (2, 3)] for l in range(LAYERS) for k in range(NC)}
 
 SLOTS = {}
 
@@ -51,41 +51,45 @@
 
 SUM_AXIS, UNIT_AXIS = "zx", "xz"
 ORDER = [
-    ("X", 0, 0), ("W", 0, 0), ("W", 1, 0), ("W", 1, 1), ("S", 0, 0), ("X", 0, 2), ("X", 0, 3), ("X", 0, 4),
-    ("W", 1, 2), ("X", 0, 1), ("V", 0, 0), ("X", 0, 5), ("K", -1, 0), ("S", 0, 2), ("S", 0, 3), ("W", 0, 1),
-    ("L", -1, 0), ("K", -1, 2), ("S", 0, 4), ("K", -1, 3), ("A", 0, 0, 0), ("V", 1, 0), ("L", -1, 2), ("V", 0, 1),
-    ("W", 0, 2), ("L", -1, 3), ("K", -1, 4), ("B", 0, 0, 0), ("S", 0, 1), ("A", 0, 2, 0), ("A", 0, 2, 1),
-    ("A", 0, 0, 1), ("L", -1, 4), ("C", 0, 0, 0), ("A", 0, 3, 0), ("A", 0, 3, 1), ("V", 0, 2), ("B", 0, 2, 0),
-    ("B", 0, 0, 1), ("B", 0, 2, 1), ("A", 0, 4, 1), ("S", 0, 5), ("W", 0, 3), ("D", 0, 0, 0), ("K", -1, 1),
-    ("A", 0, 4, 0), ("A", 0, 0, 2), ("A", 0, 2, 2), ("C", 0, 2, 1), ("C", 0, 0, 1), ("B", 0, 0, 2), ("B", 0, 3, 0),
-    ("L", -1, 1), ("B", 0, 2, 2), ("C", 0, 2, 0), ("A", 0, 3, 2), ("V", 0, 3), ("D", 0, 2, 1), ("C", 0, 0, 2),
-    ("K", -1, 5), ("D", 0, 0, 1), ("B", 0, 3, 1), ("C", 0, 2, 2), ("A", 0, 4, 2), ("D", 0, 2, 0), ("D", 0, 0, 2),
-    ("B", 0, 3, 2), ("A", 0, 1, 0), ("L", -1, 5), ("D", 0, 2, 2), ("C", 0, 3, 1), ("C", 0, 3, 0), ("A", 0, 1, 2),
-    ("B", 0, 4, 2), ("B", 0, 4, 0), ("E", 0, 0), ("C", 0, 3, 2), ("B", 0, 1, 0), ("E", 0, 2), ("D", 0, 3, 0),
-    ("B", 0, 4, 1), ("B", 0, 1, 2), ("D", 0, 3, 1), ("A", 0, 1, 1), ("G", 0, 0), ("C", 0, 4, 2), ("D", 0, 3, 2),
-    ("A", 0, 5, 2), ("C", 0, 4, 0), ("G", 0, 2), ("A", 0, 5, 0), ("C", 0, 4, 1), ("B", 0, 1, 1), ("C", 0, 1, 2),
-    ("C", 0, 1, 0), ("H", 0, 0), ("A", 0, 5, 1), ("E", 0, 3), ("B", 0, 5, 0), ("H", 0, 2), ("D", 0, 4, 1),
-    ("D", 0, 4, 0), ("C", 0, 1, 1), ("D", 0, 4, 2), ("B", 0, 5, 2), ("I", 0, 0), ("B", 0, 5, 1), ("D", 0, 1, 0),
-    ("D", 0, 1, 2), ("G", 0, 3), ("D", 0, 1, 1), ("C", 0, 5, 0), ("E", 0, 4), ("C", 0, 5, 2), ("C", 0, 5, 1),
-    ("I", 0, 2), ("J", 0, 0), ("E", 0, 1), ("H", 0, 3), ("D", 0, 5, 0), ("D", 0, 5, 2), ("D", 0, 5, 1), ("G", 0, 4),
-    ("Q", 0, 0), ("J", 0, 2), ("G", 0, 1), ("E", 0, 5), ("I", 0, 3), ("H", 0, 4), ("Q", 0, 2), ("K", 0, 0),
-    ("H", 0, 1), ("V", 1, 2), ("G", 0, 5), ("J", 0, 3), ("I", 0, 4), ("V", 1, 1), ("L", 0, 0), ("K", 0, 2),
-    ("I", 0, 1), ("H", 0, 5), ("Q", 0, 3), ("J", 0, 4), ("A", 1, 0, 0), ("L", 0, 2), ("A", 1, 0, 1), ("K", 0, 3),
-    ("I", 0, 5), ("J", 0, 1), ("B", 1, 0, 0), ("Q", 0, 4), ("A", 1, 2, 0), ("B", 1, 0, 1), ("A", 1, 2, 1),
-    ("L", 0, 3), ("J", 0, 5), ("Q", 0, 1), ("C", 1, 0, 0), ("B", 1, 2, 0), ("K", 0, 4), ("C", 1, 0, 1),
-    ("B", 1, 2, 1), ("A", 1, 3, 1), ("Q", 0, 5), ("W", 1, 3), ("D", 1, 0, 1), ("L", 0, 4), ("K", 0, 1),
-    ("A", 1, 3, 0), ("C", 1, 2, 1), ("B", 1, 3, 1), ("C", 1, 2, 0), ("A", 1, 4, 0), ("B", 1, 3, 0), ("K", 0, 5),
-    ("A", 1, 4, 1), ("L", 0, 1), ("B", 1, 4, 0), ("D", 1, 2, 0), ("C", 1, 3, 1), ("D", 1, 2, 1), ("V", 1, 3),
-    ("C", 1, 3, 0), ("L", 0, 5), ("D", 1, 0, 0), ("B", 1, 4, 1), ("A", 1, 1, 0), ("C", 1, 4, 0), ("A", 1, 1, 1),
-    ("A", 1, 5, 0), ("D", 1, 3, 1), ("D", 1, 3, 0), ("A", 1, 5, 1), ("C", 1, 4, 1), ("B", 1, 1, 0), ("E", 1, 2),
-    ("E", 1, 0), ("B", 1, 1, 1), ("E", 1, 3), ("D", 1, 4, 0), ("B", 1, 5, 1), ("D", 1, 4, 1), ("G", 1, 2),
-    ("C", 1, 1, 0), ("G", 1, 0), ("B", 1, 5, 0), ("C", 1, 1, 1), ("G", 1, 3), ("C", 1, 5, 1), ("E", 1, 4),
-    ("C", 1, 5, 0), ("D", 1, 1, 0), ("H", 1, 2), ("D", 1, 1, 1), ("H", 1, 3), ("H", 1, 0), ("D", 1, 5, 1),
-    ("D", 1, 5, 0), ("G", 1, 4), ("E", 1, 1), ("I", 1, 2), ("E", 1, 5), ("I", 1, 3), ("H", 1, 4), ("I", 1, 0),
-    ("G", 1, 1), ("J", 1, 2), ("G", 1, 5), ("J", 1, 3), ("J", 1, 0), ("H", 1, 1), ("I", 1, 4), ("K", 1, 2),
-    ("H", 1, 5), ("K", 1, 3), ("J", 1, 4), ("I", 1, 1), ("L", 1, 2), ("K", 1, 0), ("L", 1, 3), ("I", 1, 5),
-    ("L", 1, 0), ("M", 1, 3), ("M", 1, 2), ("J", 1, 1), ("K", 1, 4), ("J", 1, 5), ("M", 1, 0), ("L", 1, 4),
-    ("K", 1, 1), ("K", 1, 5), ("L", 1, 1), ("M", 1, 4), ("L", 1, 5), ("M", 1, 1), ("M", 1, 5),
+    ("X", 0, 0), ("W", 0, 0), ("W", 1, 0), ("X", 0, 3), ("W", 1, 2), ("X", 0, 5), ("S", 0, 0), ("V", 0, 0),
+    ("S", 0, 3), ("X", 0, 2), ("S", 0, 5), ("K", -1, 0), ("W", 0, 2), ("K", -1, 3), ("W", 1, 1), ("K", -1, 5),
+    ("S", 0, 2), ("X", 0, 4), ("L", -1, 0), ("V", 0, 2), ("V", 1, 2), ("W", 0, 1), ("L", -1, 3), ("L", -1, 5),
+    ("K", -1, 2), ("A", 0, 0, 0), ("A", 0, 3, 0), ("A", 0, 3, 2), ("A", 0, 5, 0), ("L", -1, 2), ("B", 0, 0, 0),
+    ("V", 0, 1), ("A", 0, 5, 2), ("X", 0, 1), ("B", 0, 3, 0), ("S", 0, 4), ("A", 0, 0, 2), ("B", 0, 3, 2),
+    ("W", 0, 3), ("B", 0, 5, 0), ("A", 0, 2, 0), ("B", 0, 5, 2), ("A", 0, 3, 1), ("K", -1, 4), ("A", 0, 5, 1),
+    ("C", 0, 5, 0), ("C", 0, 3, 2), ("A", 0, 0, 1), ("B", 0, 3, 1), ("L", -1, 4), ("S", 0, 1), ("C", 0, 3, 0),
+    ("B", 0, 5, 1), ("C", 0, 5, 2), ("D", 0, 3, 2), ("B", 0, 2, 0), ("A", 0, 2, 2), ("C", 0, 3, 1), ("B", 0, 0, 1),
+    ("C", 0, 5, 1), ("V", 0, 3), ("D", 0, 3, 0), ("B", 0, 0, 2), ("A", 0, 2, 1), ("D", 0, 5, 0), ("D", 0, 5, 2),
+    ("K", -1, 1), ("D", 0, 3, 1), ("C", 0, 0, 0), ("D", 0, 5, 1), ("B", 0, 2, 2), ("C", 0, 0, 1), ("A", 0, 4, 1),
+    ("C", 0, 0, 2), ("C", 0, 2, 0), ("B", 0, 2, 1), ("A", 0, 4, 0), ("L", -1, 1), ("E", 0, 3), ("A", 0, 4, 2),
+    ("D", 0, 0, 1), ("C", 0, 2, 2), ("E", 0, 5), ("D", 0, 0, 2), ("D", 0, 0, 0), ("A", 0, 1, 1), ("G", 0, 3),
+    ("B", 0, 4, 1), ("C", 0, 2, 1), ("A", 0, 1, 2), ("A", 0, 1, 0), ("B", 0, 4, 0), ("G", 0, 5), ("B", 0, 4, 2),
+    ("E", 0, 0), ("D", 0, 2, 2), ("B", 0, 1, 1), ("H", 0, 3), ("B", 0, 1, 2), ("D", 0, 2, 0), ("D", 0, 2, 1),
+    ("B", 0, 1, 0), ("H", 0, 5), ("C", 0, 4, 1), ("C", 0, 4, 0), ("C", 0, 4, 2), ("G", 0, 0), ("C", 0, 1, 1),
+    ("C", 0, 1, 2), ("I", 0, 3), ("E", 0, 2), ("D", 0, 4, 1), ("C", 0, 1, 0), ("D", 0, 4, 0), ("D", 0, 4, 2),
+    ("I", 0, 5), ("D", 0, 1, 2), ("D", 0, 1, 1), ("J", 0, 3), ("D", 0, 1, 0), ("H", 0, 0), ("G", 0, 2), ("V", 1, 0),
+    ("E", 0, 4), ("J", 0, 5), ("Q", 0, 3), ("E", 0, 1), ("I", 0, 0), ("Q", 0, 5), ("G", 0, 4), ("V", 1, 1),
+    ("H", 0, 2), ("K", 0, 3), ("J", 0, 0), ("G", 0, 1), ("K", 0, 5), ("H", 0, 4), ("I", 0, 2), ("L", 0, 3),
+    ("Q", 0, 0), ("H", 0, 1), ("L", 0, 5), ("I", 0, 4), ("J", 0, 2), ("A", 1, 3, 1), ("K", 0, 0), ("A", 1, 3, 2),
+    ("I", 0, 1), ("A", 1, 3, 0), ("Q", 0, 2), ("A", 1, 5, 1), ("J", 0, 4), ("A", 1, 5, 2), ("L", 0, 0),
+    ("B", 1, 3, 1), ("J", 0, 1), ("B", 1, 3, 0), ("A", 1, 5, 0), ("B", 1, 5, 1), ("K", 0, 2), ("Q", 0, 4),
+    ("B", 1, 5, 2), ("B", 1, 3, 2), ("A", 1, 0, 0), ("A", 1, 0, 2), ("Q", 0, 1), ("L", 0, 2), ("C", 1, 3, 0),
+    ("A", 1, 0, 1), ("W", 1, 3), ("C", 1, 5, 2), ("B", 1, 0, 0), ("K", 0, 4), ("C", 1, 3, 2), ("B", 1, 0, 2),
+    ("C", 1, 5, 1), ("B", 1, 5, 0), ("K", 0, 1), ("C", 1, 3, 1), ("A", 1, 2, 0), ("B", 1, 0, 1), ("A", 1, 2, 1),
+    ("D", 1, 5, 2), ("L", 0, 4), ("C", 1, 5, 0), ("D", 1, 3, 0), ("C", 1, 0, 2), ("D", 1, 3, 2), ("A", 1, 2, 2),
+    ("L", 0, 1), ("V", 1, 3), ("D", 1, 3, 1), ("D", 1, 5, 1), ("C", 1, 0, 1), ("C", 1, 0, 0), ("B", 1, 2, 0),
+    ("A", 1, 4, 0), ("A", 1, 4, 1), ("B", 1, 2, 1), ("D", 1, 5, 0), ("D", 1, 0, 2), ("A", 1, 4, 2), ("B", 1, 2, 2),
+    ("D", 1, 0, 1), ("A", 1, 1, 1), ("D", 1, 0, 0), ("A", 1, 1, 0), ("B", 1, 4, 0), ("E", 1, 3), ("B", 1, 4, 1),
+    ("A", 1, 1, 2), ("C", 1, 2, 1), ("E", 1, 5), ("B", 1, 4, 2), ("B", 1, 1, 1), ("C", 1, 2, 0), ("C", 1, 2, 2),
+    ("G", 1, 3), ("E", 1, 0), ("B", 1, 1, 0), ("B", 1, 1, 2), ("G", 1, 5), ("C", 1, 4, 0), ("C", 1, 4, 1),
+    ("C", 1, 4, 2), ("H", 1, 3), ("D", 1, 2, 0), ("D", 1, 2, 1), ("G", 1, 0), ("D", 1, 2, 2), ("C", 1, 1, 1),
+    ("C", 1, 1, 0), ("C", 1, 1, 2), ("D", 1, 4, 1), ("D", 1, 4, 0), ("D", 1, 4, 2), ("H", 1, 5), ("E", 1, 2),
+    ("D", 1, 1, 2), ("D", 1, 1, 0), ("D", 1, 1, 1), ("H", 1, 0), ("I", 1, 3), ("E", 1, 4), ("I", 1, 5), ("G", 1, 2),
+    ("E", 1, 1), ("I", 1, 0), ("J", 1, 3), ("J", 1, 5), ("G", 1, 4), ("H", 1, 2), ("G", 1, 1), ("K", 1, 3),
+    ("J", 1, 0), ("H", 1, 4), ("K", 1, 5), ("I", 1, 2), ("H", 1, 1), ("K", 1, 0), ("I", 1, 4), ("L", 1, 3),
+    ("L", 1, 5), ("J", 1, 2), ("L", 1, 0), ("I", 1, 1), ("J", 1, 4), ("K", 1, 2), ("M", 1, 5), ("M", 1, 3),
+    ("M", 1, 0), ("J", 1, 1), ("K", 1, 4), ("L", 1, 2), ("K", 1, 1), ("L", 1, 4), ("M", 1, 2), ("L", 1, 1),
+    ("M", 1, 4), ("M", 1, 1),
 ]
 
 

time: 131 us -> 128 us (0.977)
  Pallas kernels: 129 us -> 126 us
    pallas_call x1, Pallas kernels: 129 us -> 126 us  [per_device(): pl.pallas_call(kernel, out_shape=jax.ShapeDtypeStruct((T, DB), BF), in_sp...]
where the time goes in v7:
time: 128 us
  Pallas kernels  126 us (98%)
  local copies, waits for them, and re-layouts  2.06 us (2%)
    pallas_call x1, Pallas kernels, per_device(): pl.pallas_call(kernel, out_shape=jax.ShapeDtypeStruct((T, DB), BF), in_sp...  126 us

profile of v7, /device:TPU:1, one launch (start us, length us, event | category | flops | bytes accessed | tf_op | source)
XLA Modules:
  0.0 127.9 jit_solution(11823679683485711529)
XLA Ops:
  0.0 125.9 %shard_map.64 = bf16[1536,256]{1,0:T(8,128)(2,1)} custom-call(bf16[1536,256]{1,0:T(8,128)(2,1)} %x_hbm.1, bf16[2,256,1408]{2,1,0:T(8,128)(2,1)} %wg_hbm.1, bf16[2,256,1408]{2,1,0:T(8,128)(2,1)} %wu_hbm.1, bf16[2,11,128,256]{3,2,1,0:T(8,128)(2,1)} %bitcast.1, f32[2,256]{1,0:T(2,128)} %gain_hbm.1, f32[2,256]{1,0:T(2,128)} %shift_hbm.1), custom_call_target="tpu_custom_call" | custom-call | tf_op jit(solution)/shard_map/pallas_call | solution.py:567
  125.9 2.1 %copy.8 = bf16[1536,256]{1,0:T(8,128)(2,1)} copy(bf16[1536,256]{1,0:T(8,128)(2,1)} %shard_map.64) | data formatting | bytes 1572864

commit v8 on v6

--- a/solution.py
+++ b/solution.py
@@ -50,42 +50,42 @@
 WAIT_LATER = 30
 
 SUM_AXIS, UNIT_AXIS = "zx", "xz"
+DIRECT = (4, 5)
 ORDER = [
-    ("X", 0, 0), ("W", 0, 0), ("W", 1, 0), ("W", 1, 1), ("S", 0, 0), ("X", 0, 2), ("X", 0, 3), ("X", 0, 4),
-    ("W", 1, 2), ("X", 0, 1), ("V", 0, 0), ("X", 0, 5), ("K", -1, 0), ("S", 0, 2), ("S", 0, 3), ("W", 0, 1),
-    ("L", -1, 0), ("K", -1, 2), ("S", 0, 4), ("K", -1, 3), ("A", 0, 0, 0), ("V", 1, 0), ("L", -1, 2), ("V", 0, 1),
-    ("W", 0, 2), ("L", -1, 3), ("K", -1, 4), ("B", 0, 0, 0), ("S", 0, 1), ("A", 0, 2, 0), ("A", 0, 2, 1),
-    ("A", 0, 0, 1), ("L", -1, 4), ("C", 0, 0, 0), ("A", 0, 3, 0), ("A", 0, 3, 1), ("V", 0, 2), ("B", 0, 2, 0),
-    ("B", 0, 0, 1), ("B", 0, 2, 1), ("A", 0, 4, 1), ("S", 0, 5), ("W", 0, 3), ("D", 0, 0, 0), ("K", -1, 1),
-    ("A", 0, 4, 0), ("A", 0, 0, 2), ("A", 0, 2, 2), ("C", 0, 2, 1), ("C", 0, 0, 1), ("B", 0, 0, 2), ("B", 0, 3, 0),
-    ("L", -1, 1), ("B", 0, 2, 2), ("C", 0, 2, 0), ("A", 0, 3, 2), ("V", 0, 3), ("D", 0, 2, 1), ("C", 0, 0, 2),
-    ("K", -1, 5), ("D", 0, 0, 1), ("B", 0, 3, 1), ("C", 0, 2, 2), ("A", 0, 4, 2), ("D", 0, 2, 0), ("D", 0, 0, 2),
-    ("B", 0, 3, 2), ("A", 0, 1, 0), ("L", -1, 5), ("D", 0, 2, 2), ("C", 0, 3, 1), ("C", 0, 3, 0), ("A", 0, 1, 2),
-    ("B", 0, 4, 2), ("B", 0, 4, 0), ("E", 0, 0), ("C", 0, 3, 2), ("B", 0, 1, 0), ("E", 0, 2), ("D", 0, 3, 0),
-    ("B", 0, 4, 1), ("B", 0, 1, 2), ("D", 0, 3, 1), ("A", 0, 1, 1), ("G", 0, 0), ("C", 0, 4, 2), ("D", 0, 3, 2),
-    ("A", 0, 5, 2), ("C", 0, 4, 0), ("G", 0, 2), ("A", 0, 5, 0), ("C", 0, 4, 1), ("B", 0, 1, 1), ("C", 0, 1, 2),
-    ("C", 0, 1, 0), ("H", 0, 0), ("A", 0, 5, 1), ("E", 0, 3), ("B", 0, 5, 0), ("H", 0, 2), ("D", 0, 4, 1),
-    ("D", 0, 4, 0), ("C", 0, 1, 1), ("D", 0, 4, 2), ("B", 0, 5, 2), ("I", 0, 0), ("B", 0, 5, 1), ("D", 0, 1, 0),
-    ("D", 0, 1, 2), ("G", 0, 3), ("D", 0, 1, 1), ("C", 0, 5, 0), ("E", 0, 4), ("C", 0, 5, 2), ("C", 0, 5, 1),
-    ("I", 0, 2), ("J", 0, 0), ("E", 0, 1), ("H", 0, 3), ("D", 0, 5, 0), ("D", 0, 5, 2), ("D", 0, 5, 1), ("G", 0, 4),
-    ("Q", 0, 0), ("J", 0, 2), ("G", 0, 1), ("E", 0, 5), ("I", 0, 3), ("H", 0, 4), ("Q", 0, 2), ("K", 0, 0),
-    ("H", 0, 1), ("V", 1, 2), ("G", 0, 5), ("J", 0, 3), ("I", 0, 4), ("V", 1, 1), ("L", 0, 0), ("K", 0, 2),
-    ("I", 0, 1), ("H", 0, 5), ("Q", 0, 3), ("J", 0, 4), ("A", 1, 0, 0), ("L", 0, 2), ("A", 1, 0, 1), ("K", 0, 3),
-    ("I", 0, 5), ("J", 0, 1), ("B", 1, 0, 0), ("Q", 0, 4), ("A", 1, 2, 0), ("B", 1, 0, 1), ("A", 1, 2, 1),
-    ("L", 0, 3), ("J", 0, 5), ("Q", 0, 1), ("C", 1, 0, 0), ("B", 1, 2, 0), ("K", 0, 4), ("C", 1, 0, 1),
-    ("B", 1, 2, 1), ("A", 1, 3, 1), ("Q", 0, 5), ("W", 1, 3), ("D", 1, 0, 1), ("L", 0, 4), ("K", 0, 1),
-    ("A", 1, 3, 0), ("C", 1, 2, 1), ("B", 1, 3, 1), ("C", 1, 2, 0), ("A", 1, 4, 0), ("B", 1, 3, 0), ("K", 0, 5),
-    ("A", 1, 4, 1), ("L", 0, 1), ("B", 1, 4, 0), ("D", 1, 2, 0), ("C", 1, 3, 1), ("D", 1, 2, 1), ("V", 1, 3),
-    ("C", 1, 3, 0), ("L", 0, 5), ("D", 1, 0, 0), ("B", 1, 4, 1), ("A", 1, 1, 0), ("C", 1, 4, 0), ("A", 1, 1, 1),
-    ("A", 1, 5, 0), ("D", 1, 3, 1), ("D", 1, 3, 0), ("A", 1, 5, 1), ("C", 1, 4, 1), ("B", 1, 1, 0), ("E", 1, 2),
-    ("E", 1, 0), ("B", 1, 1, 1), ("E", 1, 3), ("D", 1, 4, 0), ("B", 1, 5, 1), ("D", 1, 4, 1), ("G", 1, 2),
-    ("C", 1, 1, 0), ("G", 1, 0), ("B", 1, 5, 0), ("C", 1, 1, 1), ("G", 1, 3), ("C", 1, 5, 1), ("E", 1, 4),
-    ("C", 1, 5, 0), ("D", 1, 1, 0), ("H", 1, 2), ("D", 1, 1, 1), ("H", 1, 3), ("H", 1, 0), ("D", 1, 5, 1),
-    ("D", 1, 5, 0), ("G", 1, 4), ("E", 1, 1), ("I", 1, 2), ("E", 1, 5), ("I", 1, 3), ("H", 1, 4), ("I", 1, 0),
-    ("G", 1, 1), ("J", 1, 2), ("G", 1, 5), ("J", 1, 3), ("J", 1, 0), ("H", 1, 1), ("I", 1, 4), ("K", 1, 2),
-    ("H", 1, 5), ("K", 1, 3), ("J", 1, 4), ("I", 1, 1), ("L", 1, 2), ("K", 1, 0), ("L", 1, 3), ("I", 1, 5),
-    ("L", 1, 0), ("M", 1, 3), ("M", 1, 2), ("J", 1, 1), ("K", 1, 4), ("J", 1, 5), ("M", 1, 0), ("L", 1, 4),
-    ("K", 1, 1), ("K", 1, 5), ("L", 1, 1), ("M", 1, 4), ("L", 1, 5), ("M", 1, 1), ("M", 1, 5),
+    ("X", 0, 0), ("W", 0, 0), ("W", 1, 2), ("W", 1, 1), ("X", 0, 3), ("S", 0, 0), ("X", 0, 1), ("V", 0, 0),
+    ("S", 0, 3), ("X", 0, 2), ("S", 0, 1), ("K", -1, 0), ("W", 0, 1), ("K", -1, 3), ("S", 0, 2), ("W", 1, 0),
+    ("K", -1, 1), ("V", 0, 1), ("X", 0, 5), ("L", -1, 0), ("L", -1, 3), ("L", -1, 1), ("W", 0, 2), ("V", 1, 0),
+    ("K", -1, 2), ("A", 0, 0, 0), ("A", 0, 3, 0), ("A", 0, 3, 1), ("A", 0, 0, 1), ("L", -1, 2), ("V", 0, 2),
+    ("S", 0, 5), ("A", 0, 1, 1), ("B", 0, 3, 0), ("B", 0, 0, 0), ("A", 0, 1, 0), ("X", 0, 4), ("B", 0, 3, 1),
+    ("W", 0, 3), ("A", 0, 2, 1), ("A", 0, 2, 0), ("A", 0, 2, 2), ("K", -1, 5), ("A", 0, 3, 2), ("B", 0, 2, 1),
+    ("S", 0, 4), ("A", 0, 1, 2), ("B", 0, 2, 0), ("B", 0, 2, 2), ("C", 0, 3, 1), ("B", 0, 3, 2), ("C", 0, 3, 0),
+    ("L", -1, 5), ("B", 0, 1, 1), ("C", 0, 2, 1), ("V", 0, 3), ("B", 0, 1, 2), ("C", 0, 2, 0), ("C", 0, 2, 2),
+    ("B", 0, 1, 0), ("C", 0, 3, 2), ("A", 0, 0, 2), ("C", 0, 1, 1), ("D", 0, 2, 1), ("K", -1, 4), ("D", 0, 2, 0),
+    ("D", 0, 2, 2), ("C", 0, 1, 2), ("D", 0, 3, 0), ("D", 0, 3, 1), ("C", 0, 1, 0), ("D", 0, 3, 2), ("A", 0, 5, 1),
+    ("B", 0, 0, 1), ("B", 0, 0, 2), ("A", 0, 5, 0), ("L", -1, 4), ("D", 0, 1, 1), ("E", 0, 2), ("A", 0, 5, 2),
+    ("D", 0, 1, 2), ("E", 0, 3), ("C", 0, 0, 0), ("D", 0, 1, 0), ("C", 0, 0, 1), ("A", 0, 4, 2), ("A", 0, 4, 1),
+    ("G", 0, 2), ("B", 0, 5, 1), ("C", 0, 0, 2), ("A", 0, 4, 0), ("B", 0, 5, 2), ("G", 0, 3), ("E", 0, 1),
+    ("B", 0, 5, 0), ("B", 0, 4, 2), ("B", 0, 4, 1), ("H", 0, 2), ("D", 0, 0, 2), ("D", 0, 0, 0), ("D", 0, 0, 1),
+    ("B", 0, 4, 0), ("C", 0, 5, 1), ("C", 0, 5, 2), ("H", 0, 3), ("G", 0, 1), ("C", 0, 5, 0), ("C", 0, 4, 2),
+    ("C", 0, 4, 1), ("I", 0, 2), ("E", 0, 0), ("C", 0, 4, 0), ("D", 0, 5, 2), ("D", 0, 5, 1), ("D", 0, 5, 0),
+    ("I", 0, 3), ("D", 0, 4, 1), ("J", 0, 2), ("H", 0, 1), ("D", 0, 4, 2), ("D", 0, 4, 0), ("G", 0, 0), ("V", 1, 2),
+    ("E", 0, 5), ("J", 0, 3), ("Q", 0, 2), ("E", 0, 4), ("I", 0, 1), ("Q", 0, 3), ("H", 0, 0), ("G", 0, 5),
+    ("K", 0, 2), ("J", 0, 1), ("V", 1, 1), ("G", 0, 4), ("K", 0, 3), ("H", 0, 5), ("I", 0, 0), ("Q", 0, 1),
+    ("L", 0, 2), ("H", 0, 4), ("L", 0, 3), ("J", 0, 0), ("I", 0, 5), ("K", 0, 1), ("A", 1, 2, 0), ("A", 1, 2, 1),
+    ("I", 0, 4), ("Q", 0, 0), ("J", 0, 5), ("A", 1, 3, 1), ("L", 0, 1), ("J", 0, 4), ("B", 1, 2, 0), ("A", 1, 3, 0),
+    ("B", 1, 2, 1), ("K", 0, 0), ("B", 1, 3, 1), ("Q", 0, 5), ("A", 1, 1, 1), ("Q", 0, 4), ("C", 1, 2, 0),
+    ("L", 0, 0), ("W", 1, 3), ("A", 1, 1, 0), ("C", 1, 3, 1), ("B", 1, 3, 0), ("K", 0, 4), ("C", 1, 2, 1),
+    ("B", 1, 1, 1), ("A", 1, 0, 1), ("D", 1, 3, 1), ("L", 0, 4), ("V", 1, 3), ("B", 1, 1, 0), ("C", 1, 3, 0),
+    ("K", 0, 5), ("D", 1, 2, 0), ("A", 1, 0, 0), ("B", 1, 0, 1), ("D", 1, 2, 1), ("C", 1, 1, 0), ("C", 1, 1, 1),
+    ("L", 0, 5), ("D", 1, 3, 0), ("A", 1, 4, 0), ("B", 1, 0, 0), ("A", 1, 4, 1), ("E", 1, 2), ("C", 1, 0, 1),
+    ("E", 1, 3), ("D", 1, 1, 1), ("D", 1, 1, 0), ("B", 1, 4, 0), ("C", 1, 0, 0), ("A", 1, 5, 1), ("G", 1, 2),
+    ("A", 1, 5, 0), ("G", 1, 3), ("B", 1, 4, 1), ("E", 1, 1), ("D", 1, 0, 0), ("B", 1, 5, 1), ("D", 1, 0, 1),
+    ("H", 1, 2), ("B", 1, 5, 0), ("C", 1, 4, 0), ("H", 1, 3), ("C", 1, 4, 1), ("C", 1, 5, 1), ("G", 1, 1),
+    ("E", 1, 0), ("C", 1, 5, 0), ("D", 1, 4, 0), ("D", 1, 4, 1), ("I", 1, 3), ("I", 1, 2), ("D", 1, 5, 1),
+    ("D", 1, 5, 0), ("H", 1, 1), ("G", 1, 0), ("E", 1, 4), ("J", 1, 3), ("J", 1, 2), ("E", 1, 5), ("H", 1, 0),
+    ("I", 1, 1), ("G", 1, 4), ("K", 1, 3), ("K", 1, 2), ("J", 1, 1), ("G", 1, 5), ("I", 1, 0), ("H", 1, 4),
+    ("L", 1, 3), ("L", 1, 2), ("K", 1, 1), ("J", 1, 0), ("H", 1, 5), ("I", 1, 4), ("L", 1, 1), ("M", 1, 3),
+    ("M", 1, 2), ("K", 1, 0), ("I", 1, 5), ("J", 1, 4), ("M", 1, 1), ("L", 1, 0), ("J", 1, 5), ("M", 1, 0),
 ]
 
 
@@ -471,6 +471,16 @@
             else:
                 dst = gathered(LAYERS, k, part_rows(me), R)
             dst[...] = nb[l, k, me]
+            if l + 1 == LAYERS and k in DIRECT:
+                for dz in (2, 1, 3, 0):
+                    for dy in (2, 1, 3, 0):
+                        for core in (1, 0):
+                            if dz + dy == 0 and core == 1:
+                                continue
+                            at = (turn(z, dz) * 4 + x, turn(y, dy) * 2 + core)
+                            send(nb.at[1, k, turn(z, dz)], dst, ("xg", k) if core else ("dd", k), at)
+                all_sent(ov.at[0:31 * R, :])
+                return
             for d in (2, 1, 3):
                 name = ("xq", k) if l + 1 < LAYERS else ("xg", k)
                 send(nb.at[l, k, turn(me, d)], dst, name, at_unit(l, turn(me, d)))
@@ -542,6 +552,11 @@
         for stage, *key in ORDER:
             stages[stage](*key)
             wait_sent(WAIT_LATER)
+        for k in DIRECT:
+            rows = pl.ds(k * TC, TC)
+            arrived(ov.at[0:15 * R, :], ("xg", k))
+            out_copies.append(pltpu.make_async_copy(ov.at[rows, :], out_hbm.at[rows, :], local.at[14 + k]))
+            out_copies[-1].start()
         wait_sent(0)
         for copy in out_copies:
             copy.wait()

time: 131 us -> 124 us (0.947)
  Pallas kernels: 129 us -> 122 us
    pallas_call x1, Pallas kernels: 129 us -> 122 us  [per_device(): pl.pallas_call(kernel, out_shape=jax.ShapeDtypeStruct((T, DB), BF), in_sp...]
where the time goes in v8:
time: 124 us
  Pallas kernels  122 us (98%)
  local copies, waits for them, and re-layouts  2.06 us (2%)
    pallas_call x1, Pallas kernels, per_device(): pl.pallas_call(kernel, out_shape=jax.ShapeDtypeStruct((T, DB), BF), in_sp...  122 us

profile of v8, /device:TPU:1, one launch (start us, length us, event | category | flops | bytes accessed | tf_op | source)
XLA Modules:
  0.0 124.1 jit_solution(995962118325255924)
XLA Ops:
  0.0 122.0 %shard_map.64 = bf16[1536,256]{1,0:T(8,128)(2,1)} custom-call(bf16[1536,256]{1,0:T(8,128)(2,1)} %x_hbm.1, bf16[2,256,1408]{2,1,0:T(8,128)(2,1)} %wg_hbm.1, bf16[2,256,1408]{2,1,0:T(8,128)(2,1)} %wu_hbm.1, bf16[2,11,128,256]{3,2,1,0:T(8,128)(2,1)} %bitcast.1, f32[2,256]{1,0:T(2,128)} %gain_hbm.1, f32[2,256]{1,0:T(2,128)} %shift_hbm.1), custom_call_target="tpu_custom_call" | custom-call | tf_op jit(solution)/shard_map/pallas_call | solution.py:578
  122.1 2.1 %copy.8 = bf16[1536,256]{1,0:T(8,128)(2,1)} copy(bf16[1536,256]{1,0:T(8,128)(2,1)} %shard_map.64) | data formatting | bytes 1572864

commit v9 on v8

--- a/solution.py
+++ b/solution.py
@@ -52,40 +52,41 @@
 SUM_AXIS, UNIT_AXIS = "zx", "xz"
 DIRECT = (4, 5)
 ORDER = [
-    ("X", 0, 0), ("W", 0, 0), ("W", 1, 2), ("W", 1, 1), ("X", 0, 3), ("S", 0, 0), ("X", 0, 1), ("V", 0, 0),
-    ("S", 0, 3), ("X", 0, 2), ("S", 0, 1), ("K", -1, 0), ("W", 0, 1), ("K", -1, 3), ("S", 0, 2), ("W", 1, 0),
-    ("K", -1, 1), ("V", 0, 1), ("X", 0, 5), ("L", -1, 0), ("L", -1, 3), ("L", -1, 1), ("W", 0, 2), ("V", 1, 0),
-    ("K", -1, 2), ("A", 0, 0, 0), ("A", 0, 3, 0), ("A", 0, 3, 1), ("A", 0, 0, 1), ("L", -1, 2), ("V", 0, 2),
-    ("S", 0, 5), ("A", 0, 1, 1), ("B", 0, 3, 0), ("B", 0, 0, 0), ("A", 0, 1, 0), ("X", 0, 4), ("B", 0, 3, 1),
-    ("W", 0, 3), ("A", 0, 2, 1), ("A", 0, 2, 0), ("A", 0, 2, 2), ("K", -1, 5), ("A", 0, 3, 2), ("B", 0, 2, 1),
-    ("S", 0, 4), ("A", 0, 1, 2), ("B", 0, 2, 0), ("B", 0, 2, 2), ("C", 0, 3, 1), ("B", 0, 3, 2), ("C", 0, 3, 0),
-    ("L", -1, 5), ("B", 0, 1, 1), ("C", 0, 2, 1), ("V", 0, 3), ("B", 0, 1, 2), ("C", 0, 2, 0), ("C", 0, 2, 2),
-    ("B", 0, 1, 0), ("C", 0, 3, 2), ("A", 0, 0, 2), ("C", 0, 1, 1), ("D", 0, 2, 1), ("K", -1, 4), ("D", 0, 2, 0),
-    ("D", 0, 2, 2), ("C", 0, 1, 2), ("D", 0, 3, 0), ("D", 0, 3, 1), ("C", 0, 1, 0), ("D", 0, 3, 2), ("A", 0, 5, 1),
-    ("B", 0, 0, 1), ("B", 0, 0, 2), ("A", 0, 5, 0), ("L", -1, 4), ("D", 0, 1, 1), ("E", 0, 2), ("A", 0, 5, 2),
-    ("D", 0, 1, 2), ("E", 0, 3), ("C", 0, 0, 0), ("D", 0, 1, 0), ("C", 0, 0, 1), ("A", 0, 4, 2), ("A", 0, 4, 1),
-    ("G", 0, 2), ("B", 0, 5, 1), ("C", 0, 0, 2), ("A", 0, 4, 0), ("B", 0, 5, 2), ("G", 0, 3), ("E", 0, 1),
-    ("B", 0, 5, 0), ("B", 0, 4, 2), ("B", 0, 4, 1), ("H", 0, 2), ("D", 0, 0, 2), ("D", 0, 0, 0), ("D", 0, 0, 1),
-    ("B", 0, 4, 0), ("C", 0, 5, 1), ("C", 0, 5, 2), ("H", 0, 3), ("G", 0, 1), ("C", 0, 5, 0), ("C", 0, 4, 2),
-    ("C", 0, 4, 1), ("I", 0, 2), ("E", 0, 0), ("C", 0, 4, 0), ("D", 0, 5, 2), ("D", 0, 5, 1), ("D", 0, 5, 0),
-    ("I", 0, 3), ("D", 0, 4, 1), ("J", 0, 2), ("H", 0, 1), ("D", 0, 4, 2), ("D", 0, 4, 0), ("G", 0, 0), ("V", 1, 2),
-    ("E", 0, 5), ("J", 0, 3), ("Q", 0, 2), ("E", 0, 4), ("I", 0, 1), ("Q", 0, 3), ("H", 0, 0), ("G", 0, 5),
-    ("K", 0, 2), ("J", 0, 1), ("V", 1, 1), ("G", 0, 4), ("K", 0, 3), ("H", 0, 5), ("I", 0, 0), ("Q", 0, 1),
-    ("L", 0, 2), ("H", 0, 4), ("L", 0, 3), ("J", 0, 0), ("I", 0, 5), ("K", 0, 1), ("A", 1, 2, 0), ("A", 1, 2, 1),
-    ("I", 0, 4), ("Q", 0, 0), ("J", 0, 5), ("A", 1, 3, 1), ("L", 0, 1), ("J", 0, 4), ("B", 1, 2, 0), ("A", 1, 3, 0),
-    ("B", 1, 2, 1), ("K", 0, 0), ("B", 1, 3, 1), ("Q", 0, 5), ("A", 1, 1, 1), ("Q", 0, 4), ("C", 1, 2, 0),
-    ("L", 0, 0), ("W", 1, 3), ("A", 1, 1, 0), ("C", 1, 3, 1), ("B", 1, 3, 0), ("K", 0, 4), ("C", 1, 2, 1),
-    ("B", 1, 1, 1), ("A", 1, 0, 1), ("D", 1, 3, 1), ("L", 0, 4), ("V", 1, 3), ("B", 1, 1, 0), ("C", 1, 3, 0),
-    ("K", 0, 5), ("D", 1, 2, 0), ("A", 1, 0, 0), ("B", 1, 0, 1), ("D", 1, 2, 1), ("C", 1, 1, 0), ("C", 1, 1, 1),
-    ("L", 0, 5), ("D", 1, 3, 0), ("A", 1, 4, 0), ("B", 1, 0, 0), ("A", 1, 4, 1), ("E", 1, 2), ("C", 1, 0, 1),
-    ("E", 1, 3), ("D", 1, 1, 1), ("D", 1, 1, 0), ("B", 1, 4, 0), ("C", 1, 0, 0), ("A", 1, 5, 1), ("G", 1, 2),
-    ("A", 1, 5, 0), ("G", 1, 3), ("B", 1, 4, 1), ("E", 1, 1), ("D", 1, 0, 0), ("B", 1, 5, 1), ("D", 1, 0, 1),
-    ("H", 1, 2), ("B", 1, 5, 0), ("C", 1, 4, 0), ("H", 1, 3), ("C", 1, 4, 1), ("C", 1, 5, 1), ("G", 1, 1),
-    ("E", 1, 0), ("C", 1, 5, 0), ("D", 1, 4, 0), ("D", 1, 4, 1), ("I", 1, 3), ("I", 1, 2), ("D", 1, 5, 1),
-    ("D", 1, 5, 0), ("H", 1, 1), ("G", 1, 0), ("E", 1, 4), ("J", 1, 3), ("J", 1, 2), ("E", 1, 5), ("H", 1, 0),
-    ("I", 1, 1), ("G", 1, 4), ("K", 1, 3), ("K", 1, 2), ("J", 1, 1), ("G", 1, 5), ("I", 1, 0), ("H", 1, 4),
-    ("L", 1, 3), ("L", 1, 2), ("K", 1, 1), ("J", 1, 0), ("H", 1, 5), ("I", 1, 4), ("L", 1, 1), ("M", 1, 3),
-    ("M", 1, 2), ("K", 1, 0), ("I", 1, 5), ("J", 1, 4), ("M", 1, 1), ("L", 1, 0), ("J", 1, 5), ("M", 1, 0),
+    ("X", 0, 0), ("W", 0, 0), ("W", 1, 2), ("S", 0, 0), ("W", 1, 0), ("X", 0, 3), ("X", 0, 5), ("X", 0, 1),
+    ("V", 0, 0), ("K", -1, 0), ("X", 0, 2), ("V", 1, 2), ("S", 0, 3), ("S", 0, 5), ("S", 0, 1), ("W", 0, 1),
+    ("L", -1, 0), ("K", -1, 3), ("W", 1, 1), ("K", -1, 1), ("V", 0, 1), ("A", 0, 0, 0), ("W", 0, 2), ("L", -1, 3),
+    ("K", -1, 5), ("V", 1, 1), ("L", -1, 1), ("A", 0, 0, 1), ("A", 0, 3, 1), ("L", -1, 5), ("A", 0, 3, 0),
+    ("V", 0, 2), ("B", 0, 0, 0), ("S", 0, 2), ("A", 0, 1, 0), ("X", 0, 4), ("A", 0, 1, 1), ("B", 0, 3, 1),
+    ("B", 0, 0, 1), ("W", 0, 3), ("B", 0, 3, 0), ("A", 0, 5, 0), ("A", 0, 3, 2), ("S", 0, 4), ("K", -1, 2),
+    ("A", 0, 0, 2), ("C", 0, 3, 1), ("A", 0, 1, 2), ("B", 0, 3, 2), ("C", 0, 3, 0), ("B", 0, 0, 2), ("L", -1, 2),
+    ("C", 0, 0, 0), ("V", 0, 3), ("B", 0, 1, 1), ("D", 0, 3, 1), ("A", 0, 5, 1), ("C", 0, 3, 2), ("D", 0, 3, 0),
+    ("C", 0, 0, 1), ("C", 0, 0, 2), ("B", 0, 1, 0), ("A", 0, 2, 1), ("K", -1, 4), ("D", 0, 3, 2), ("B", 0, 1, 2),
+    ("D", 0, 0, 0), ("A", 0, 2, 0), ("D", 0, 0, 2), ("D", 0, 0, 1), ("A", 0, 2, 2), ("B", 0, 5, 1), ("A", 0, 5, 2),
+    ("C", 0, 1, 0), ("L", -1, 4), ("B", 0, 2, 1), ("E", 0, 3), ("B", 0, 5, 0), ("C", 0, 1, 1), ("E", 0, 0),
+    ("C", 0, 1, 2), ("B", 0, 2, 0), ("B", 0, 2, 2), ("B", 0, 5, 2), ("A", 0, 4, 1), ("D", 0, 1, 0), ("G", 0, 3),
+    ("D", 0, 1, 1), ("D", 0, 1, 2), ("C", 0, 2, 1), ("C", 0, 5, 0), ("C", 0, 2, 0), ("G", 0, 0), ("C", 0, 2, 2),
+    ("A", 0, 4, 2), ("C", 0, 5, 2), ("H", 0, 3), ("C", 0, 5, 1), ("A", 0, 4, 0), ("E", 0, 1), ("D", 0, 2, 2),
+    ("D", 0, 2, 1), ("H", 0, 0), ("D", 0, 2, 0), ("B", 0, 4, 2), ("B", 0, 4, 1), ("I", 0, 3), ("D", 0, 5, 0),
+    ("D", 0, 5, 2), ("D", 0, 5, 1), ("B", 0, 4, 0), ("G", 0, 1), ("E", 0, 2), ("I", 0, 0), ("J", 0, 3),
+    ("C", 0, 4, 1), ("E", 0, 5), ("C", 0, 4, 2), ("C", 0, 4, 0), ("H", 0, 1), ("J", 0, 0), ("G", 0, 2), ("Q", 0, 3),
+    ("D", 0, 4, 1), ("D", 0, 4, 2), ("D", 0, 4, 0), ("G", 0, 5), ("I", 0, 1), ("Q", 0, 0), ("H", 0, 2), ("K", 0, 3),
+    ("V", 1, 0), ("E", 0, 4), ("J", 0, 1), ("H", 0, 5), ("L", 0, 3), ("I", 0, 2), ("K", 0, 0), ("G", 0, 4),
+    ("Q", 0, 1), ("I", 0, 5), ("J", 0, 2), ("A", 1, 3, 0), ("A", 1, 3, 1), ("L", 0, 0), ("K", 0, 1), ("Q", 0, 2),
+    ("J", 0, 5), ("H", 0, 4), ("B", 1, 3, 0), ("B", 1, 3, 1), ("A", 1, 0, 1), ("L", 0, 1), ("Q", 0, 5),
+    ("A", 1, 0, 0), ("I", 0, 4), ("W", 1, 3), ("K", 0, 2), ("C", 1, 3, 0), ("C", 1, 3, 1), ("B", 1, 0, 1),
+    ("A", 1, 1, 0), ("B", 1, 0, 0), ("J", 0, 4), ("L", 0, 2), ("A", 1, 1, 1), ("K", 0, 5), ("C", 1, 0, 1),
+    ("B", 1, 1, 0), ("A", 1, 2, 0), ("C", 1, 0, 0), ("Q", 0, 4), ("B", 1, 1, 1), ("D", 1, 3, 1), ("L", 0, 5),
+    ("V", 1, 3), ("A", 1, 2, 1), ("K", 0, 4), ("B", 1, 2, 0), ("D", 1, 3, 0), ("D", 1, 0, 0), ("D", 1, 0, 1),
+    ("C", 1, 1, 0), ("C", 1, 1, 1), ("A", 1, 5, 1), ("A", 1, 5, 0), ("B", 1, 2, 1), ("L", 0, 4), ("E", 1, 3),
+    ("E", 1, 0), ("D", 1, 1, 0), ("C", 1, 2, 0), ("D", 1, 1, 1), ("B", 1, 5, 1), ("A", 1, 4, 1), ("G", 1, 3),
+    ("C", 1, 2, 1), ("A", 1, 4, 0), ("B", 1, 5, 0), ("D", 1, 2, 0), ("G", 1, 0), ("E", 1, 1), ("B", 1, 4, 1),
+    ("H", 1, 3), ("D", 1, 2, 1), ("B", 1, 4, 0), ("C", 1, 5, 1), ("G", 1, 1), ("C", 1, 5, 0), ("H", 1, 0),
+    ("C", 1, 4, 1), ("I", 1, 3), ("E", 1, 2), ("C", 1, 4, 0), ("D", 1, 5, 1), ("D", 1, 5, 0), ("H", 1, 1),
+    ("I", 1, 0), ("D", 1, 4, 1), ("D", 1, 4, 0), ("J", 1, 3), ("G", 1, 2), ("E", 1, 5), ("J", 1, 0), ("I", 1, 1),
+    ("E", 1, 4), ("H", 1, 2), ("G", 1, 5), ("K", 1, 3), ("K", 1, 0), ("J", 1, 1), ("G", 1, 4), ("I", 1, 2),
+    ("H", 1, 5), ("L", 1, 3), ("L", 1, 0), ("K", 1, 1), ("J", 1, 2), ("H", 1, 4), ("M", 1, 3), ("I", 1, 5),
+    ("L", 1, 1), ("M", 1, 0), ("K", 1, 2), ("I", 1, 4), ("J", 1, 5), ("M", 1, 1), ("L", 1, 2), ("J", 1, 4),
+    ("M", 1, 2),
 ]
 
 
@@ -128,7 +129,7 @@
 
     other = (ra_at, y * 2 + (1 - c))
 
-    peers = [at_z(zp), at_z(zo), at_z(zm), at_x(xp), at_x(xo), at_x(xm), at_y(yp), at_y(ym), other]
+    peers = [at_z(zp), at_z(zm), at_x(xp), at_x(xm), at_y(yp), at_y(ym), other]
     peers += [(z * 4 + xp, y * 2 + (1 - c)), (z * 4 + xm, y * 2 + (1 - c))]
     peers += [(zp * 4 + x, y * 2 + (1 - c)), (zm * 4 + x, y * 2 + (1 - c))]
     barrier = pltpu.get_barrier_semaphore()
@@ -540,7 +541,6 @@
         def stage_w_both(l, j):
             if l + j == 0:
                 stage_w(l, j)
-                gains_send()
                 return
             pl.semaphore_signal(go, inc=1, device_id=other, device_id_type=MESH)
             stage_w(l, j)
@@ -551,6 +551,8 @@
         )
         for stage, *key in ORDER:
             stages[stage](*key)
+            if stage == "C" and not gain_copies:
+                gains_send()
             wait_sent(WAIT_LATER)
         for k in DIRECT:
             rows = pl.ds(k * TC, TC)

time: 124 us -> 125 us (level)
  no operation moved by 1% of the time
where the time goes in v9:
time: 125 us
  Pallas kernels  123 us (98%)
  local copies, waits for them, and re-layouts  2.06 us (2%)
    pallas_call x1, Pallas kernels, per_device(): pl.pallas_call(kernel, out_shape=jax.ShapeDtypeStruct((T, DB), BF), in_sp...  123 us

profile of v9, /device:TPU:1, one launch (start us, length us, event | category | flops | bytes accessed | tf_op | source)
XLA Modules:
  0.0 124.6 jit_solution(416386552125022971)
XLA Ops:
  0.0 122.5 %shard_map.64 = bf16[1536,256]{1,0:T(8,128)(2,1)} custom-call(bf16[1536,256]{1,0:T(8,128)(2,1)} %x_hbm.1, bf16[2,256,1408]{2,1,0:T(8,128)(2,1)} %wg_hbm.1, bf16[2,256,1408]{2,1,0:T(8,128)(2,1)} %wu_hbm.1, bf16[2,11,128,256]{3,2,1,0:T(8,128)(2,1)} %bitcast.1, f32[2,256]{1,0:T(2,128)} %gain_hbm.1, f32[2,256]{1,0:T(2,128)} %shift_hbm.1), custom_call_target="tpu_custom_call" | custom-call | tf_op jit(solution)/shard_map/pallas_call | solution.py:580
  122.5 2.1 %copy.8 = bf16[1536,256]{1,0:T(8,128)(2,1)} copy(bf16[1536,256]{1,0:T(8,128)(2,1)} %shard_map.64) | data formatting | bytes 1572864

commit v10 on v8

--- a/solution.py
+++ b/solution.py
@@ -128,7 +128,7 @@
 
     other = (ra_at, y * 2 + (1 - c))
 
-    peers = [at_z(zp), at_z(zo), at_z(zm), at_x(xp), at_x(xo), at_x(xm), at_y(yp), at_y(ym), other]
+    peers = [at_z(zp), at_z(zm), at_x(xp), at_x(xm), at_y(yp), at_y(ym), other]
     peers += [(z * 4 + xp, y * 2 + (1 - c)), (z * 4 + xm, y * 2 + (1 - c))]
     peers += [(zp * 4 + x, y * 2 + (1 - c)), (zm * 4 + x, y * 2 + (1 - c))]
     barrier = pltpu.get_barrier_semaphore()
@@ -540,7 +540,6 @@
         def stage_w_both(l, j):
             if l + j == 0:
                 stage_w(l, j)
-                gains_send()
                 return
             pl.semaphore_signal(go, inc=1, device_id=other, device_id_type=MESH)
             stage_w(l, j)
@@ -551,6 +550,8 @@
         )
         for stage, *key in ORDER:
             stages[stage](*key)
+            if stage == "C" and not gain_copies:
+                gains_send()
             wait_sent(WAIT_LATER)
         for k in DIRECT:
             rows = pl.ds(k * TC, TC)

time: 124 us -> 124 us (level)
  no operation moved by 1% of the time
where the time goes in v10:
time: 124 us
  Pallas kernels  122 us (98%)
  local copies, waits for them, and re-layouts  2.06 us (2%)
    pallas_call x1, Pallas kernels, per_device(): pl.pallas_call(kernel, out_shape=jax.ShapeDtypeStruct((T, DB), BF), in_sp...  122 us

profile of v10, /device:TPU:1, one launch (start us, length us, event | category | flops | bytes accessed | tf_op | source)
XLA Modules:
  0.0 124.1 jit_solution(9177828091485227256)
XLA Ops:
  0.0 122.0 %shard_map.64 = bf16[1536,256]{1,0:T(8,128)(2,1)} custom-call(bf16[1536,256]{1,0:T(8,128)(2,1)} %x_hbm.1, bf16[2,256,1408]{2,1,0:T(8,128)(2,1)} %wg_hbm.1, bf16[2,256,1408]{2,1,0:T(8,128)(2,1)} %wu_hbm.1, bf16[2,11,128,256]{3,2,1,0:T(8,128)(2,1)} %bitcast.1, f32[2,256]{1,0:T(2,128)} %gain_hbm.1, f32[2,256]{1,0:T(2,128)} %shift_hbm.1), custom_call_target="tpu_custom_call" | custom-call | tf_op jit(solution)/shard_map/pallas_call | solution.py:579
  122.0 2.1 %copy.8 = bf16[1536,256]{1,0:T(8,128)(2,1)} copy(bf16[1536,256]{1,0:T(8,128)(2,1)} %shard_map.64) | data formatting | bytes 1572864
